TPU v7x, 32 devices: a whole 2x2x4 slice. The times are simulated.
32 devices in a mesh: kv: 8 (over z, x), tp: 4 (over y, core).
Axes of the slice: x: 2, y: 2, z: 4, core: 2. Of those that a mesh axis runs over, the one named last changes fastest.
Arguments:
- tokens: bfloat16 [64, 2048], P(None, 'kv'), may hold values from -16 to 16
- norm_gain: float32 [2048], P('kv'), may hold values from 0.1 to 1.9
- query_weight: bfloat16 [2048, 2048], P('kv', 'tp'), may hold values from -0.125 to 0.125
- key_weight: bfloat16 [2048, 2048], P('kv', 'tp'), may hold values from -0.125 to 0.125
- value_weight: bfloat16 [2048, 2048], P('kv', 'tp'), may hold values from -0.125 to 0.125
- gate_weight: bfloat16 [2048, 2048], P('kv', 'tp'), may hold values from -0.125 to 0.125
- beta_weight: bfloat16 [2048, 16], replicated, may hold values from -0.125 to 0.125
- decay_weight: bfloat16 [2048, 16], replicated, may hold values from -0.5 to 0.5
- decay_rate: float32 [16], P('tp'), may hold values from 0.0005 to 0.1
- head_gain: float32 [128], replicated, may hold values from 0.1 to 1.9
- carried_state: float32 [64, 16, 128, 128], P('kv', 'tp'), may hold values from -4 to 4
- block_keys: bfloat16 [64, 16, 64, 128], P('kv', 'tp'), may hold values from -1 to 1, as said below
- block_values: bfloat16 [64, 16, 64, 128], P('kv', 'tp'), may hold values from -6 to 6
- block_beta: float32 [64, 16, 64], P('kv', 'tp'), may hold values from 0.1 to 0.9
- block_decay: float32 [64, 16, 64], P('kv', 'tp'), may hold values from -1.2 to 0
- live_count: int32 [64], P('kv'), may hold values from 1 to 64, 1638 in all
- out_weight: bfloat16 [2048, 2048], P('tp', 'kv'), may hold values from -0.125 to 0.125
- mlp_gain: float32 [2048], replicated, may hold values from 0.1 to 1.9
- up_weight: bfloat16 [2048, 8192], P('kv', 'tp'), may hold values from -0.125 to 0.125
- down_weight: bfloat16 [8192, 2048], P('tp', 'kv'), may hold values from -0.0625 to 0.0625
Outputs:
- mixed: bfloat16 [64, 2048], P(None, 'kv')
- new_state: float32 [64, 16, 128, 128], P('kv', 'tp')
Inputs may be any that keep to these rules, and one draw needn't show every extreme that they name: `block_keys`: every key vector along the last dimension has unit length up to rounding.
All inputs are finite; a program needn't handle non-finite values. No bound on the sum of `live_count` on one device may be relied on, other than what follows from the above.
Results may differ from a plain program's by a relative error of at most 0.023.
Values may be sent and summed in bfloat16 or wider, within the bound.
No kernel may reach another device: no remote copies, remote signals or barrier semaphores. Data moves between devices by JAX's collectives and lax.ppermute only.
A program may use at most 64 MiB of HBM per device.

v0:
```python
import jax
import jax.numpy as jnp
from jax import lax
from jax.sharding import PartitionSpec as P

MODEL = 2048


EPS = 1e-06
PRECISE = lax.Precision.HIGHEST


def unit_inverse(strict_lower):
    slots_count = strict_lower.shape[-1]
    identity = jnp.eye(slots_count, dtype=strict_lower.dtype)
    powered = -strict_lower
    product_sum = identity + powered
    for repeat in range(slots_count.bit_length() - 2):
        powered = jnp.matmul(powered, powered, precision=PRECISE)
        product_sum = product_sum + jnp.matmul(product_sum, powered, precision=PRECISE)
    return product_sum


def delta_block(
    queries,
    key_new,
    value_new,
    beta_new,
    decay_new,
    keys,
    values,
    betas,
    decays,
    live_count,
    carried_state,
):
    slots_count = keys.shape[2]
    slot_ids = jnp.arange(slots_count, dtype=jnp.int32)
    newest = (live_count - 1)[:, None, None]
    pending = slot_ids[None, None, :] < newest
    current = slot_ids[None, None, :] == newest
    keys_all = jnp.where(
        pending[..., None],
        keys,
        jnp.where(current[..., None], key_new[:, :, None, :], jnp.zeros_like(keys)),
    )
    values_all = jnp.where(
        pending[..., None],
        values,
        jnp.where(current[..., None], value_new[:, :, None, :], jnp.zeros_like(values)),
    )
    betas_all = jnp.where(pending, betas, jnp.where(current, beta_new[:, :, None], 0.0))
    decays_all = jnp.where(pending, decays, jnp.where(current, decay_new[:, :, None], 0.0))
    totals = jnp.cumsum(decays_all, axis=2)
    strict = slot_ids[:, None] > slot_ids[None, :]
    spread = jnp.where(strict, totals[..., :, None] - totals[..., None, :], 0.0)
    intersection = jnp.einsum(
        "shid,shjd->shij", keys_all, keys_all, preferred_element_type=jnp.float32
    )
    strict_lower = jnp.where(strict, betas_all[..., :, None] * intersection * jnp.exp(spread), 0.0)
    inverse = unit_inverse(strict_lower)
    key_vals = keys_all.astype(jnp.float32)
    right_values = betas_all[..., None] * values_all.astype(jnp.float32)
    right_keys = (betas_all * jnp.exp(totals))[..., None] * key_vals
    solved_values = jnp.einsum("shij,shjv->shiv", inverse, right_values, precision=PRECISE)
    solved_keys = jnp.einsum("shij,shjk->shik", inverse, right_keys, precision=PRECISE)
    update = solved_values - jnp.einsum(
        "shik,shkv->shiv", solved_keys, carried_state, precision=PRECISE
    )
    ending = totals[..., -1]
    faded_keys = key_vals * jnp.exp(ending[..., None] - totals)[..., None]
    new_state = jnp.exp(ending)[..., None, None] * carried_state + jnp.einsum(
        "shik,shiv->shkv", faded_keys, update, precision=PRECISE
    )
    readout = jnp.einsum("shk,shkv->shv", queries, new_state, precision=PRECISE)
    return (readout, new_state)


def body(
    tokens,
    norm_gain,
    query_weight,
    key_weight,
    value_weight,
    gate_weight,
    beta_weight,
    decay_weight,
    decay_rate,
    head_gain,
    carried_state,
    block_keys,
    block_values,
    block_beta,
    block_decay,
    live_count,
    out_weight,
    mlp_gain,
    up_weight,
    down_weight,
):
    kv_index = lax.axis_index("kv")
    tp_index = lax.axis_index("tp")
    columns = tokens.shape[1]
    seqs_here = carried_state.shape[0]
    heads_here = carried_state.shape[1]
    head_width = carried_state.shape[2]
    token_vals = tokens.astype(jnp.float32)
    squares = jnp.sum(token_vals * token_vals, axis=1)
    normed = (token_vals * norm_gain).astype(jnp.bfloat16)
    stacked = jnp.concatenate([query_weight, key_weight, value_weight, gate_weight], axis=1)
    beta_part = lax.dynamic_slice(
        beta_weight, (kv_index * columns, tp_index * heads_here), (columns, heads_here)
    )
    decay_part = lax.dynamic_slice(
        decay_weight, (kv_index * columns, tp_index * heads_here), (columns, heads_here)
    )
    small_weights = jnp.concatenate([beta_part, decay_part], axis=1)
    projected = jnp.dot(normed, stacked, preferred_element_type=jnp.float32)
    gating = jnp.dot(normed, small_weights, preferred_element_type=jnp.float32)
    projected, gating, squares = (
        lax.psum_scatter(
            projected.astype(jnp.bfloat16), "kv", scatter_dimension=0, tiled=True
        ).astype(jnp.float32),
        lax.psum_scatter(gating.astype(jnp.bfloat16), "kv", scatter_dimension=0, tiled=True).astype(
            jnp.float32
        ),
        lax.psum_scatter(
            squares.astype(jnp.bfloat16), "kv", scatter_dimension=0, tiled=True
        ).astype(jnp.float32),
    )
    inverse_rms = lax.rsqrt(squares / MODEL + EPS)[:, None]
    projected = (projected * inverse_rms).reshape(seqs_here, 4, heads_here, head_width)
    gating = gating * inverse_rms
    queries = projected[:, 0]
    key_raw = projected[:, 1]
    key_new = (key_raw * lax.rsqrt(jnp.sum(key_raw * key_raw, axis=2, keepdims=True) + EPS)).astype(
        jnp.bfloat16
    )
    value_new = projected[:, 2].astype(jnp.bfloat16)
    gate_raw = projected[:, 3]
    beta_new = jax.nn.sigmoid(gating[:, :heads_here])
    decay_new = -decay_rate * jax.nn.softplus(gating[:, heads_here:])
    readout, new_state = delta_block(
        queries,
        key_new,
        value_new,
        beta_new,
        decay_new,
        block_keys,
        block_values,
        block_beta,
        block_decay,
        live_count,
        carried_state,
    )
    scaled = (
        readout * lax.rsqrt(jnp.mean(readout * readout, axis=2, keepdims=True) + EPS) * head_gain
    )
    mixed_heads = (
        (scaled * jax.nn.silu(gate_raw))
        .reshape(seqs_here, heads_here * head_width)
        .astype(jnp.bfloat16)
    )
    attended = jnp.dot(
        lax.all_gather(mixed_heads, "kv", axis=0, tiled=True),
        out_weight,
        preferred_element_type=jnp.float32,
    )
    attended = lax.psum(attended.astype(jnp.bfloat16), "tp").astype(jnp.float32)
    residual = lax.optimization_barrier((token_vals + attended).astype(jnp.bfloat16))
    resid_vals = residual.astype(jnp.float32)
    mlp_squares = jnp.sum(resid_vals * resid_vals, axis=1)
    gain_part = lax.dynamic_slice_in_dim(mlp_gain, kv_index * columns, columns, 0)
    mlp_in = (resid_vals * gain_part).astype(jnp.bfloat16)
    pre_act = jnp.dot(mlp_in, up_weight, preferred_element_type=jnp.float32)
    pre_act, mlp_squares = (
        lax.psum_scatter(
            pre_act.astype(jnp.bfloat16), "kv", scatter_dimension=0, tiled=True
        ).astype(jnp.float32),
        lax.psum_scatter(
            mlp_squares.astype(jnp.bfloat16), "kv", scatter_dimension=0, tiled=True
        ).astype(jnp.float32),
    )
    hidden = jnp.square(
        jax.nn.relu(pre_act * lax.rsqrt(mlp_squares / MODEL + EPS)[:, None])
    ).astype(jnp.bfloat16)
    output_part = jnp.dot(
        lax.all_gather(hidden, "kv", axis=0, tiled=True),
        down_weight,
        preferred_element_type=jnp.float32,
    )
    output_part = lax.psum(output_part.astype(jnp.bfloat16), "tp").astype(jnp.float32)
    mixed = (resid_vals + output_part).astype(jnp.bfloat16)
    return (mixed, new_state)


def solution(mesh):
    placed = (
        P(None, "kv"),
        P("kv"),
        P("kv", "tp"),
        P("kv", "tp"),
        P("kv", "tp"),
        P("kv", "tp"),
        P(),
        P(),
        P("tp"),
        P(),
        P("kv", "tp", None, None),
        P("kv", "tp", None, None),
        P("kv", "tp", None, None),
        P("kv", "tp", None),
        P("kv", "tp", None),
        P("kv"),
        P("tp", "kv"),
        P(),
        P("kv", "tp"),
        P("tp", "kv"),
    )
    return jax.shard_map(
        body,
        mesh=mesh,
        in_specs=placed,
        out_specs=(P(None, "kv"), P("kv", "tp", None, None)),
        check_vma=False,
    )
```

profile of v0, /device:TPU:0, one launch (start us, length us, event | category | flops | bytes accessed | tf_op | source)
XLA Modules:
  0.0 257.9 jit_solution(3725630350873671478)
XLA Ops:
  7.3 2.4 convolution_convert_fusion.1
  9.8 0.1 fusion.32
  9.9 0.8 dynamic_slice.10
  10.7 0.8 dynamic_slice.9
  11.4 0.1 convolution_convert_fusion.4
  11.6 38.9 %all-reduce.3 = (bf16[64]{0:T(256)(128)(2,1)S(1)}, bf16[64,8]{1,0:T(8,128)(2,1)S(1)}) all-reduce(bf16[64]{0:T(256)(128)(2,1)S(1)} %fusion.32, bf16[64,8]{1,0:T(8,128)(2,1)S(1)} %convolution_convert_fusion.4), channel_id=3, replica_groups=mesh['kv'=8,'tp'=4] {'kv'}, use_global_device_ids=true, to_apply=%region_2.0.clone | all-reduce | flops 576 | bytes 2304
  50.5 0.6 dynamic-slice
  52.0 0.1 copy.48
  52.1 0.1 iota_compare_fusion.3
  52.1 0.1 copy.53
  52.3 0.9 reduce_window_sum.11
  53.2 0.2 slice_reduce_fusion
  53.4 0.1 exponential_multiply_fusion
  53.5 0.1 copy.50
  53.6 0.8 dynamic_slice.11
  54.4 23.1 %reduce-scatter.3.cloned.1.call-done = bf16[8,2048]{1,0:T(8,128)(2,1)} async-done(((bf16[64,2048]{1,0:T(8,128)(2,1)}), bf16[8,2048]{1,0:T(8,128)(2,1)}) %reduce-scatter.3.cloned.1.call-update) | async-done | bytes 32784 | tf_op jit(solution)/shard_map/reduce_scatter | solution.py:121
  77.5 0.8 convert_multiply_fusion.8
  78.3 0.1 multiply_reduce_fusion
  78.5 0.9 fusion.2
  79.4 1.2 fusion.66
  80.6 1.2 fusion.67
  81.8 1.3 convolution_add_fusion.4
  83.1 1.2 fusion.68
  84.4 1.2 convolution_add_fusion.3
  85.6 1.2 fusion.69
  86.8 1.2 convolution_add_fusion.2
  88.0 1.2 fusion.70
  89.2 1.4 convolution_add_fusion.1
  90.6 1.2 convolution_add_fusion
  91.8 1.3 fusion.3
  93.2 1.3 fusion.11
  94.6 2.1 convolution_subtract_fusion
  96.7 4.3 %multiply_add_fusion = f32[8,4,128,128]{3,2,1,0:T(8,128)S(1)} fusion(f32[8,4,128,128]{3,2,1,0:T(8,128)S(1)} %copy-done.1, f32[8,4,64,128]{3,2,1,0:T(8,128)S(1)} %convolution_subtract_fusion, f32[8,4]{1,0:T(8,128)S(1)} %copy.50, f32[8,4,64]{2,1,0:T(4,128)S(1)} %copy.52, bf16[8,4,64,128]{3,2,1,0:T(8,128)(2,1)S(1)} %copy-done.4, ...), kind=kOutput, calls=%fused_computation.2 | convolution fusion | flops 404750336 | bytes 5784704 | tf_op jit(solution)/shard_map/shik,shiv->shkv/dot_general | solution.py:72
  101.0 1.9 fusion.46
  102.9 0.1 fusion.42
  103.1 30.6 %all_gather.6 = bf16[64,512]{1,0:T(8,128)(2,1)S(1)} all-gather(bf16[8,512]{1,0:T(8,128)(2,1)S(1)} %fusion.49), channel_id=1, replica_groups=mesh['kv'=8,'tp'=4] {'kv'}, dimensions={0}, use_global_device_ids=true | all-gather | bytes 73728 | tf_op jit(solution)/shard_map/all_gather | solution.py:165
  133.6 0.2 convolution_convert_fusion.3
  133.8 10.3 %psum.14 = bf16[64,256]{1,0:T(8,128)(2,1)S(1)} all-reduce(bf16[64,256]{1,0:T(8,128)(2,1)S(1)} %convolution_convert_fusion.3), channel_id=1, replica_groups=mesh['kv'=8,'tp'=4] {'tp'}, use_global_device_ids=true, to_apply=%region_7.8 | all-reduce | flops 16384 | bytes 65536 | tf_op jit(solution)/shard_map/psum | solution.py:169
  144.1 1.0 convolution_convert_fusion
  145.1 0.1 fusion.35
  145.2 19.5 %all-reduce.2 = bf16[64]{0:T(256)(128)(2,1)S(1)} all-reduce(bf16[64]{0:T(256)(128)(2,1)S(1)} %fusion.35), channel_id=6, replica_groups=mesh['kv'=8,'tp'=4] {'kv'}, use_global_device_ids=true, to_apply=%region_10.11.clone | all-reduce | flops 64 | bytes 256
  164.7 0.1 fusion.59
  164.8 42.1 %reduce-scatter.5.cloned.1.call-done = bf16[8,2048]{1,0:T(8,128)(2,1)} async-done(((bf16[64,2048]{1,0:T(8,128)(2,1)}), bf16[8,2048]{1,0:T(8,128)(2,1)}) %reduce-scatter.5.cloned.1.call-update) | async-done | bytes 32784 | tf_op jit(solution)/shard_map/reduce_scatter | solution.py:177
  206.9 0.8 multiply_convert_fusion
  207.7 30.9 %all_gather.7 = bf16[64,2048]{1,0:T(8,128)(2,1)S(1)} all-gather(bf16[8,2048]{1,0:T(8,128)(2,1)S(1)} %multiply_convert_fusion), channel_id=1, replica_groups=mesh['kv'=8,'tp'=4] {'kv'}, dimensions={0}, use_global_device_ids=true | all-gather | bytes 294912 | tf_op jit(solution)/shard_map/all_gather | solution.py:188
  238.6 1.5 convolution_convert_fusion.2
  240.2 10.3 %psum.15 = bf16[64,256]{1,0:T(8,128)(2,1)S(1)} all-reduce(bf16[64,256]{1,0:T(8,128)(2,1)S(1)} %convolution_convert_fusion.2), channel_id=1, replica_groups=mesh['kv'=8,'tp'=4] {'tp'}, use_global_device_ids=true, to_apply=%region_11.12 | all-reduce | flops 16384 | bytes 65536 | tf_op jit(solution)/shard_map/psum | solution.py:192
  250.4 0.6 fusion.36
  (56 shorter events, 0.8 us)
Async XLA Ops:
  7.2 136.9 %copy-start = (bf16[256,2048]{1,0:T(8,128)(2,1)S(1)}, bf16[256,2048]{1,0:T(8,128)(2,1)}, u32[]{:S(2)}) copy-start(bf16[256,2048]{1,0:T(8,128)(2,1)} %param.38) | copy-start | bytes 3145732
  7.2 43.3 %copy-start.14 = (u32[32]{0:T(128)S(1)}, u32[32]{0:T(128)}, u32[]{:S(2)}) copy-start(u32[32]{0:T(128)} %constant.49) | copy-start | bytes 388
  7.2 2.6 copy-start.7
  7.2 4.2 %copy-start.11 = (f32[256]{0:T(256)S(1)}, f32[256]{0:T(256)}, u32[]{:S(2)}) copy-start(f32[256]{0:T(256)} %param.21) | copy-start | bytes 3076
  7.2 4.2 %copy-start.12 = (f32[4]{0:T(128)S(1)}, f32[4]{0:T(128)}, u32[]{:S(2)}) copy-start(f32[4]{0:T(128)} %param.28) | copy-start | bytes 52
  7.2 44.8 %copy-start.13 = (s32[8]{0:T(128)S(1)}, s32[8]{0:T(128)}, u32[]{:S(2)}) copy-start(s32[8]{0:T(128)} %param.35) | copy-start | bytes 100
  7.2 45.0 %copy-start.8 = (f32[8,4,64]{2,1,0:T(4,128)S(1)}, f32[8,4,64]{2,1,0:T(4,128)}, u32[]{:S(2)}) copy-start(f32[8,4,64]{2,1,0:T(4,128)} %param.34) | copy-start | bytes 24580
  7.2 46.1 %copy-start.9 = (f32[8,4,64]{2,1,0:T(4,128)S(1)}, f32[8,4,64]{2,1,0:T(4,128)}, u32[]{:S(2)}) copy-start(f32[8,4,64]{2,1,0:T(4,128)} %param.33) | copy-start | bytes 24580
  7.3 71.2 %copy-start.3 = (bf16[8,4,64,128]{3,2,1,0:T(8,128)(2,1)S(1)}, bf16[8,4,64,128]{3,2,1,0:T(8,128)(2,1)}, u32[]{:S(2)}) copy-start(bf16[8,4,64,128]{3,2,1,0:T(8,128)(2,1)} %param.31) | copy-start | bytes 1572868
  7.3 70.2 %reduce-scatter.3.cloned.1.call-start = ((), (), s32[]{:S(2)}) async-start(), calls=%async_computation.2 | async-start | bytes 294912 | tf_op jit(solution)/shard_map/reduce_scatter | solution.py:121
  9.7 197.2 %reduce-scatter.5.cloned.1.call-start = ((), (), s32[]{:S(2)}) async-start(), calls=%async_computation.3 | async-start | bytes 294912 | tf_op jit(solution)/shard_map/reduce_scatter | solution.py:177
  91.8 1.4 copy-start.5
  91.8 2.7 %copy-start.1 = (f32[8,4,128,128]{3,2,1,0:T(8,128)S(1)}, f32[8,4,128,128]{3,2,1,0:T(8,128)}, u32[]{:S(2)}) copy-start(f32[8,4,128,128]{3,2,1,0:T(8,128)} %param.30) | copy-start | bytes 6291460
  94.6 2.1 copy-start.4
  101.0 44.2 %copy-start.2 = (f32[8,4,128,128]{3,2,1,0:T(8,128)}, f32[8,4,128,128]{3,2,1,0:T(8,128)S(1)}, u32[]{:S(2)}) copy-start(f32[8,4,128,128]{3,2,1,0:T(8,128)S(1)} %multiply_add_fusion) | copy-start | bytes 6291460
  101.0 2.0 copy-start.10
  101.0 32.6 %copy-start.6 = (bf16[512,256]{1,0:T(8,128)(2,1)S(1)}, bf16[512,256]{1,0:T(8,128)(2,1)}, u32[]{:S(2)}) copy-start(bf16[512,256]{1,0:T(8,128)(2,1)} %param.36) | copy-start | bytes 786436
Sparse Core Ops, SparseCore 0:
  12.0 65.4 reduce-scatter.2
  145.2 61.5 reduce-scatter.4
where the time goes:
time: 258 us
  blocking collectives  140 us (54%)
  waiting for transfers between devices  65.2 us (25%)
  matrix products  29.3 us (11%)
  between operations  15.1 us (6%)
  other arithmetic  4.31 us (2%)
  local copies, waits for them, and re-layouts  3.42 us (1%)
    unnamed x2, blocking collectives  58.4 us
    reduce_scatter x1, waiting for transfers between devices, body(): lax.psum_scatter(pre_act.astype(jnp.bfloat16), 'kv', scatter_dimension=0,...  42.1 us
    all_gather x1, blocking collectives, body(): lax.all_gather(hidden, 'kv', axis=0, tiled=True)  30.9 us
    all_gather x1, blocking collectives, body(): lax.all_gather(mixed_heads, 'kv', axis=0, tiled=True)  30.6 us
    reduce_scatter x1, waiting for transfers between devices, body(): lax.psum_scatter(projected.astype(jnp.bfloat16), 'kv', scatter_dimension=...  23.1 us
    psum x1, blocking collectives, body(): attended = lax.psum(attended.astype(jnp.bfloat16), 'tp').astype(jnp.float32)  10.3 us
    psum x1, blocking collectives, body(): lax.psum(output_part.astype(jnp.bfloat16), 'tp').astype(jnp.float32)  10.3 us
    dot_general x5, matrix products, unit_inverse(): jnp.matmul(product_sum, powered, precision=PRECISE)  6.34 us
  transfers between devices with their start and end apart: 2, of which 2 were waited for; matrix products, arithmetic and copies ran while one was open for 2% of the time, Pallas kernels for 0%

commit v1 on v0

--- a/solution.py
+++ b/solution.py
@@ -74,6 +74,38 @@
     )
     readout = jnp.einsum("shk,shkv->shv", queries, new_state, precision=PRECISE)
     return (readout, new_state)
+
+
+def scatter_sum(wide, extras):
+    parts = lax.axis_size("kv")
+    rows, width = wide.shape
+    count = extras.shape[1]
+    high = extras.astype(jnp.bfloat16)
+    low = (extras - high.astype(jnp.float32)).astype(jnp.bfloat16)
+    padding = jnp.zeros((rows, 128 - 2 * count), jnp.bfloat16)
+    payload = jnp.concatenate([wide.astype(jnp.bfloat16), high, low, padding], axis=1)
+    payload = payload.reshape(parts, rows // parts, width + 128)
+    arrived = lax.all_to_all(payload, "kv", 0, 0, tiled=True).astype(jnp.float32)
+    summed = jnp.sum(arrived, axis=0)
+    tail = summed[:, width:]
+    return summed[:, :width], tail[:, :count] + tail[:, count : 2 * count]
+
+
+def gather_rows(mine):
+    parts = lax.axis_size("kv")
+    rows, width = mine.shape
+    copies = jnp.broadcast_to(mine[None], (parts, rows, width))
+    return lax.all_to_all(copies, "kv", 0, 0, tiled=True).reshape(parts * rows, width)
+
+
+def sum_over_tp(part):
+    count = lax.axis_size("tp")
+    mine = part.astype(jnp.bfloat16)
+    total = mine.astype(jnp.float32)
+    for step in range(1, count):
+        swaps = [(place, place ^ step) for place in range(count)]
+        total = total + lax.ppermute(mine, "tp", swaps).astype(jnp.float32)
+    return total
 
 
 def body(
@@ -104,6 +136,7 @@
     seqs_here = carried_state.shape[0]
     heads_here = carried_state.shape[1]
     head_width = carried_state.shape[2]
+    width = 4 * heads_here * head_width
     token_vals = tokens.astype(jnp.float32)
     squares = jnp.sum(token_vals * token_vals, axis=1)
     normed = (token_vals * norm_gain).astype(jnp.bfloat16)
@@ -117,20 +150,11 @@
     small_weights = jnp.concatenate([beta_part, decay_part], axis=1)
     projected = jnp.dot(normed, stacked, preferred_element_type=jnp.float32)
     gating = jnp.dot(normed, small_weights, preferred_element_type=jnp.float32)
-    projected, gating, squares = (
-        lax.psum_scatter(
-            projected.astype(jnp.bfloat16), "kv", scatter_dimension=0, tiled=True
-        ).astype(jnp.float32),
-        lax.psum_scatter(gating.astype(jnp.bfloat16), "kv", scatter_dimension=0, tiled=True).astype(
-            jnp.float32
-        ),
-        lax.psum_scatter(
-            squares.astype(jnp.bfloat16), "kv", scatter_dimension=0, tiled=True
-        ).astype(jnp.float32),
-    )
-    inverse_rms = lax.rsqrt(squares / MODEL + EPS)[:, None]
+    extras = jnp.concatenate([squares[:, None], gating], axis=1)
+    projected, extras = scatter_sum(projected, extras)
+    inverse_rms = lax.rsqrt(extras[:, :1] / MODEL + EPS)
+    gating = extras[:, 1:] * inverse_rms
     projected = (projected * inverse_rms).reshape(seqs_here, 4, heads_here, head_width)
-    gating = gating * inverse_rms
     queries = projected[:, 0]
     key_raw = projected[:, 1]
     key_new = (key_raw * lax.rsqrt(jnp.sum(key_raw * key_raw, axis=2, keepdims=True) + EPS)).astype(
@@ -161,36 +185,20 @@
         .reshape(seqs_here, heads_here * head_width)
         .astype(jnp.bfloat16)
     )
-    attended = jnp.dot(
-        lax.all_gather(mixed_heads, "kv", axis=0, tiled=True),
-        out_weight,
-        preferred_element_type=jnp.float32,
-    )
-    attended = lax.psum(attended.astype(jnp.bfloat16), "tp").astype(jnp.float32)
+    attended = jnp.dot(gather_rows(mixed_heads), out_weight, preferred_element_type=jnp.float32)
+    attended = sum_over_tp(attended)
     residual = lax.optimization_barrier((token_vals + attended).astype(jnp.bfloat16))
     resid_vals = residual.astype(jnp.float32)
-    mlp_squares = jnp.sum(resid_vals * resid_vals, axis=1)
+    mlp_squares = jnp.sum(resid_vals * resid_vals, axis=1, keepdims=True)
     gain_part = lax.dynamic_slice_in_dim(mlp_gain, kv_index * columns, columns, 0)
     mlp_in = (resid_vals * gain_part).astype(jnp.bfloat16)
     pre_act = jnp.dot(mlp_in, up_weight, preferred_element_type=jnp.float32)
-    pre_act, mlp_squares = (
-        lax.psum_scatter(
-            pre_act.astype(jnp.bfloat16), "kv", scatter_dimension=0, tiled=True
-        ).astype(jnp.float32),
-        lax.psum_scatter(
-            mlp_squares.astype(jnp.bfloat16), "kv", scatter_dimension=0, tiled=True
-        ).astype(jnp.float32),
-    )
-    hidden = jnp.square(
-        jax.nn.relu(pre_act * lax.rsqrt(mlp_squares / MODEL + EPS)[:, None])
-    ).astype(jnp.bfloat16)
-    output_part = jnp.dot(
-        lax.all_gather(hidden, "kv", axis=0, tiled=True),
-        down_weight,
-        preferred_element_type=jnp.float32,
-    )
-    output_part = lax.psum(output_part.astype(jnp.bfloat16), "tp").astype(jnp.float32)
-    mixed = (resid_vals + output_part).astype(jnp.bfloat16)
+    pre_act, mlp_squares = scatter_sum(pre_act, mlp_squares)
+    hidden = jnp.square(jax.nn.relu(pre_act * lax.rsqrt(mlp_squares / MODEL + EPS))).astype(
+        jnp.bfloat16
+    )
+    output_part = jnp.dot(gather_rows(hidden), down_weight, preferred_element_type=jnp.float32)
+    mixed = (resid_vals + sum_over_tp(output_part)).astype(jnp.bfloat16)
     return (mixed, new_state)
 
 

time: 258 us -> 97.8 us (0.38)
  blocking collectives: 140 us -> 35.2 us
  waiting for transfers between devices: 65.2 us -> 14 us
  between operations: 15.1 us -> 1.11 us
  starting transfers between devices: 0.08 us -> 11.1 us
    reduce_scatter x2 -> x0, waiting for transfers between devices: 65.2 us -> none  [the longest x1 42.1 us: body(): lax.psum_scatter(pre_act.astype(jnp.bfloat16), 'kv', scatter_dimension=0,...]
    all_gather x2 -> x0, blocking collectives: 61.5 us -> none  [the longest x1 30.9 us: body(): lax.all_gather(hidden, 'kv', axis=0, tiled=True)]
    unnamed x2 -> x0, blocking collectives: 58.4 us -> none
    all_to_all x0 -> x3, blocking collectives: none -> 35.2 us  [the longest x2 22 us: gather_rows(): lax.all_to_all(copies, 'kv', 0, 0, tiled=True).reshape(parts * rows, width)]
    psum x2 -> x0, blocking collectives: 20.5 us -> none  [the longest x1 10.3 us: body(): attended = lax.psum(attended.astype(jnp.bfloat16), 'tp').astype(jnp.float32)]
    all_to_all x0 -> x1, waiting for transfers between devices: none -> 9.12 us  [scatter_sum(): lax.all_to_all(payload, 'kv', 0, 0, tiled=True).astype(jnp.float32)]
    all_to_all x0 -> x1, starting transfers between devices: none -> 7.28 us  [scatter_sum(): lax.all_to_all(payload, 'kv', 0, 0, tiled=True).astype(jnp.float32)]
    ppermute x0 -> x6, waiting for transfers between devices: none -> 4.88 us  [sum_over_tp(): total = total + lax.ppermute(mine, 'tp', swaps).astype(jnp.float32)]
  transfers between devices with their start and end apart: 2 -> 7, of which waited for: 2 -> 5; matrix products, arithmetic and copies ran while one was open for 2% -> 1% of each run, Pallas kernels for 0% -> 0%
where the time goes in v1:
time: 97.8 us; the launch traced here: 97.2 us
  blocking collectives  35.2 us (36%)
  matrix products  27.5 us (28%)
  waiting for transfers between devices  14 us (14%)
  starting transfers between devices  11.1 us (11%)
  local copies, waits for them, and re-layouts  4.43 us (5%)
  other arithmetic  3.92 us (4%)
  between operations  1.11 us (1%)
    all_to_all x2, blocking collectives, gather_rows(): lax.all_to_all(copies, 'kv', 0, 0, tiled=True).reshape(parts * rows, width)  22 us
    all_to_all x1, blocking collectives, scatter_sum(): lax.all_to_all(payload, 'kv', 0, 0, tiled=True).astype(jnp.float32)  13.2 us
    all_to_all x1, waiting for transfers between devices, scatter_sum(): lax.all_to_all(payload, 'kv', 0, 0, tiled=True).astype(jnp.float32)  9.12 us
    all_to_all x1, starting transfers between devices, scatter_sum(): lax.all_to_all(payload, 'kv', 0, 0, tiled=True).astype(jnp.float32)  7.28 us
    dot_general x5, matrix products, unit_inverse(): jnp.matmul(product_sum, powered, precision=PRECISE)  6.38 us
    dot_general x5, matrix products, unit_inverse(): powered = jnp.matmul(powered, powered, precision=PRECISE)  5.98 us
    ppermute x6, waiting for transfers between devices, sum_over_tp(): total = total + lax.ppermute(mine, 'tp', swaps).astype(jnp.float32)  4.88 us
    dot_general x1, matrix products, delta_block(): jnp.einsum('shik,shiv->shkv', faded_keys, update, precision=PRECISE)  4.26 us
  transfers between devices with their start and end apart: 7, of which 5 were waited for; matrix products, arithmetic and copies ran while one was open for 1% of the time, Pallas kernels for 0%

profile of v1, /device:TPU:0, one launch (start us, length us, event | category | flops | bytes accessed | tf_op | source)
XLA Modules:
  0.0 97.2 jit_solution(493984767193832922)
XLA Ops:
  0.7 0.9 dynamic_slice.10
  1.5 0.8 dynamic_slice.9
  2.3 0.9 fusion.34
  3.1 0.9 fusion.46
  4.1 0.1 copy.96
  4.2 0.1 copy.97
  4.3 1.6 %convolution_convert_fusion.1 = bf16[64,2048]{1,0:T(8,128)(2,1)S(1)} fusion(bf16[256,512]{1,0:T(8,128)(2,1)} %param.25, bf16[256,512]{1,0:T(8,128)(2,1)} %param.24, bf16[256,512]{1,0:T(8,128)(2,1)} %param.23, bf16[256,512]{1,0:T(8,128)(2,1)} %param.22, bf16[64,256]{1,0:T(8,128)(2,1)} %param.20, f32[256]{0:T(256)} %param.21), kind=kOutput, calls=%fused_computation.1 | convolution fusion | flops 71483392 | bytes 1344512 | tf_op jit(solution)/shard_map/dot_general | solution.py:151
  5.9 0.8 concatenate.21
  6.7 7.3 %all-to-all-start = ((bf16[8,8,2176]{2,1,0:T(8,128)(2,1)}), bf16[8,8,2176]{2,1,0:T(8,128)(2,1)S(1)}, u32[]{:S(2)}, u32[]{:S(2)}) async-start(bf16[8,8,2176]{2,1,0:T(8,128)(2,1)} %bitcast.1), calls=%async_computation | async-start | bytes 557056 | tf_op jit(solution)/shard_map/all_to_all | solution.py:88
  14.2 9.1 %all-to-all-done = bf16[8,8,2176]{2,1,0:T(8,128)(2,1)S(1)} async-done(((bf16[8,8,2176]{2,1,0:T(8,128)(2,1)}), bf16[8,8,2176]{2,1,0:T(8,128)(2,1)S(1)}, u32[]{:S(2)}, u32[]{:S(2)}) %all-to-all-start) | async-done | bytes 278560 | tf_op jit(solution)/shard_map/all_to_all | solution.py:88
  23.4 0.1 rsqrt_reduce_fusion
  23.9 0.9 reduce_window_sum.11
  24.8 0.2 slice_reduce_fusion
  25.4 0.9 fusion.3
  26.3 1.2 %fusion.74 = f32[8,4,64,64]{3,2,1,0:T(8,128)S(1)} fusion(f32[8,4,64,64]{3,2,1,0:T(8,128)S(1)} %fusion.3), kind=kOutput, calls=%fused_computation.124 | convolution fusion | flops 100663296 | bytes 1048576 | tf_op jit(solution)/shard_map/dot_general | solution.py:19
  27.5 1.2 %fusion.75 = f32[8,4,64,64]{3,2,1,0:T(8,128)S(1)} fusion(f32[8,4,64,64]{3,2,1,0:T(8,128)S(1)} %fusion.74), kind=kOutput, calls=%fused_computation.125 | convolution fusion | flops 100663296 | bytes 1048576 | tf_op jit(solution)/shard_map/dot_general | solution.py:19
  28.7 1.3 %convolution_add_fusion.4 = f32[8,4,64,64]{3,2,1,0:T(8,128)S(1)} fusion(f32[8,4,64,64]{3,2,1,0:T(8,128)S(1)} %fusion.74, f32[8,4,64,64]{3,2,1,0:T(8,128)S(1)} %fusion.3, f32[64,64]{1,0:T(8,128)S(1)} %fusion.45), kind=kOutput, calls=%fused_computation.8 | convolution fusion | flops 100925440 | bytes 1589248 | tf_op jit(solution)/shard_map/dot_general | solution.py:20
  30.0 1.2 %fusion.76 = f32[8,4,64,64]{3,2,1,0:T(8,128)S(1)} fusion(f32[8,4,64,64]{3,2,1,0:T(8,128)S(1)} %fusion.75), kind=kOutput, calls=%fused_computation.126 | convolution fusion | flops 100663296 | bytes 1048576 | tf_op jit(solution)/shard_map/dot_general | solution.py:19
  31.2 1.2 %convolution_add_fusion.3 = f32[8,4,64,64]{3,2,1,0:T(8,128)S(1)} fusion(f32[8,4,64,64]{3,2,1,0:T(8,128)S(1)} %convolution_add_fusion.4, f32[8,4,64,64]{3,2,1,0:T(8,128)S(1)} %fusion.75), kind=kOutput, calls=%fused_computation.7 | convolution fusion | flops 100794368 | bytes 1572864 | tf_op jit(solution)/shard_map/dot_general | solution.py:20
  32.4 1.2 %fusion.77 = f32[8,4,64,64]{3,2,1,0:T(8,128)S(1)} fusion(f32[8,4,64,64]{3,2,1,0:T(8,128)S(1)} %fusion.76), kind=kOutput, calls=%fused_computation.127 | convolution fusion | flops 100663296 | bytes 1048576 | tf_op jit(solution)/shard_map/dot_general | solution.py:19
  33.6 1.2 %convolution_add_fusion.2 = f32[8,4,64,64]{3,2,1,0:T(8,128)S(1)} fusion(f32[8,4,64,64]{3,2,1,0:T(8,128)S(1)} %convolution_add_fusion.3, f32[8,4,64,64]{3,2,1,0:T(8,128)S(1)} %fusion.76), kind=kOutput, calls=%fused_computation.6 | convolution fusion | flops 100794368 | bytes 1572864 | tf_op jit(solution)/shard_map/dot_general | solution.py:20
  34.9 1.2 %fusion.78 = f32[8,4,64,64]{3,2,1,0:T(8,128)S(1)} fusion(f32[8,4,64,64]{3,2,1,0:T(8,128)S(1)} %fusion.77), kind=kOutput, calls=%fused_computation.128 | convolution fusion | flops 100663296 | bytes 1048576 | tf_op jit(solution)/shard_map/dot_general | solution.py:19
  36.1 1.4 %convolution_add_fusion.1 = f32[8,4,64,64]{3,2,1,0:T(8,128)S(1)} fusion(f32[8,4,64,64]{3,2,1,0:T(8,128)S(1)} %convolution_add_fusion.2, f32[8,4,64,64]{3,2,1,0:T(8,128)S(1)} %fusion.77), kind=kOutput, calls=%fused_computation.5 | convolution fusion | flops 100794368 | bytes 1572864 | tf_op jit(solution)/shard_map/dot_general | solution.py:20
  37.6 1.3 %convolution_add_fusion = f32[8,4,64,64]{3,2,1,0:T(8,128)S(1)} fusion(f32[8,4,64,64]{3,2,1,0:T(8,128)S(1)} %convolution_add_fusion.1, f32[8,4,64,64]{3,2,1,0:T(8,128)S(1)} %fusion.78), kind=kOutput, calls=%fused_computation.4 | convolution fusion | flops 100794368 | bytes 1572864 | tf_op jit(solution)/shard_map/dot_general | solution.py:20
  38.9 1.3 %fusion.4 = f32[8,4,64,128]{3,2,1,0:T(8,128)S(1)} fusion(f32[8,4,64,64]{3,2,1,0:T(8,128)S(1)} %convolution_add_fusion, f32[8,4,64]{2,1,0:T(4,128)S(1)} %copy.110, bf16[8,4,64,128]{3,2,1,0:T(8,128)(2,1)S(1)} %copy-done.4, pred[8,64]{1,0:T(8,128)(4,1)S(1)} %get-tuple-element.10, pred[8,64]{1,0:T(8,128)(4,1)S(1)} %get-tuple-element.9, ...), kind=kOutput, calls=%fused_computation.18 | convolution fusion | flops 202375168 | bytes 2114560 | tf_op jit(solution)/shard_map/shij,shjk->shik/dot_general | solution.py:66
  40.2 1.3 %fusion.12 = f32[8,4,64,128]{3,2,1,0:T(8,128)S(1)} fusion(f32[8,4,64,64]{3,2,1,0:T(8,128)S(1)} %convolution_add_fusion, bf16[8,4,64,128]{3,2,1,0:T(8,128)(2,1)S(1)} %copy-done.6, f32[8,4,64]{2,1,0:T(4,128)S(1)} %copy.105, pred[8,64]{1,0:T(8,128)(4,1)S(1)} %get-tuple-element.10, pred[8,64]{1,0:T(8,128)(4,1)S(1)} %get-tuple-element.9, ...), kind=kOutput, calls=%fused_computation.26 | convolution fusion | flops 202375168 | bytes 2114560 | tf_op jit(solution)/shard_map/shij,shjv->shiv/dot_general | solution.py:65
  41.6 2.1 %convolution_subtract_fusion = f32[8,4,64,128]{3,2,1,0:T(8,128)S(1)} fusion(f32[8,4,64,128]{3,2,1,0:T(8,128)S(1)} %fusion.12, f32[8,4,64,128]{3,2,1,0:T(8,128)S(1)} %fusion.4, f32[8,4,128,128]{3,2,1,0:T(8,128)S(1)} %copy-done.1), kind=kOutput, calls=%fused_computation.9 | convolution fusion | flops 402915328 | bytes 5242880 | tf_op jit(solution)/shard_map/shik,shkv->shiv/dot_general | solution.py:67
  43.7 4.3 %multiply_add_fusion = f32[8,4,128,128]{3,2,1,0:T(8,128)S(1)} fusion(f32[8,4,128,128]{3,2,1,0:T(8,128)S(1)} %copy-done.1, f32[8,4,64,128]{3,2,1,0:T(8,128)S(1)} %convolution_subtract_fusion, f32[8,4]{1,0:T(8,128)S(1)} %copy.100, f32[8,4,64]{2,1,0:T(4,128)S(1)} %copy.102, bf16[8,4,64,128]{3,2,1,0:T(8,128)(2,1)S(1)} %copy-done.4, ...), kind=kOutput, calls=%fused_computation.3 | convolution fusion | flops 404750336 | bytes 5784704 | tf_op jit(solution)/shard_map/shik,shiv->shkv/dot_general | solution.py:72
  48.0 1.9 %fusion.53 = f32[8,4,1,128]{3,2,1,0:T(1,128)S(1)} fusion(f32[8,4,128,128]{3,2,1,0:T(8,128)S(1)} %multiply_add_fusion, f32[8,4,128,1]{2,0,1,3:T(8,128)S(1)} %slice_bitcast_fusion.2), kind=kOutput, calls=%fused_computation.84 | convolution fusion | flops 6291456 | bytes 2129920 | tf_op jit(solution)/shard_map/shk,shkv->shv/dot_general | solution.py:75
  50.1 10.3 %all_to_all.20 = bf16[8,8,512]{2,1,0:T(8,128)(2,1)S(1)} all-to-all(bf16[8,8,512]{2,1,0:T(8,128)(2,1)S(1)} %broadcast_in_dim.149), channel_id=1, replica_groups=mesh['kv'=8,'tp'=4] {'kv'}, dimensions={0} | all-to-all | bytes 131072 | tf_op jit(solution)/shard_map/all_to_all | solution.py:98
  60.4 0.2 convolution_convert_fusion.3
  60.6 1.6 %collective-permute-start.1 = (bf16[64,256]{1,0:T(8,128)(2,1)S(1)}, bf16[64,256]{1,0:T(8,128)(2,1)S(1)}, u32[]{:S(2)}, u32[]{:S(2)}) collective-permute-start(bf16[64,256]{1,0:T(8,128)(2,1)S(1)} %convolution_convert_fusion.3), channel_id=1, source_target_pairs={{0,2},{1,3},{2,0},{3,1},{4,6},{5,7},{6,4},{7,5},{8,10},{9,11},{10,... | collective-permute-start | bytes 98312 | tf_op jit(solution)/shard_map/ppermute | solution.py:107
  62.2 0.3 collective-permute-start.2
  62.5 0.8 dynamic_slice.11
  63.3 1.4 %collective-permute-done.1 = bf16[64,256]{1,0:T(8,128)(2,1)S(1)} collective-permute-done((bf16[64,256]{1,0:T(8,128)(2,1)S(1)}, bf16[64,256]{1,0:T(8,128)(2,1)S(1)}, u32[]{:S(2)}, u32[]{:S(2)}) %collective-permute-start.1) | collective-permute-done | bytes 32800 | tf_op jit(solution)/shard_map/ppermute | solution.py:107
  64.6 1.0 collective-permute-done.2
  65.8 0.1 copy.112
  66.0 0.1 copy.113
  66.1 0.3 fusion
  66.6 13.2 %all_to_all.21 = bf16[8,8,2176]{2,1,0:T(8,128)(2,1)S(1)} all-to-all(bf16[8,8,2176]{2,1,0:T(8,128)(2,1)S(1)} %concatenate.23), channel_id=1, replica_groups=mesh['kv'=8,'tp'=4] {'kv'}, dimensions={0} | all-to-all | bytes 557056 | tf_op jit(solution)/shard_map/all_to_all | solution.py:88
  79.8 0.2 fusion.64
  80.1 11.7 %all_to_all.22 = bf16[8,8,2048]{2,1,0:T(8,128)(2,1)S(1)} all-to-all(bf16[8,8,2048]{2,1,0:T(8,128)(2,1)S(1)} %broadcast_in_dim.151), channel_id=1, replica_groups=mesh['kv'=8,'tp'=4] {'kv'}, dimensions={0} | all-to-all | bytes 524288 | tf_op jit(solution)/shard_map/all_to_all | solution.py:98
  91.8 0.3 convolution_convert_fusion.2
  92.2 0.9 collective-permute-start.4
  93.1 0.9 collective-permute-start.5
  94.0 2.2 %collective-permute-done.4 = bf16[64,256]{1,0:T(8,128)(2,1)S(1)} collective-permute-done((bf16[64,256]{1,0:T(8,128)(2,1)S(1)}, bf16[64,256]{1,0:T(8,128)(2,1)S(1)}, u32[]{:S(2)}, u32[]{:S(2)}) %collective-permute-start.4) | collective-permute-done | bytes 32800 | tf_op jit(solution)/shard_map/ppermute | solution.py:107
  96.2 0.4 collective-permute-done.5
  96.6 0.6 fusion.38
  (75 shorter events, 2.0 us)
Async XLA Ops:
  0.6 65.5 %copy-start = (bf16[256,2048]{1,0:T(8,128)(2,1)S(1)}, bf16[256,2048]{1,0:T(8,128)(2,1)}, u32[]{:S(2)}) copy-start(bf16[256,2048]{1,0:T(8,128)(2,1)} %param.38) | copy-start | bytes 3145732
  4.3 9.8 %copy-start.12 = (f32[4]{0:T(128)S(1)}, f32[4]{0:T(128)}, u32[]{:S(2)}) copy-start(f32[4]{0:T(128)} %param.28) | copy-start | bytes 52
  4.3 9.8 %copy-start.13 = (s32[8]{0:T(128)S(1)}, s32[8]{0:T(128)}, u32[]{:S(2)}) copy-start(s32[8]{0:T(128)} %param.35) | copy-start | bytes 100
  4.3 19.5 %copy-start.9 = (f32[8,4,64]{2,1,0:T(4,128)S(1)}, f32[8,4,64]{2,1,0:T(4,128)}, u32[]{:S(2)}) copy-start(f32[8,4,64]{2,1,0:T(4,128)} %param.34) | copy-start | bytes 24580
  4.3 20.9 %copy-start.10 = (f32[8,4,64]{2,1,0:T(4,128)S(1)}, f32[8,4,64]{2,1,0:T(4,128)}, u32[]{:S(2)}) copy-start(f32[8,4,64]{2,1,0:T(4,128)} %param.33) | copy-start | bytes 24580
  4.3 21.0 %copy-start.3 = (bf16[8,4,64,128]{3,2,1,0:T(8,128)(2,1)S(1)}, bf16[8,4,64,128]{3,2,1,0:T(8,128)(2,1)}, u32[]{:S(2)}) copy-start(bf16[8,4,64,128]{3,2,1,0:T(8,128)(2,1)} %param.31) | copy-start | bytes 1572868
  6.7 16.5 %all-to-all-start = ((bf16[8,8,2176]{2,1,0:T(8,128)(2,1)}), bf16[8,8,2176]{2,1,0:T(8,128)(2,1)S(1)}, u32[]{:S(2)}, u32[]{:S(2)}) async-start(bf16[8,8,2176]{2,1,0:T(8,128)(2,1)} %bitcast.1), calls=%async_computation | async-start | bytes 557056 | tf_op jit(solution)/shard_map/all_to_all | solution.py:88
  37.6 1.3 %copy-start.4 = (bf16[8,4,64,128]{3,2,1,0:T(8,128)(2,1)S(1)}, bf16[8,4,64,128]{3,2,1,0:T(8,128)(2,1)}, u32[]{:S(2)}) copy-start(bf16[8,4,64,128]{3,2,1,0:T(8,128)(2,1)} %param.31) | copy-start | bytes 1572868
  38.8 1.4 %copy-start.6 = (bf16[8,4,64,128]{3,2,1,0:T(8,128)(2,1)S(1)}, bf16[8,4,64,128]{3,2,1,0:T(8,128)(2,1)}, u32[]{:S(2)}) copy-start(bf16[8,4,64,128]{3,2,1,0:T(8,128)(2,1)} %param.32) | copy-start | bytes 1572868
  38.9 2.7 %copy-start.1 = (f32[8,4,128,128]{3,2,1,0:T(8,128)S(1)}, f32[8,4,128,128]{3,2,1,0:T(8,128)}, u32[]{:S(2)}) copy-start(f32[8,4,128,128]{3,2,1,0:T(8,128)} %param.30) | copy-start | bytes 6291460
  48.0 18.4 %copy-start.2 = (f32[8,4,128,128]{3,2,1,0:T(8,128)}, f32[8,4,128,128]{3,2,1,0:T(8,128)S(1)}, u32[]{:S(2)}) copy-start(f32[8,4,128,128]{3,2,1,0:T(8,128)S(1)} %multiply_add_fusion) | copy-start | bytes 6291460
  48.0 2.0 %copy-start.11 = (f32[128]{0:T(128)S(1)}, f32[128]{0:T(128)}, u32[]{:S(2)}) copy-start(f32[128]{0:T(128)} %param.29) | copy-start | bytes 1540
  48.0 12.4 %copy-start.7 = (bf16[512,256]{1,0:T(8,128)(2,1)S(1)}, bf16[512,256]{1,0:T(8,128)(2,1)}, u32[]{:S(2)}) copy-start(bf16[512,256]{1,0:T(8,128)(2,1)} %param.36) | copy-start | bytes 786436
  48.0 17.6 %copy-start.8 = (bf16[64,256]{1,0:T(8,128)(2,1)S(1)}, bf16[64,256]{1,0:T(8,128)(2,1)}, u32[]{:S(2)}) copy-start(bf16[64,256]{1,0:T(8,128)(2,1)} %param.20) | copy-start | bytes 98308
  60.6 2.7 %collective-permute-start = (bf16[64,256]{1,0:T(8,128)(2,1)S(1)}, bf16[64,256]{1,0:T(8,128)(2,1)S(1)}, u32[]{:S(2)}, u32[]{:S(2)}) collective-permute-start(bf16[64,256]{1,0:T(8,128)(2,1)S(1)} %convolution_convert_fusion.3), channel_id=1, source_target_pairs={{0,1},{1,0},{2,3},{3,2},{4,5},{5,4},{6,7},{7,6},{8,9},{9,8},{10,11... | collective-permute-start | bytes 98312 | tf_op jit(solution)/shard_map/ppermute | solution.py:107
  60.6 4.0 %collective-permute-start.1 = (bf16[64,256]{1,0:T(8,128)(2,1)S(1)}, bf16[64,256]{1,0:T(8,128)(2,1)S(1)}, u32[]{:S(2)}, u32[]{:S(2)}) collective-permute-start(bf16[64,256]{1,0:T(8,128)(2,1)S(1)} %convolution_convert_fusion.3), channel_id=1, source_target_pairs={{0,2},{1,3},{2,0},{3,1},{4,6},{5,7},{6,4},{7,5},{8,10},{9,11},{10,... | collective-permute-start | bytes 98312 | tf_op jit(solution)/shard_map/ppermute | solution.py:107
  62.2 3.4 %collective-permute-start.2 = (bf16[64,256]{1,0:T(8,128)(2,1)S(1)}, bf16[64,256]{1,0:T(8,128)(2,1)S(1)}, u32[]{:S(2)}, u32[]{:S(2)}) collective-permute-start(bf16[64,256]{1,0:T(8,128)(2,1)S(1)} %convolution_convert_fusion.3), channel_id=1, source_target_pairs={{0,3},{1,2},{2,1},{3,0},{4,7},{5,6},{6,5},{7,4},{8,11},{9,10},{10,... | collective-permute-start | bytes 98312 | tf_op jit(solution)/shard_map/ppermute | solution.py:107
  66.4 25.3 %copy-start.5 = (bf16[2048,256]{1,0:T(8,128)(2,1)S(1)}, bf16[2048,256]{1,0:T(8,128)(2,1)}, u32[]{:S(2)}) copy-start(bf16[2048,256]{1,0:T(8,128)(2,1)} %param.39) | copy-start | bytes 3145732
  92.1 1.9 %collective-permute-start.3 = (bf16[64,256]{1,0:T(8,128)(2,1)S(1)}, bf16[64,256]{1,0:T(8,128)(2,1)S(1)}, u32[]{:S(2)}, u32[]{:S(2)}) collective-permute-start(bf16[64,256]{1,0:T(8,128)(2,1)S(1)} %convolution_convert_fusion.2), channel_id=1, source_target_pairs={{0,1},{1,0},{2,3},{3,2},{4,5},{5,4},{6,7},{7,6},{8,9},{9,8},{10,11... | collective-permute-start | bytes 98312 | tf_op jit(solution)/shard_map/ppermute | solution.py:107
  92.2 4.0 %collective-permute-start.4 = (bf16[64,256]{1,0:T(8,128)(2,1)S(1)}, bf16[64,256]{1,0:T(8,128)(2,1)S(1)}, u32[]{:S(2)}, u32[]{:S(2)}) collective-permute-start(bf16[64,256]{1,0:T(8,128)(2,1)S(1)} %convolution_convert_fusion.2), channel_id=1, source_target_pairs={{0,2},{1,3},{2,0},{3,1},{4,6},{5,7},{6,4},{7,5},{8,10},{9,11},{10,... | collective-permute-start | bytes 98312 | tf_op jit(solution)/shard_map/ppermute | solution.py:107
  93.1 3.5 %collective-permute-start.5 = (bf16[64,256]{1,0:T(8,128)(2,1)S(1)}, bf16[64,256]{1,0:T(8,128)(2,1)S(1)}, u32[]{:S(2)}, u32[]{:S(2)}) collective-permute-start(bf16[64,256]{1,0:T(8,128)(2,1)S(1)} %convolution_convert_fusion.2), channel_id=1, source_target_pairs={{0,3},{1,2},{2,1},{3,0},{4,7},{5,6},{6,5},{7,4},{8,11},{9,10},{10,... | collective-permute-start | bytes 98312 | tf_op jit(solution)/shard_map/ppermute | solution.py:107

commit v2 on v1

--- a/solution.py
+++ b/solution.py
@@ -7,73 +7,65 @@
 
 
 EPS = 1e-06
-PRECISE = lax.Precision.HIGHEST
+def product(spec, left, right):
+    return jnp.einsum(
+        spec,
+        left.astype(jnp.bfloat16),
+        right.astype(jnp.bfloat16),
+        preferred_element_type=jnp.float32,
+    )
 
 
 def unit_inverse(strict_lower):
-    slots_count = strict_lower.shape[-1]
-    identity = jnp.eye(slots_count, dtype=strict_lower.dtype)
-    powered = -strict_lower
-    product_sum = identity + powered
-    for repeat in range(slots_count.bit_length() - 2):
-        powered = jnp.matmul(powered, powered, precision=PRECISE)
-        product_sum = product_sum + jnp.matmul(product_sum, powered, precision=PRECISE)
-    return product_sum
-
-
-def delta_block(
-    queries,
-    key_new,
-    value_new,
-    beta_new,
-    decay_new,
-    keys,
-    values,
-    betas,
-    decays,
-    live_count,
-    carried_state,
-):
-    slots_count = keys.shape[2]
-    slot_ids = jnp.arange(slots_count, dtype=jnp.int32)
-    newest = (live_count - 1)[:, None, None]
-    pending = slot_ids[None, None, :] < newest
-    current = slot_ids[None, None, :] == newest
-    keys_all = jnp.where(
-        pending[..., None],
-        keys,
-        jnp.where(current[..., None], key_new[:, :, None, :], jnp.zeros_like(keys)),
-    )
-    values_all = jnp.where(
-        pending[..., None],
-        values,
-        jnp.where(current[..., None], value_new[:, :, None, :], jnp.zeros_like(values)),
-    )
-    betas_all = jnp.where(pending, betas, jnp.where(current, beta_new[:, :, None], 0.0))
-    decays_all = jnp.where(pending, decays, jnp.where(current, decay_new[:, :, None], 0.0))
-    totals = jnp.cumsum(decays_all, axis=2)
-    strict = slot_ids[:, None] > slot_ids[None, :]
+    count = strict_lower.shape[-1]
+    row = jnp.arange(count)[:, None]
+    column = jnp.arange(count)[None, :]
+    inverse = jnp.eye(count, dtype=jnp.float32) + jnp.zeros_like(strict_lower)
+    size = 1
+    while size < count:
+        joins = (row // (2 * size) == column // (2 * size)) & (row // size != column // size)
+        corner = jnp.where(joins, strict_lower, 0.0)
+        if size == 1:
+            inverse = inverse - corner
+        else:
+            middle = product("shij,shjk->shik", inverse, corner)
+            inverse = inverse - product("shij,shjk->shik", middle, inverse)
+        size *= 2
+    return inverse
+
+
+def earlier_state(keys, values, betas, decays, live_count, carried_state):
+    count = keys.shape[2]
+    slots = jnp.arange(count, dtype=jnp.int32)
+    pending = (slots[None, :] < (live_count - 1)[:, None])[:, None, :]
+    betas = jnp.where(pending, betas, 0.0)
+    decays = jnp.where(pending, decays, 0.0)
+    upto = (slots[:, None] <= slots[None, :]).astype(jnp.float32)
+    totals = jnp.einsum("shi,ij->shj", decays, upto, precision=lax.Precision.HIGHEST)
+    strict = slots[:, None] > slots[None, :]
     spread = jnp.where(strict, totals[..., :, None] - totals[..., None, :], 0.0)
-    intersection = jnp.einsum(
-        "shid,shjd->shij", keys_all, keys_all, preferred_element_type=jnp.float32
-    )
-    strict_lower = jnp.where(strict, betas_all[..., :, None] * intersection * jnp.exp(spread), 0.0)
+    overlap = product("shid,shjd->shij", keys, keys)
+    strict_lower = jnp.where(strict, betas[..., :, None] * overlap * jnp.exp(spread), 0.0)
     inverse = unit_inverse(strict_lower)
-    key_vals = keys_all.astype(jnp.float32)
-    right_values = betas_all[..., None] * values_all.astype(jnp.float32)
-    right_keys = (betas_all * jnp.exp(totals))[..., None] * key_vals
-    solved_values = jnp.einsum("shij,shjv->shiv", inverse, right_values, precision=PRECISE)
-    solved_keys = jnp.einsum("shij,shjk->shik", inverse, right_keys, precision=PRECISE)
-    update = solved_values - jnp.einsum(
-        "shik,shkv->shiv", solved_keys, carried_state, precision=PRECISE
-    )
+    recalled = product("shik,shkv->shiv", keys, carried_state)
+    wanted = betas[..., None] * (values - jnp.exp(totals)[..., None] * recalled)
+    update = product("shij,shjv->shiv", inverse, wanted)
     ending = totals[..., -1]
-    faded_keys = key_vals * jnp.exp(ending[..., None] - totals)[..., None]
-    new_state = jnp.exp(ending)[..., None, None] * carried_state + jnp.einsum(
-        "shik,shiv->shkv", faded_keys, update, precision=PRECISE
-    )
-    readout = jnp.einsum("shk,shkv->shv", queries, new_state, precision=PRECISE)
-    return (readout, new_state)
+    faded = jnp.exp(ending[..., None] - totals)[..., None] * update
+    return jnp.exp(ending)[..., None, None] * carried_state + product(
+        "shik,shiv->shkv", keys, faded
+    )
+
+
+def newest_step(queries, key, value, beta, decay, state):
+    key = key.astype(jnp.float32)[..., None]
+    fade = jnp.exp(decay)[..., None]
+    recalled = fade * jnp.sum(key * state, axis=2)
+    update = beta[..., None] * (value.astype(jnp.float32) - recalled)
+    answered = fade * jnp.sum(queries[..., None] * state, axis=2)
+    readout = answered + jnp.sum(key[..., 0] * queries, axis=2, keepdims=True) * update
+    new_state = fade[..., None] * state + key * update[:, :, None, :]
+    return readout, new_state
 
 
 def scatter_sum(wide, extras):
@@ -164,19 +156,10 @@
     gate_raw = projected[:, 3]
     beta_new = jax.nn.sigmoid(gating[:, :heads_here])
     decay_new = -decay_rate * jax.nn.softplus(gating[:, heads_here:])
-    readout, new_state = delta_block(
-        queries,
-        key_new,
-        value_new,
-        beta_new,
-        decay_new,
-        block_keys,
-        block_values,
-        block_beta,
-        block_decay,
-        live_count,
-        carried_state,
-    )
+    state = earlier_state(
+        block_keys, block_values, block_beta, block_decay, live_count, carried_state
+    )
+    readout, new_state = newest_step(queries, key_new, value_new, beta_new, decay_new, state)
     scaled = (
         readout * lax.rsqrt(jnp.mean(readout * readout, axis=2, keepdims=True) + EPS) * head_gain
     )

time: 97.8 us -> 92 us (0.941)
  waiting for transfers between devices: 14 us -> 2.01 us
  other arithmetic: 3.92 us -> 8.14 us
  matrix products: 27.5 us -> 23.5 us
  local copies, waits for them, and re-layouts: 4.43 us -> 7.81 us
  blocking collectives: 35.2 us -> 37.6 us
    all_to_all x1, waiting for transfers between devices: 9.12 us -> 0.01 us  [scatter_sum(): lax.all_to_all(payload, 'kv', 0, 0, tiled=True).astype(jnp.float32)]
    dot_general x16 -> x9, matrix products: 24.2 us -> 18.4 us  [the longest x8 18.2 us: product(): jnp.einsum(spec, left.astype(jnp.bfloat16), right.astype(jnp.bfloat16), p...]
    ppermute x6, waiting for transfers between devices: 4.88 us -> 2.01 us  [sum_over_tp(): total = total + lax.ppermute(mine, 'tp', swaps).astype(jnp.float32)]
    all_to_all x2, blocking collectives: 22 us -> 24.4 us  [gather_rows(): lax.all_to_all(copies, 'kv', 0, 0, tiled=True).reshape(parts * rows, width)]
    add x0 -> x1, other arithmetic: none -> 1.7 us  [newest_step(): new_state = fade[..., None] * state + key * update[:, :, None, :]]
    dot_general x1, matrix products: 0.29 us -> 1.51 us  [body(): jnp.dot(gather_rows(hidden), down_weight, preferred_element_type=jnp.floa...]
    unnamed x28, local copies, waits for them, and re-layouts: 0.09 us -> 1.29 us
    concatenate x2, local copies, waits for them, and re-layouts: 0.9 us -> 2.01 us  [scatter_sum(): jnp.concatenate([wide.astype(jnp.bfloat16), high, low, padding], axis=1)]
  transfers between devices with their start and end apart: 7 -> 7, of which waited for: 5 -> 3; matrix products, arithmetic and copies ran while one was open for 1% -> 20% of each run, Pallas kernels for 0% -> 0%
where the time goes in v2:
time: 92 us; the launch traced here: 91.2 us
  blocking collectives  37.6 us (41%)
  matrix products  23.5 us (26%)
  starting transfers between devices  11.1 us (12%)
  other arithmetic  8.14 us (9%)
  local copies, waits for them, and re-layouts  7.81 us (8%)
  waiting for transfers between devices  2.01 us (2%)
  between operations  0.94 us (1%)
    all_to_all x2, blocking collectives, gather_rows(): lax.all_to_all(copies, 'kv', 0, 0, tiled=True).reshape(parts * rows, width)  24.4 us
    dot_general x8, matrix products, product(): jnp.einsum(spec, left.astype(jnp.bfloat16), right.astype(jnp.bfloat16), p...  18.2 us
    all_to_all x1, blocking collectives, scatter_sum(): lax.all_to_all(payload, 'kv', 0, 0, tiled=True).astype(jnp.float32)  13.3 us
    all_to_all x1, starting transfers between devices, scatter_sum(): lax.all_to_all(payload, 'kv', 0, 0, tiled=True).astype(jnp.float32)  7.28 us
    ppermute x6, starting transfers between devices, sum_over_tp(): total = total + lax.ppermute(mine, 'tp', swaps).astype(jnp.float32)  3.84 us
    concatenate x2, local copies, waits for them, and re-layouts, scatter_sum(): jnp.concatenate([wide.astype(jnp.bfloat16), high, low, padding], axis=1)  2.01 us
    ppermute x6, waiting for transfers between devices, sum_over_tp(): total = total + lax.ppermute(mine, 'tp', swaps).astype(jnp.float32)  2.01 us
  transfers between devices with their start and end apart: 7, of which 3 were waited for; matrix products, arithmetic and copies ran while one was open for 20% of the time, Pallas kernels for 0%

profile of v2, /device:TPU:0, one launch (start us, length us, event | category | flops | bytes accessed | tf_op | source)
XLA Modules:
  0.0 91.2 jit_solution(7106639098814874741)
XLA Ops:
  0.7 0.9 dynamic_slice.10
  1.5 0.8 dynamic_slice.9
  2.3 0.9 fusion.57
  3.1 0.9 fusion.73
  4.3 1.6 %convolution_convert_fusion.1 = bf16[64,2048]{1,0:T(8,128)(2,1)S(1)} fusion(bf16[256,512]{1,0:T(8,128)(2,1)} %param.25, bf16[256,512]{1,0:T(8,128)(2,1)} %param.24, bf16[256,512]{1,0:T(8,128)(2,1)} %param.23, bf16[256,512]{1,0:T(8,128)(2,1)} %param.22, bf16[64,256]{1,0:T(8,128)(2,1)} %param.20, f32[256]{0:T(256)} %param.21), kind=kOutput, calls=%fused_computation.1 | convolution fusion | flops 71483392 | bytes 1344512 | tf_op jit(solution)/shard_map/dot_general | solution.py:143
  5.9 0.8 concatenate.21
  6.7 7.3 %all-to-all-start = ((bf16[8,8,2176]{2,1,0:T(8,128)(2,1)}), bf16[8,8,2176]{2,1,0:T(8,128)(2,1)S(1)}, u32[]{:S(2)}, u32[]{:S(2)}) async-start(bf16[8,8,2176]{2,1,0:T(8,128)(2,1)} %bitcast.1), calls=%async_computation | async-start | bytes 557056 | tf_op jit(solution)/shard_map/all_to_all | solution.py:80
  14.2 0.1 fusion.69
  14.3 0.2 slice_reduce_fusion
  14.6 0.7 copy.94
  15.3 0.5 neg.19
  15.8 0.6 fusion.4
  16.5 0.1 compare_and_fusion
  16.6 0.4 convolution_subtract_fusion.4
  17.0 1.4 %convolution_subtract_fusion.3 = f32[8,4,64,64]{3,2,1,0:T(8,128)} fusion(f32[8,4,64,64]{3,2,1,0:T(8,128)S(1)} %convolution_subtract_fusion.4, f32[8,4,64,64]{3,2,1,0:T(8,128)S(1)} %fusion.4, pred[64,64]{1,0:T(8,128)(4,1)S(1)} %get-tuple-element.25), kind=kOutput, calls=%fused_computation.14 | convolution fusion | flops 34209792 | bytes 1576960 | tf_op jit(solution)/shard_map/shij,shjk->shik/dot_general | solution.py:11
  18.4 3.5 %convolution_subtract_fusion.2 = f32[8,4,64,64]{3,2,1,0:T(8,128)} fusion(f32[8,4,64,64]{3,2,1,0:T(8,128)} %convolution_subtract_fusion.3, f32[8,4,64,64]{3,2,1,0:T(8,128)S(1)} %fusion.4, pred[64,64]{1,0:T(8,128)(4,1)S(1)} %get-tuple-element.24), kind=kOutput, calls=%fused_computation.13 | convolution fusion | flops 34209792 | bytes 1576960 | tf_op jit(solution)/shard_map/shij,shjk->shik/dot_general | solution.py:11
  21.9 2.5 %convolution_subtract_fusion.1 = f32[8,4,64,64]{3,2,1,0:T(8,128)S(1)} fusion(f32[8,4,64,64]{3,2,1,0:T(8,128)} %convolution_subtract_fusion.2, f32[8,4,64,64]{3,2,1,0:T(8,128)S(1)} %fusion.4, pred[64,64]{1,0:T(8,128)(4,1)S(1)} %get-tuple-element.23), kind=kOutput, calls=%fused_computation.12 | convolution fusion | flops 34209792 | bytes 1576960 | tf_op jit(solution)/shard_map/shij,shjk->shik/dot_general | solution.py:11
  24.4 1.2 %fusion.6 = bf16[8,4,64,64]{3,2,1,0:T(8,128)(2,1)} fusion(f32[8,4,64,64]{3,2,1,0:T(8,128)S(1)} %convolution_subtract_fusion.1, f32[8,4,64,64]{3,2,1,0:T(8,128)S(1)} %fusion.4, pred[64,64]{1,0:T(8,128)(4,1)S(1)} %get-tuple-element.22), kind=kOutput, calls=%fused_computation.25 | convolution fusion | flops 34340864 | bytes 1314816 | tf_op jit(solution)/shard_map/shij,shjk->shik/dot_general | solution.py:11
  25.6 0.6 broadcast_bitcast_fusion.2
  26.2 3.4 %fusion.5 = bf16[8,4,64,128]{3,2,1,0:T(8,128)(2,1)} fusion(bf16[8,4,64,128]{3,2,1,0:T(8,128)(2,1)} %param.31, f32[8,4,128,128]{3,2,1,0:T(8,128)} %param.30, bf16[8,4,64,128]{3,2,1,0:T(8,128)(2,1)} %param.32, f32[8,4,64]{2,1,0:T(4,128)S(1)} %copy.98, f32[8,4,64]{2,1,0:T(4,128)S(1)} %get-tuple-element.20), kind=kOutput, calls=%fused_computation.19 | convolution fusion | flops 68943872 | bytes 3686400 | tf_op jit(solution)/shard_map/shik,shkv->shiv/dot_general | solution.py:11
  29.8 0.1 rsqrt_reduce_fusion
  30.1 0.6 copy.134
  30.8 0.8 multiply_reduce_fusion.3
  31.5 0.6 copy.135
  32.1 0.7 add_divide_fusion
  32.8 5.2 %multiply_reduce_fusion.1 = (f32[8,4,128]{2,1,0:T(4,128)}, f32[8,4,128]{2,1,0:T(4,128)}, f32[8,4,128,128]{3,2,1,0:T(8,128)}) fusion(f32[8,4,128]{2,1,0:T(4,128)} %bitcast.92, f32[8,4,128]{2,1,0:T(4,128)S(1)} %get-tuple-element.9, bf16[8,4,64,128]{3,2,1,0:T(8,128)(2,1)} %param.31, bf16[8,4,64,64]{3,2,1,0:T(8,128)(2,1)} %fusion.6, ...), kind=kOutput, calls=%fused_computation.6 | convolution fusion | flops 104325120 | bytes 5578880 | tf_op jit(solution)/shard_map/shik,shiv->shkv/dot_general | solution.py:11
  38.0 0.9 multiply_reduce_fusion.2
  39.0 0.8 fusion.82
  39.8 12.7 %all_to_all.20 = bf16[8,8,512]{2,1,0:T(8,128)(2,1)S(1)} all-to-all(bf16[8,8,512]{2,1,0:T(8,128)(2,1)S(1)} %broadcast_in_dim.114), channel_id=1, replica_groups=mesh['kv'=8,'tp'=4] {'kv'}, dimensions={0} | all-to-all | bytes 131072 | tf_op jit(solution)/shard_map/all_to_all | solution.py:90
  52.5 0.2 convolution_convert_fusion.8
  52.8 1.6 %collective-permute-start.1 = (bf16[64,256]{1,0:T(8,128)(2,1)S(1)}, bf16[64,256]{1,0:T(8,128)(2,1)S(1)}, u32[]{:S(2)}, u32[]{:S(2)}) collective-permute-start(bf16[64,256]{1,0:T(8,128)(2,1)S(1)} %convolution_convert_fusion.8), channel_id=1, source_target_pairs={{0,2},{1,3},{2,0},{3,1},{4,6},{5,7},{6,4},{7,5},{8,10},{9,11},{10,... | collective-permute-start | bytes 98312 | tf_op jit(solution)/shard_map/ppermute | solution.py:99
  54.3 0.3 collective-permute-start
  54.6 0.8 dynamic_slice.11
  55.4 1.0 %collective-permute-done.2 = bf16[64,256]{1,0:T(8,128)(2,1)S(1)} collective-permute-done((bf16[64,256]{1,0:T(8,128)(2,1)S(1)}, bf16[64,256]{1,0:T(8,128)(2,1)S(1)}, u32[]{:S(2)}, u32[]{:S(2)}) %collective-permute-start.2) | collective-permute-done | bytes 32800 | tf_op jit(solution)/shard_map/ppermute | solution.py:99
  56.4 0.4 collective-permute-done.1
  57.0 0.1 copy.102
  57.2 0.1 copy.103
  57.3 1.0 %fusion = bf16[8,8,2048]{2,1,0:T(8,128)(2,1)} fusion(bf16[256,2048]{1,0:T(8,128)(2,1)S(1)} %copy-done, bf16[64,256]{1,0:T(8,128)(2,1)S(1)} %fusion.58, f32[256]{0:T(256)S(1)} %dynamic_slice.11), kind=kOutput, calls=%fused_computation.2 | convolution fusion | flops 67289088 | bytes 1344512 | tf_op jit(solution)/shard_map/dot_general | solution.py:178
  58.3 1.2 %concatenate.23 = bf16[8,8,2176]{2,1,0:T(8,128)(2,1)S(1)} concatenate(bf16[8,8,2048]{2,1,0:T(8,128)(2,1)} %fusion, bf16[8,8,1]{2,1,0:T(8,128)(2,1)S(1)} %copy.102, bf16[8,8,1]{2,1,0:T(8,128)(2,1)S(1)} %copy.103, bf16[8,8,126]{2,1,0:T(8,128)(2,1)S(1)} %broadcast_in_dim.115), dimensions={2} | concatenate | bytes 557056 | tf_op jit(solution)/shard_map/concatenate | solution.py:78
  59.5 13.3 %all_to_all.21 = bf16[8,8,2176]{2,1,0:T(8,128)(2,1)S(1)} all-to-all(bf16[8,8,2176]{2,1,0:T(8,128)(2,1)S(1)} %concatenate.23), channel_id=1, replica_groups=mesh['kv'=8,'tp'=4] {'kv'}, dimensions={0} | all-to-all | bytes 557056 | tf_op jit(solution)/shard_map/all_to_all | solution.py:80
  72.8 0.2 fusion.95
  73.1 11.7 %all_to_all.22 = bf16[8,8,2048]{2,1,0:T(8,128)(2,1)S(1)} all-to-all(bf16[8,8,2048]{2,1,0:T(8,128)(2,1)S(1)} %broadcast_in_dim.116), channel_id=1, replica_groups=mesh['kv'=8,'tp'=4] {'kv'}, dimensions={0} | all-to-all | bytes 524288 | tf_op jit(solution)/shard_map/all_to_all | solution.py:90
  84.8 1.5 %convolution_convert_fusion.7 = bf16[64,256]{1,0:T(8,128)(2,1)S(1)} fusion(bf16[2048,256]{1,0:T(8,128)(2,1)} %param.39, bf16[8,8,2048]{2,1,0:T(8,128)(2,1)S(1)} %all_to_all.22), kind=kOutput, calls=%fused_computation.27 | convolution fusion | flops 67125248 | bytes 1343488 | tf_op jit(solution)/shard_map/dot_general | solution.py:183
  86.4 0.8 collective-permute-start.4
  87.2 1.0 %collective-permute-start.3 = (bf16[64,256]{1,0:T(8,128)(2,1)S(1)}, bf16[64,256]{1,0:T(8,128)(2,1)S(1)}, u32[]{:S(2)}, u32[]{:S(2)}) collective-permute-start(bf16[64,256]{1,0:T(8,128)(2,1)S(1)} %convolution_convert_fusion.7), channel_id=1, source_target_pairs={{0,1},{1,0},{2,3},{3,2},{4,5},{5,4},{6,7},{7,6},{8,9},{9,8},{10,11... | collective-permute-start | bytes 98312 | tf_op jit(solution)/shard_map/ppermute | solution.py:99
  88.3 1.7 %multiply_add_fusion = f32[8,4,128,128]{3,2,1,0:T(8,128)} fusion(f32[8,4,128,128]{3,2,1,0:T(8,128)S(1)} %copy-done.2, f32[8,4,128]{2,1,0:T(4,128)S(1)} %get-tuple-element.7, f32[8,4]{1,0:T(8,128)S(1)} %copy-done.6, f32[8,4,128]{2,1,0:T(4,128)S(1)} %get-tuple-element.9), kind=kLoop, calls=%fused_computation.4 | loop fusion | flops 1572864 | bytes 4227200 | tf_op jit(solution)/shard_map/add | solution.py:67
  90.0 0.6 collective-permute-done.4
  90.5 0.6 fusion.61
  (69 shorter events, 1.5 us)
Async XLA Ops:
  0.6 56.7 %copy-start = (bf16[256,2048]{1,0:T(8,128)(2,1)S(1)}, bf16[256,2048]{1,0:T(8,128)(2,1)}, u32[]{:S(2)}) copy-start(bf16[256,2048]{1,0:T(8,128)(2,1)} %param.38) | copy-start | bytes 3145732
  4.3 9.8 %copy-start.11 = (s32[8]{0:T(128)S(1)}, s32[8]{0:T(128)}, u32[]{:S(2)}) copy-start(s32[8]{0:T(128)} %param.35) | copy-start | bytes 100
  4.3 9.9 %copy-start.7 = (f32[8,4,64]{2,1,0:T(4,128)S(1)}, f32[8,4,64]{2,1,0:T(4,128)}, u32[]{:S(2)}) copy-start(f32[8,4,64]{2,1,0:T(4,128)} %param.33) | copy-start | bytes 24580
  4.3 9.9 %copy-start.8 = (f32[8,4,64]{2,1,0:T(4,128)S(1)}, f32[8,4,64]{2,1,0:T(4,128)}, u32[]{:S(2)}) copy-start(f32[8,4,64]{2,1,0:T(4,128)} %param.34) | copy-start | bytes 24580
  4.3 11.0 %copy-start.12 = (f32[4]{0:T(128)S(1)}, f32[4]{0:T(128)}, u32[]{:S(2)}) copy-start(f32[4]{0:T(128)} %param.28) | copy-start | bytes 52
  4.3 11.5 %copy-start.3 = (bf16[8,4,64,128]{3,2,1,0:T(8,128)(2,1)S(1)}, bf16[8,4,64,128]{3,2,1,0:T(8,128)(2,1)}, u32[]{:S(2)}) copy-start(bf16[8,4,64,128]{3,2,1,0:T(8,128)(2,1)} %param.31) | copy-start | bytes 1572868
  6.7 22.9 %all-to-all-start = ((bf16[8,8,2176]{2,1,0:T(8,128)(2,1)}), bf16[8,8,2176]{2,1,0:T(8,128)(2,1)S(1)}, u32[]{:S(2)}, u32[]{:S(2)}) async-start(bf16[8,8,2176]{2,1,0:T(8,128)(2,1)} %bitcast.1), calls=%async_computation | async-start | bytes 557056 | tf_op jit(solution)/shard_map/all_to_all | solution.py:80
  24.4 1.2 %copy-start.9 = (f32[128]{0:T(128)S(1)}, f32[128]{0:T(128)}, u32[]{:S(2)}) copy-start(f32[128]{0:T(128)} %param.29) | copy-start | bytes 1540
  26.2 5.9 %copy-start.10 = (f32[4]{0:T(128)S(1)}, f32[4]{0:T(128)}, u32[]{:S(2)}) copy-start(f32[4]{0:T(128)} %neg.19) | copy-start | bytes 52
  26.2 6.6 %copy-start.1 = (f32[8,4,128,128]{3,2,1,0:T(8,128)S(1)}, f32[8,4,128,128]{3,2,1,0:T(8,128)}, u32[]{:S(2)}) copy-start(f32[8,4,128,128]{3,2,1,0:T(8,128)} %param.30) | copy-start | bytes 6291460
  32.8 19.7 %copy-start.4 = (bf16[512,256]{1,0:T(8,128)(2,1)S(1)}, bf16[512,256]{1,0:T(8,128)(2,1)}, u32[]{:S(2)}) copy-start(bf16[512,256]{1,0:T(8,128)(2,1)} %param.36) | copy-start | bytes 786436
  32.8 24.0 %copy-start.5 = (bf16[64,256]{1,0:T(8,128)(2,1)S(1)}, bf16[64,256]{1,0:T(8,128)(2,1)}, u32[]{:S(2)}) copy-start(bf16[64,256]{1,0:T(8,128)(2,1)} %param.20) | copy-start | bytes 98308
  52.7 3.7 %collective-permute-start.2 = (bf16[64,256]{1,0:T(8,128)(2,1)S(1)}, bf16[64,256]{1,0:T(8,128)(2,1)S(1)}, u32[]{:S(2)}, u32[]{:S(2)}) collective-permute-start(bf16[64,256]{1,0:T(8,128)(2,1)S(1)} %convolution_convert_fusion.8), channel_id=1, source_target_pairs={{0,3},{1,2},{2,1},{3,0},{4,7},{5,6},{6,5},{7,4},{8,11},{9,10},{10,... | collective-permute-start | bytes 98312 | tf_op jit(solution)/shard_map/ppermute | solution.py:99
  52.8 4.0 %collective-permute-start.1 = (bf16[64,256]{1,0:T(8,128)(2,1)S(1)}, bf16[64,256]{1,0:T(8,128)(2,1)S(1)}, u32[]{:S(2)}, u32[]{:S(2)}) collective-permute-start(bf16[64,256]{1,0:T(8,128)(2,1)S(1)} %convolution_convert_fusion.8), channel_id=1, source_target_pairs={{0,2},{1,3},{2,0},{3,1},{4,6},{5,7},{6,4},{7,5},{8,10},{9,11},{10,... | collective-permute-start | bytes 98312 | tf_op jit(solution)/shard_map/ppermute | solution.py:99
  54.3 2.4 %collective-permute-start = (bf16[64,256]{1,0:T(8,128)(2,1)S(1)}, bf16[64,256]{1,0:T(8,128)(2,1)S(1)}, u32[]{:S(2)}, u32[]{:S(2)}) collective-permute-start(bf16[64,256]{1,0:T(8,128)(2,1)S(1)} %convolution_convert_fusion.8), channel_id=1, source_target_pairs={{0,1},{1,0},{2,3},{3,2},{4,5},{5,4},{6,7},{7,6},{8,9},{9,8},{10,11... | collective-permute-start | bytes 98312 | tf_op jit(solution)/shard_map/ppermute | solution.py:99
  58.3 29.9 %copy-start.2 = (f32[8,4,128,128]{3,2,1,0:T(8,128)S(1)}, f32[8,4,128,128]{3,2,1,0:T(8,128)}, u32[]{:S(2)}) copy-start(f32[8,4,128,128]{3,2,1,0:T(8,128)} %get-tuple-element.28) | copy-start | bytes 6291460
  58.3 29.9 %copy-start.6 = (f32[8,4]{1,0:T(8,128)S(1)}, f32[8,4]{1,0:T(8,128)}, u32[]{:S(2)}) copy-start(f32[8,4]{1,0:T(8,128)} %get-tuple-element.19) | copy-start | bytes 388
  86.3 3.6 %collective-permute-start.5 = (bf16[64,256]{1,0:T(8,128)(2,1)S(1)}, bf16[64,256]{1,0:T(8,128)(2,1)S(1)}, u32[]{:S(2)}, u32[]{:S(2)}) collective-permute-start(bf16[64,256]{1,0:T(8,128)(2,1)S(1)} %convolution_convert_fusion.7), channel_id=1, source_target_pairs={{0,3},{1,2},{2,1},{3,0},{4,7},{5,6},{6,5},{7,4},{8,11},{9,10},{10,... | collective-permute-start | bytes 98312 | tf_op jit(solution)/shard_map/ppermute | solution.py:99
  86.4 4.1 %collective-permute-start.4 = (bf16[64,256]{1,0:T(8,128)(2,1)S(1)}, bf16[64,256]{1,0:T(8,128)(2,1)S(1)}, u32[]{:S(2)}, u32[]{:S(2)}) collective-permute-start(bf16[64,256]{1,0:T(8,128)(2,1)S(1)} %convolution_convert_fusion.7), channel_id=1, source_target_pairs={{0,2},{1,3},{2,0},{3,1},{4,6},{5,7},{6,4},{7,5},{8,10},{9,11},{10,... | collective-permute-start | bytes 98312 | tf_op jit(solution)/shard_map/ppermute | solution.py:99
  87.2 3.3 %collective-permute-start.3 = (bf16[64,256]{1,0:T(8,128)(2,1)S(1)}, bf16[64,256]{1,0:T(8,128)(2,1)S(1)}, u32[]{:S(2)}, u32[]{:S(2)}) collective-permute-start(bf16[64,256]{1,0:T(8,128)(2,1)S(1)} %convolution_convert_fusion.7), channel_id=1, source_target_pairs={{0,1},{1,0},{2,3},{3,2},{4,5},{5,4},{6,7},{7,6},{8,9},{9,8},{10,11... | collective-permute-start | bytes 98312 | tf_op jit(solution)/shard_map/ppermute | solution.py:99

commit v3 on v2

v3 whole, which is shorter than its diff:
```python
import functools

import jax
import jax.numpy as jnp
from jax import lax
from jax.experimental import pallas as pl
from jax.experimental.pallas import tpu as pltpu
from jax.sharding import PartitionSpec as P

MODEL = 2048
EPS = 1e-06
LANES = 128
VMEM = pltpu.VMEM
SMEM = pltpu.SMEM


def in_vmem():
    return pl.BlockSpec(memory_space=VMEM)


def room(megabytes):
    return pltpu.CompilerParams(vmem_limit_bytes=megabytes << 20)


def held(value):
    return pltpu.with_memory_space_constraint(value, VMEM)


def afar(value):
    return pltpu.with_memory_space_constraint(value, pltpu.HBM)


def in_smem():
    return pl.BlockSpec(memory_space=SMEM)


def dot(left, right, contract=((1,), (0,)), precision=None):
    return lax.dot_general(
        left,
        right,
        (contract, ((), ())),
        precision=precision,
        preferred_element_type=jnp.float32,
    )


def halves(value):
    high = value.astype(jnp.bfloat16).astype(jnp.float32)
    return high, value - high


def project_kernel(
    at_ref,
    tokens_ref,
    gain_ref,
    beta_ref,
    decay_ref,
    *rest,
    count,
):
    weight_refs = rest[:count]
    out_ref = rest[count]
    buffers = rest[count + 1 : 2 * count + 1]
    semaphore = rest[2 * count + 1]
    copies = [
        pltpu.make_async_copy(weight_refs[i], buffers[i], semaphore.at[i]) for i in range(count)
    ]
    for copy in copies:
        copy.start()
    parts, rows, _ = out_ref.shape
    tokens = tokens_ref[...].astype(jnp.float32)
    batch = tokens.shape[0]
    normed = (tokens * gain_ref[...]).astype(jnp.bfloat16)
    squares = jnp.sum(tokens * tokens, axis=1, keepdims=True)
    heads = beta_ref.shape[0]
    small = jnp.concatenate(
        [
            beta_ref[...],
            decay_ref[...],
            jnp.zeros((LANES - 2 * heads, beta_ref.shape[1]), jnp.bfloat16),
        ],
        axis=0,
    )
    gating = dot(normed, small, ((1,), (1,)))
    lane = lax.broadcasted_iota(jnp.int32, (batch, LANES), 1)
    high, low = halves(gating)
    square_high, square_low = halves(squares)
    tile = high + pltpu.roll(low, 2 * heads, axis=1)
    tile = jnp.where(lane == 4 * heads, square_high, tile)
    tile = jnp.where(lane == 4 * heads + 1, square_low, tile)
    width = buffers[0].shape[1]
    out_ref[:, :, count * width :] = tile.reshape(parts, rows, LANES).astype(jnp.bfloat16)
    for i in range(count):
        copies[i].wait()
        made = dot(normed, buffers[i][...])
        out_ref[:, :, i * width : (i + 1) * width] = made.reshape(parts, rows, width).astype(
            jnp.bfloat16
        )


def project(kv_index, parts, tokens, norm_gain, weights, beta_weight, decay_weight):
    batch, columns = tokens.shape
    width = weights[0].shape[1]
    count = len(weights)
    betas, decays = beta_weight.T, decay_weight.T
    heads = betas.shape[0]
    where = kv_index
    if columns % LANES:
        betas = lax.dynamic_slice_in_dim(betas, kv_index * columns, columns, 1)
        decays = lax.dynamic_slice_in_dim(decays, kv_index * columns, columns, 1)
        where = jnp.zeros_like(kv_index)
    whole = lambda i, at: (0, 0)
    spec = pltpu.PrefetchScalarGridSpec(
        num_scalar_prefetch=1,
        grid=(1,),
        in_specs=[
            pl.BlockSpec((batch, columns), whole),
            pl.BlockSpec((1, columns), whole),
            pl.BlockSpec((heads, columns), lambda i, at: (0, at[0])),
            pl.BlockSpec((heads, columns), lambda i, at: (0, at[0])),
        ]
        + [pl.BlockSpec(memory_space=pl.ANY)] * count,
        out_specs=in_vmem(),
        scratch_shapes=[pltpu.VMEM((columns, width), jnp.bfloat16)] * count
        + [pltpu.SemaphoreType.DMA((count,))],
    )
    return pl.pallas_call(
        functools.partial(project_kernel, count=count),
        grid_spec=spec,
        out_shape=VMEM((parts, batch // parts, count * width + LANES), jnp.bfloat16),
        compiler_params=room(4),
        name="project",
    )(
        where.reshape(1),
        afar(tokens),
        afar(norm_gain.reshape(1, columns)),
        afar(betas),
        afar(decays),
        *[afar(weight) for weight in weights],
    )


def block_kernel(
    live_ref,
    keys_ref,
    values_ref,
    betas_ref,
    decays_ref,
    far_state_ref,
    out_ref,
    state_ref,
    semaphore,
    *,
    group,
):
    pairs, slots, _ = keys_ref.shape
    fetch = pltpu.make_async_copy(far_state_ref, state_ref, semaphore)
    fetch.start()
    row = lax.broadcasted_iota(jnp.int32, (slots, slots), 0)
    column = lax.broadcasted_iota(jnp.int32, (slots, slots), 1)
    strict = row > column
    pending = lax.broadcasted_iota(jnp.int32, (pairs, slots), 1) < live_ref[...] - 1
    betas = jnp.where(pending, betas_ref[...], 0.0)
    decays = jnp.where(pending, decays_ref[...], 0.0)
    upto = (row <= column).astype(jnp.float32)
    totals = dot(decays, upto, precision=lax.Precision.HIGHEST)
    columns = jnp.concatenate([totals, betas], axis=0).T
    total_columns = columns[:, :pairs]
    beta_columns = columns[:, pairs:]
    ending = total_columns[slots - 1 : slots, :]
    grown = jnp.exp(total_columns)
    faded = jnp.exp(ending - total_columns)
    whole_fade = jnp.exp(totals[:, slots - 1 : slots])
    identity = (row == column).astype(jnp.float32)
    sizes = []
    size = 1
    while size < slots:
        sizes.append(size)
        size *= 2
    joins = [(row // (2 * s) == column // (2 * s)) & (row // s != column // s) for s in sizes]
    for first in range(0, pairs, group):
        members = range(first, min(first + group, pairs))
        lower = {}
        inverse = {}
        for p in members:
            keys = keys_ref[p]
            overlap = dot(keys, keys, ((1,), (1,)))
            spread = total_columns[:, p : p + 1] - totals[p : p + 1, :]
            weight = jnp.exp(jnp.where(strict, spread, 0.0))
            lower[p] = jnp.where(strict, beta_columns[:, p : p + 1] * overlap * weight, 0.0)
            inverse[p] = identity - jnp.where(joins[0], lower[p], 0.0)
        for level in range(1, len(sizes)):
            short = {p: inverse[p].astype(jnp.bfloat16) for p in members}
            middle = {
                p: dot(short[p], jnp.where(joins[level], lower[p], 0.0).astype(jnp.bfloat16))
                for p in members
            }
            for p in members:
                inverse[p] = inverse[p] - dot(middle[p].astype(jnp.bfloat16), short[p])
        if first == 0:
            fetch.wait()
        for p in members:
            keys = keys_ref[p]
            state = state_ref[p]
            recalled = dot(keys, state.astype(jnp.bfloat16))
            wanted = beta_columns[:, p : p + 1] * (
                values_ref[p].astype(jnp.float32) - grown[:, p : p + 1] * recalled
            )
            update = dot(inverse[p].astype(jnp.bfloat16), wanted.astype(jnp.bfloat16))
            update = (faded[:, p : p + 1] * update).astype(jnp.bfloat16)
            out_ref[p] = whole_fade[p : p + 1, :] * state + dot(keys, update, ((0,), (0,)))


def block_state(live_count, keys, values, betas, decays, state, group=16):
    seqs, heads, slots, width = keys.shape
    pairs = seqs * heads
    live = jnp.repeat(live_count, heads).reshape(pairs, 1)
    return pl.pallas_call(
        functools.partial(block_kernel, group=group),
        in_specs=[in_vmem()] * 5 + [pl.BlockSpec(memory_space=pl.ANY)],
        out_specs=in_vmem(),
        scratch_shapes=[VMEM((pairs, width, width), jnp.float32), pltpu.SemaphoreType.DMA],
        out_shape=VMEM((pairs, width, width), jnp.float32),
        cost_estimate=pl.CostEstimate(
            flops=60_000_000, bytes_accessed=5_000_000, transcendentals=0
        ),
        compiler_params=room(24),
        name="block_state",
    )(
        held(live),
        held(keys.reshape(pairs, slots, width)),
        held(values.reshape(pairs, slots, width)),
        held(betas.reshape(pairs, slots)),
        held(decays.reshape(pairs, slots)),
        afar(state.reshape(pairs, width, width)),
    )


def newest_kernel(
    at_ref,
    rate_ref,
    arrived_ref,
    state_ref,
    gain_ref,
    mixed_ref,
    update_ref,
    columns_ref,
    fade_ref,
    recalled_ref,
    answered_ref,
    *,
    heads,
    total_heads,
):
    seqs = arrived_ref.shape[1]
    width = state_ref.shape[1]
    summed = jnp.sum(arrived_ref[...].astype(jnp.float32), axis=0)
    tail = summed[:, 4 * heads * width :]
    lane = lax.broadcasted_iota(jnp.int32, (seqs, LANES), 1)
    is_square = (lane == 4 * total_heads) | (lane == 4 * total_heads + 1)
    squares = jnp.sum(jnp.where(is_square, tail, 0.0), axis=1, keepdims=True)
    scale = lax.rsqrt(squares / MODEL + EPS)
    gating = (tail + pltpu.roll(tail, LANES - 2 * total_heads, axis=1)) * scale
    first = at_ref[0] * heads
    part = lambda i, h: summed[:, (i * heads + h) * width : (i * heads + h + 1) * width] * scale
    queries = [part(0, h) for h in range(heads)]
    keys = []
    for h in range(heads):
        raw = part(1, h)
        keys.append(raw * lax.rsqrt(jnp.sum(raw * raw, axis=1, keepdims=True) + EPS))
    keys = [key.astype(jnp.bfloat16).astype(jnp.float32) for key in keys]
    columns = jnp.concatenate(keys + queries, axis=0).T
    columns_ref[...] = columns
    count = heads * seqs
    for h in range(heads):
        for s in range(seqs):
            state = state_ref[s * heads + h]
            j = h * seqs + s
            key_column = columns[:, j : j + 1]
            query_column = columns[:, count + j : count + j + 1]
            recalled_ref[j : j + 1, :] = jnp.sum(key_column * state, axis=0, keepdims=True)
            answered_ref[j : j + 1, :] = jnp.sum(query_column * state, axis=0, keepdims=True)
    for h in range(heads):
        pick = lambda at: jnp.sum(jnp.where(lane == at, gating, 0.0), axis=1, keepdims=True)
        beta = jax.nn.sigmoid(pick(first + h))
        raw = pick(total_heads + first + h)
        softplus = jnp.maximum(raw, 0.0) + jnp.log1p(jnp.exp(-jnp.abs(raw)))
        fade = jnp.exp(-rate_ref[h] * softplus)
        rows = slice(h * seqs, (h + 1) * seqs)
        value = part(2, h).astype(jnp.bfloat16).astype(jnp.float32)
        update = beta * (value - fade * recalled_ref[rows, :])
        agreement = jnp.sum(keys[h] * queries[h], axis=1, keepdims=True)
        readout = fade * answered_ref[rows, :] + agreement * update
        update_ref[rows, :] = update
        fade_ref[rows, :] = jnp.broadcast_to(fade, (seqs, width))
        gate = part(3, h)
        power = jnp.mean(readout * readout, axis=1, keepdims=True)
        mixed = readout * lax.rsqrt(power + EPS) * gain_ref[...] * (gate * jax.nn.sigmoid(gate))
        shape = (mixed_ref.shape[0], seqs, width)
        mixed_ref[:, :, h * width : (h + 1) * width] = jnp.broadcast_to(mixed[None], shape).astype(
            jnp.bfloat16
        )


def newest(tp_index, decay_rate, arrived, state, head_gain, heads, total_heads):
    parts, seqs, _ = arrived.shape
    width = state.shape[1]
    count = heads * seqs
    return pl.pallas_call(
        functools.partial(newest_kernel, heads=heads, total_heads=total_heads),
        in_specs=[in_smem(), in_smem(), in_vmem(), in_vmem(), in_vmem()],
        out_specs=[in_vmem()] * 4,
        out_shape=[
            VMEM((parts, seqs, heads * width), jnp.bfloat16),
            VMEM((count, width), jnp.float32),
            VMEM((width, 2 * count), jnp.float32),
            VMEM((count, width), jnp.float32),
        ],
        scratch_shapes=[pltpu.VMEM((count, width), jnp.float32)] * 2,
        compiler_params=room(4),
        name="newest",
    )(
        tp_index.reshape(1),
        decay_rate,
        held(arrived),
        held(state),
        held(head_gain.reshape(1, width)),
    )


def refresh_kernel(state_ref, update_ref, columns_ref, fade_ref, out_ref, made_ref, semaphore):
    pairs = state_ref.shape[0]
    seqs = made_ref.shape[0]
    heads = pairs // seqs
    columns = columns_ref[...]
    copies = []
    for s in range(seqs):
        for h in range(heads):
            j = h * seqs + s
            made_ref[s, h] = (
                fade_ref[j : j + 1, :] * state_ref[s * heads + h]
                + columns[:, j : j + 1] * update_ref[j : j + 1, :]
            )
        copies.append(pltpu.make_async_copy(made_ref.at[s], out_ref.at[s], semaphore.at[s]))
        copies[-1].start()
    for copy in copies:
        copy.wait()


def refresh(state, update, columns, fade, seqs):
    pairs, width, _ = state.shape
    shape = (seqs, pairs // seqs, width, width)
    return pl.pallas_call(
        refresh_kernel,
        in_specs=[in_vmem()] * 4,
        out_specs=pl.BlockSpec(memory_space=pl.ANY),
        out_shape=jax.ShapeDtypeStruct(shape, jnp.float32),
        scratch_shapes=[pltpu.VMEM(shape, jnp.float32), pltpu.SemaphoreType.DMA((seqs,))],
        cost_estimate=pl.CostEstimate(
            flops=10_000_000, bytes_accessed=4_000_000, transcendentals=0
        ),
        compiler_params=room(8),
        name="refresh",
    )(held(state), held(update), held(columns), held(fade))


def widen_kernel(residual_ref, scaled_ref, weight_ref, out_ref):
    parts, rows, _ = out_ref.shape
    value = residual_ref[...].astype(jnp.float32)
    batch = value.shape[0]
    high, low = halves(jnp.sum(value * value, axis=1, keepdims=True))
    lane = lax.broadcasted_iota(jnp.int32, (batch, LANES), 1)
    tile = jnp.where(lane == 0, high, jnp.where(lane == 1, low, 0.0))
    units = weight_ref.shape[1]
    out_ref[:, :, units:] = tile.reshape(parts, rows, LANES).astype(jnp.bfloat16)
    made = dot(scaled_ref[...], weight_ref[...])
    out_ref[:, :, :units] = made.reshape(parts, rows, units).astype(jnp.bfloat16)


def widen(parts, residual, scaled, up_weight):
    batch = residual.shape[0]
    units = up_weight.shape[1]
    return pl.pallas_call(
        widen_kernel,
        in_specs=[in_vmem()] * 3,
        out_specs=in_vmem(),
        out_shape=VMEM((parts, batch // parts, units + LANES), jnp.bfloat16),
        compiler_params=room(6),
        name="widen",
    )(held(residual), held(scaled), held(up_weight))


def activate_kernel(arrived_ref, out_ref):
    units = out_ref.shape[2]
    summed = jnp.sum(arrived_ref[...].astype(jnp.float32), axis=0)
    tail = summed[:, units:]
    lane = lax.broadcasted_iota(jnp.int32, tail.shape, 1)
    squares = jnp.sum(jnp.where(lane < 2, tail, 0.0), axis=1, keepdims=True)
    scale = lax.rsqrt(squares / MODEL + EPS)
    hidden = jnp.square(jnp.maximum(summed[:, :units] * scale, 0.0))
    out_ref[...] = jnp.broadcast_to(hidden[None], out_ref.shape).astype(jnp.bfloat16)


def activate(arrived):
    parts, seqs, wide = arrived.shape
    return pl.pallas_call(
        activate_kernel,
        in_specs=[in_vmem()],
        out_specs=in_vmem(),
        out_shape=VMEM((parts, seqs, wide - LANES), jnp.bfloat16),
        compiler_params=room(4),
        name="activate",
    )(held(arrived))


def narrow_kernel(rows_ref, weight_ref, out_ref):
    rows = rows_ref[...]
    rows = rows.reshape(rows.shape[0] * rows.shape[1], rows.shape[2])
    out_ref[...] = dot(rows, weight_ref[...]).astype(jnp.bfloat16)


def narrow(rows, weight, name):
    return pl.pallas_call(
        narrow_kernel,
        in_specs=[in_vmem()] * 2,
        out_specs=in_vmem(),
        out_shape=VMEM((rows.shape[0] * rows.shape[1], weight.shape[1]), jnp.bfloat16),
        compiler_params=room(4),
        name=name,
    )(held(rows), held(weight))


def swap_over_kv(payload):
    return lax.all_to_all(payload, "kv", 0, 0, tiled=True)


def over_tp(mine):
    count = lax.axis_size("tp")
    parts = [mine]
    for step in range(1, count):
        swaps = [(place, place ^ step) for place in range(count)]
        parts.append(lax.ppermute(mine, "tp", swaps))
    return parts


def body(
    tokens,
    norm_gain,
    query_weight,
    key_weight,
    value_weight,
    gate_weight,
    beta_weight,
    decay_weight,
    decay_rate,
    head_gain,
    carried_state,
    block_keys,
    block_values,
    block_beta,
    block_decay,
    live_count,
    out_weight,
    mlp_gain,
    up_weight,
    down_weight,
):
    kv_index = lax.axis_index("kv")
    tp_index = lax.axis_index("tp")
    parts = lax.axis_size("kv")
    seqs, heads = carried_state.shape[:2]
    payload = project(
        kv_index,
        parts,
        tokens,
        norm_gain,
        [query_weight, key_weight, value_weight, gate_weight],
        beta_weight,
        decay_weight,
    )
    arrived = swap_over_kv(payload)
    state = block_state(
        live_count, block_keys, block_values, block_beta, block_decay, carried_state
    )
    copies, update, columns, fade = newest(
        tp_index, decay_rate, arrived, state, head_gain, heads, beta_weight.shape[1]
    )
    new_state = refresh(state, update, columns, fade, seqs)
    attended = over_tp(narrow(swap_over_kv(copies), out_weight, "attend"))
    residual = tokens.astype(jnp.float32) + sum(part.astype(jnp.float32) for part in attended)
    residual = residual.astype(jnp.bfloat16)
    gain = lax.dynamic_slice_in_dim(mlp_gain, kv_index * tokens.shape[1], tokens.shape[1], 0)
    scaled = (residual.astype(jnp.float32) * gain).astype(jnp.bfloat16)
    hidden = activate(swap_over_kv(widen(parts, residual, scaled, up_weight)))
    shares = over_tp(narrow(swap_over_kv(hidden), down_weight, "narrow"))
    mixed = residual.astype(jnp.float32) + sum(share.astype(jnp.float32) for share in shares)
    return (mixed.astype(jnp.bfloat16), new_state)


def solution(mesh):
    placed = (
        P(None, "kv"),
        P("kv"),
        P("kv", "tp"),
        P("kv", "tp"),
        P("kv", "tp"),
        P("kv", "tp"),
        P(),
        P(),
        P("tp"),
        P(),
        P("kv", "tp", None, None),
        P("kv", "tp", None, None),
        P("kv", "tp", None, None),
        P("kv", "tp", None),
        P("kv", "tp", None),
        P("kv"),
        P("tp", "kv"),
        P(),
        P("kv", "tp"),
        P("tp", "kv"),
    )
    return jax.shard_map(
        body,
        mesh=mesh,
        in_specs=placed,
        out_specs=(P(None, "kv"), P("kv", "tp", None, None)),
        check_vma=False,
    )
```

time: 92 us -> 72.8 us (0.79)
  matrix products: 23.5 us -> 0 us
  Pallas kernels: 0 us -> 16.5 us
  other arithmetic: 8.14 us -> 1.43 us
  local copies, waits for them, and re-layouts: 7.81 us -> 1.69 us
  waiting for transfers between devices: 2.01 us -> 3.27 us
    dot_general x14 -> x0, matrix products: 23.5 us -> none  [the longest x8 18.2 us: product(): jnp.einsum(spec, left.astype(jnp.bfloat16), right.astype(jnp.bfloat16), p...]
    pallas_call x0 -> x8, Pallas kernels: none -> 16.5 us  [the longest x1 8.65 us: block_state(): pl.pallas_call(functools.partial(block_kernel, group=group), in_specs=[in...]
    reduce_sum x7 -> x0, other arithmetic: 2.8 us -> none  [the longest x1 0.91 us: body(): jnp.mean(readout * readout, axis=2, keepdims=True) + EPS]
    concatenate x2 -> x0, local copies, waits for them, and re-layouts: 2.01 us -> none  [scatter_sum(): jnp.concatenate([wide.astype(jnp.bfloat16), high, low, padding], axis=1)]
    add x2 -> x0, other arithmetic: 1.78 us -> none  [the longest x1 1.7 us: newest_step(): new_state = fade[..., None] * state + key * update[:, :, None, :]]
    dynamic_slice x3 -> x1, local copies, waits for them, and re-layouts: 2.38 us -> 0.85 us  [body(): lax.dynamic_slice_in_dim(mlp_gain, kv_index * tokens.shape[1], tokens.sha...]
    ppermute x6, waiting for transfers between devices: 2.01 us -> 3.27 us  [over_tp(): parts.append(lax.ppermute(mine, 'tp', swaps))]
    unnamed x28 -> x18, local copies, waits for them, and re-layouts: 1.29 us -> 0.05 us
  transfers between devices with their start and end apart: 7 -> 7, of which waited for: 3 -> 4; matrix products, arithmetic and copies ran while one was open for 20% -> 2% of each run, Pallas kernels for 0% -> 14%
where the time goes in v3:
time: 72.8 us; the launch traced here: 72.3 us
  blocking collectives  37.4 us (51%)
  Pallas kernels  16.5 us (23%)
  starting transfers between devices  11.1 us (15%)
  waiting for transfers between devices  3.27 us (4%)
  local copies, waits for them, and re-layouts  1.69 us (2%)
  other arithmetic  1.43 us (2%)
  between operations  0.84 us (1%)
    all_to_all x3, blocking collectives, swap_over_kv(): return lax.all_to_all(payload, 'kv', 0, 0, tiled=True)  37.4 us
    pallas_call x1, Pallas kernels, block_state(): pl.pallas_call(functools.partial(block_kernel, group=group), in_specs=[in...  8.65 us
    all_to_all x1, starting transfers between devices, swap_over_kv(): return lax.all_to_all(payload, 'kv', 0, 0, tiled=True)  7.29 us
    ppermute x6, starting transfers between devices, over_tp(): parts.append(lax.ppermute(mine, 'tp', swaps))  3.84 us
    ppermute x6, waiting for transfers between devices, over_tp(): parts.append(lax.ppermute(mine, 'tp', swaps))  3.27 us
    pallas_call x1, Pallas kernels, project(): pl.pallas_call(functools.partial(project_kernel, count=count), grid_spec=...  3.23 us
    pallas_call x1, Pallas kernels, newest(): pl.pallas_call(functools.partial(newest_kernel, heads=heads, total_heads=...  2.22 us
    pallas_call x1, Pallas kernels, refresh(): pl.pallas_call(refresh_kernel, in_specs=[in_vmem()] * 4, out_specs=pl.Blo...  1.51 us
  transfers between devices with their start and end apart: 7, of which 4 were waited for; matrix products, arithmetic and copies ran while one was open for 2% of the time, Pallas kernels for 14%

profile of v3, /device:TPU:0, one launch (start us, length us, event | category | flops | bytes accessed | tf_op | source)
XLA Modules:
  0.0 72.3 jit_solution(16187782931574845789)
XLA Ops:
  0.6 0.0 copy-start.2
  0.6 0.0 copy-start.3
  0.7 0.0 copy-start.5
  0.7 0.0 copy-start.6
  0.7 3.2 %project.1 = bf16[8,8,2176]{2,1,0:T(8,128)(2,1)} custom-call(s32[1]{0:T(128)} %bitcast.1.at_ref, bf16[64,256]{1,0:T(8,128)(2,1)} %tokens_ref.1, f32[1,256]{1,0:T(1,128)} %bitcast.19, bf16[16,2048]{1,0:T(8,128)(2,1)} %bitcast.17, bf16[16,2048]{1,0:T(8,128)(2,1)} %bitcast.18, bf16[256,512]{1,0:T(8,128)(2,1)} %rest_0_.1, bf16[256,512]{1,0:T(8,128)(2,1)} %rest_1_.1, ...), custom_call_target="tpu_custom_call" | custom-call | tf_op jit(solution)/shard_map/project/pallas_call | solution.py:127
  3.9 7.3 %all-to-all-start = ((bf16[8,8,2176]{2,1,0:T(8,128)(2,1)}), bf16[8,8,2176]{2,1,0:T(8,128)(2,1)S(1)}, u32[]{:S(2)}, u32[]{:S(2)}) async-start(bf16[8,8,2176]{2,1,0:T(8,128)(2,1)} %project.1), calls=%async_computation | async-start | bytes 557056 | tf_op jit(solution)/shard_map/all_to_all | solution.py:434
  11.2 0.7 %broadcast_in_dim.4 = s32[8,4]{1,0:T(8,128)S(1)} broadcast(s32[8]{0:T(128)} %param.35), dimensions={0} | broadcast | bytes 160 | tf_op jit(solution)/shard_map/broadcast_in_dim | solution.py:217
  11.9 0.1 reshape_reshape.4.live_ref
  12.0 0.0 copy-done.2
  12.0 0.0 copy-done.3
  12.0 0.0 copy-done.5
  12.0 0.0 copy-done.6
  12.0 0.0 copy-start.7
  12.0 0.0 copy-start.8
  12.1 8.7 %block_state.1.state_ref = f32[32,128,128]{2,1,0:T(8,128)S(1)} custom-call(s32[32,1]{1,0:T(8,128)S(1)} %reshape_reshape.4.live_ref, bf16[32,64,128]{2,1,0:T(8,128)(2,1)S(1)} %bitcast.11, bf16[32,64,128]{2,1,0:T(8,128)(2,1)S(1)} %bitcast.12, f32[32,64]{1,0:T(8,128)S(1)} %bitcast.13, f32[32,64]{1,0:T(8,128)S(1)} %bitcast.14, f32[32,128,128]{2,1,0:T(8,128)} %bitcast.16), custom_call_target="tpu_custom_call" | custom-call | flops 60000000 | bytes 5000000 | tf_op jit(solution)/shard_map/block_state/pallas_call | solution.py:218
  20.7 0.0 copy-start
  20.7 0.0 all-to-all-done.arrived_ref
  20.7 0.0 copy-start.4
  20.7 0.0 copy-done.7
  20.8 0.0 copy-done.8
  20.8 2.2 %newest.1 = (bf16[8,8,512]{2,1,0:T(8,128)(2,1)S(1)}, f32[32,128]{1,0:T(8,128)S(1)}, f32[128,64]{1,0:T(8,128)S(1)}, f32[32,128]{1,0:T(8,128)S(1)}) custom-call(s32[1]{0:T(128)} %bitcast.at_ref, f32[4]{0:T(128)S(1)} %copy-done.7, bf16[8,8,2176]{2,1,0:T(8,128)(2,1)S(1)} %all-to-all-done.arrived_ref, f32[32,128,128]{2,1,0:T(8,128)S(1)} %block_state.1.state_ref, ...), custom_call_target="tpu_custom_call" | custom-call | tf_op jit(solution)/shard_map/newest/pallas_call | solution.py:309
  23.0 12.7 %all_to_all.20.rows_ref = bf16[8,8,512]{2,1,0:T(8,128)(2,1)S(1)} all-to-all(bf16[8,8,512]{2,1,0:T(8,128)(2,1)S(1)} %get-tuple-element.6), channel_id=1, replica_groups=mesh['kv'=8,'tp'=4] {'kv'}, dimensions={0} | all-to-all | bytes 131072 | tf_op jit(solution)/shard_map/all_to_all | solution.py:434
  35.7 0.0 copy-done.4
  35.7 0.2 attend.1
  35.9 0.1 collective-permute-start
  35.9 1.6 %collective-permute-start.1 = (bf16[64,256]{1,0:T(8,128)(2,1)S(1)}, bf16[64,256]{1,0:T(8,128)(2,1)S(1)}, u32[]{:S(2)}, u32[]{:S(2)}) collective-permute-start(bf16[64,256]{1,0:T(8,128)(2,1)S(1)} %attend.1), channel_id=1, source_target_pairs={{0,2},{1,3},{2,0},{3,1},{4,6},{5,7},{6,4},{7,5},{8,10},{9,11},{10,... | collective-permute-start | bytes 98312 | tf_op jit(solution)/shard_map/ppermute | solution.py:442
  37.5 0.3 collective-permute-start.2
  37.8 0.0 copy-start.1
  37.8 0.8 %dynamic_slice.3 = f32[256]{0:T(256)S(1)} dynamic-slice(f32[2048]{0:T(1024)} %param.37, s32[]{:T(128)S(6)} %select_n.3), dynamic_slice_sizes={256} | dynamic-slice | bytes 2052 | tf_op jit(solution)/shard_map/dynamic_slice | solution.py:492
  38.6 0.0 collective-permute-done
  38.6 1.3 %collective-permute-done.1 = bf16[64,256]{1,0:T(8,128)(2,1)S(1)} collective-permute-done((bf16[64,256]{1,0:T(8,128)(2,1)S(1)}, bf16[64,256]{1,0:T(8,128)(2,1)S(1)}, u32[]{:S(2)}, u32[]{:S(2)}) %collective-permute-start.1) | collective-permute-done | bytes 32800 | tf_op jit(solution)/shard_map/ppermute | solution.py:442
  39.9 1.0 %collective-permute-done.2 = bf16[64,256]{1,0:T(8,128)(2,1)S(1)} collective-permute-done((bf16[64,256]{1,0:T(8,128)(2,1)S(1)}, bf16[64,256]{1,0:T(8,128)(2,1)S(1)}, u32[]{:S(2)}, u32[]{:S(2)}) %collective-permute-start.2) | collective-permute-done | bytes 32800 | tf_op jit(solution)/shard_map/ppermute | solution.py:442
  40.9 0.8 %fusion = (bf16[64,256]{1,0:T(8,128)(2,1)S(1)}, bf16[64,256]{1,0:T(8,128)(2,1)S(1)}) fusion(f32[256]{0:T(256)S(1)} %dynamic_slice.3, bf16[64,256]{1,0:T(8,128)(2,1)S(1)} %collective-permute-done.2, bf16[64,256]{1,0:T(8,128)(2,1)S(1)} %collective-permute-done.1, bf16[64,256]{1,0:T(8,128)(2,1)S(1)} %collective-permute-done, bf16[64,256]{1,0:T(8,128)(2,1)S(1)} %attend.1, ...), kind=kLoop, calls=%fused_computation.2 | loop fusion | flops 212992 | bytes 230400 | tf_op jit(solution)/shard_map/convert_element_type | solution.py:493
  41.7 0.0 copy-done
  41.7 0.3 widen.1
  42.0 13.1 %all_to_all.21.arrived_ref = bf16[8,8,2176]{2,1,0:T(8,128)(2,1)S(1)} all-to-all(bf16[8,8,2176]{2,1,0:T(8,128)(2,1)S(1)} %widen.1), channel_id=1, replica_groups=mesh['kv'=8,'tp'=4] {'kv'}, dimensions={0} | all-to-all | bytes 557056 | tf_op jit(solution)/shard_map/all_to_all | solution.py:434
  55.1 0.1 activate.1
  55.2 11.7 %all_to_all.22.rows_ref = bf16[8,8,2048]{2,1,0:T(8,128)(2,1)S(1)} all-to-all(bf16[8,8,2048]{2,1,0:T(8,128)(2,1)S(1)} %activate.1), channel_id=1, replica_groups=mesh['kv'=8,'tp'=4] {'kv'}, dimensions={0} | all-to-all | bytes 524288 | tf_op jit(solution)/shard_map/all_to_all | solution.py:434
  66.9 0.0 copy-done.1
  66.9 0.3 narrow.1
  67.2 0.1 collective-permute-start.3
  67.2 0.9 %collective-permute-start.4 = (bf16[64,256]{1,0:T(8,128)(2,1)S(1)}, bf16[64,256]{1,0:T(8,128)(2,1)S(1)}, u32[]{:S(2)}, u32[]{:S(2)}) collective-permute-start(bf16[64,256]{1,0:T(8,128)(2,1)S(1)} %narrow.1), channel_id=1, source_target_pairs={{0,2},{1,3},{2,0},{3,1},{4,6},{5,7},{6,4},{7,5},{8,10},{9,11},{10,... | collective-permute-start | bytes 98312 | tf_op jit(solution)/shard_map/ppermute | solution.py:442
  68.2 0.9 %collective-permute-start.5 = (bf16[64,256]{1,0:T(8,128)(2,1)S(1)}, bf16[64,256]{1,0:T(8,128)(2,1)S(1)}, u32[]{:S(2)}, u32[]{:S(2)}) collective-permute-start(bf16[64,256]{1,0:T(8,128)(2,1)S(1)} %narrow.1), channel_id=1, source_target_pairs={{0,3},{1,2},{2,1},{3,0},{4,7},{5,6},{6,5},{7,4},{8,11},{9,10},{10,... | collective-permute-start | bytes 98312 | tf_op jit(solution)/shard_map/ppermute | solution.py:442
  69.1 1.5 %refresh.1 = f32[8,4,128,128]{3,2,1,0:T(8,128)} custom-call(f32[32,128,128]{2,1,0:T(8,128)S(1)} %block_state.1.state_ref, f32[32,128]{1,0:T(8,128)S(1)} %get-tuple-element.7.update_ref, f32[128,64]{1,0:T(8,128)S(1)} %get-tuple-element.8.columns_ref, f32[32,128]{1,0:T(8,128)S(1)} %get-tuple-element.9.fade_ref), custom_call_target="tpu_custom_call" | custom-call | flops 10000000 | bytes 4000000 | tf_op jit(solution)/shard_map/refresh/pallas_call | solution.py:353
  70.6 0.0 collective-permute-done.3
  70.6 0.7 collective-permute-done.4
  71.3 0.4 collective-permute-done.5
  71.7 0.6 fusion.1
Async XLA Ops:
  0.6 11.4 %copy-start.2 = (bf16[8,4,64,128]{3,2,1,0:T(8,128)(2,1)S(1)}, bf16[8,4,64,128]{3,2,1,0:T(8,128)(2,1)}, u32[]{:S(2)}) copy-start(bf16[8,4,64,128]{3,2,1,0:T(8,128)(2,1)} %param.31) | copy-start | bytes 1572868
  0.6 11.4 %copy-start.3 = (bf16[8,4,64,128]{3,2,1,0:T(8,128)(2,1)S(1)}, bf16[8,4,64,128]{3,2,1,0:T(8,128)(2,1)}, u32[]{:S(2)}) copy-start(bf16[8,4,64,128]{3,2,1,0:T(8,128)(2,1)} %param.32) | copy-start | bytes 1572868
  0.7 11.4 %copy-start.5 = (f32[8,4,64]{2,1,0:T(4,128)S(1)}, f32[8,4,64]{2,1,0:T(4,128)}, u32[]{:S(2)}) copy-start(f32[8,4,64]{2,1,0:T(4,128)} %param.33) | copy-start | bytes 24580
  0.7 11.4 %copy-start.6 = (f32[8,4,64]{2,1,0:T(4,128)S(1)}, f32[8,4,64]{2,1,0:T(4,128)}, u32[]{:S(2)}) copy-start(f32[8,4,64]{2,1,0:T(4,128)} %param.34) | copy-start | bytes 24580
  3.9 16.8 %all-to-all-start = ((bf16[8,8,2176]{2,1,0:T(8,128)(2,1)}), bf16[8,8,2176]{2,1,0:T(8,128)(2,1)S(1)}, u32[]{:S(2)}, u32[]{:S(2)}) async-start(bf16[8,8,2176]{2,1,0:T(8,128)(2,1)} %project.1), calls=%async_computation | async-start | bytes 557056 | tf_op jit(solution)/shard_map/all_to_all | solution.py:434
  12.0 8.7 %copy-start.7 = (f32[4]{0:T(128)S(1)}, f32[4]{0:T(128)}, u32[]{:S(2)}) copy-start(f32[4]{0:T(128)} %rate_ref.1) | copy-start | bytes 52
  12.0 8.7 %copy-start.8 = (f32[128]{0:T(128)S(1)}, f32[128]{0:T(128)}, u32[]{:S(2)}) copy-start(f32[128]{0:T(128)} %param.29) | copy-start | bytes 1540
  20.7 21.0 %copy-start = (bf16[256,2048]{1,0:T(8,128)(2,1)S(1)}, bf16[256,2048]{1,0:T(8,128)(2,1)}, u32[]{:S(2)}) copy-start(bf16[256,2048]{1,0:T(8,128)(2,1)} %weight_ref.4) | copy-start | bytes 3145732
  20.7 15.0 %copy-start.4 = (bf16[512,256]{1,0:T(8,128)(2,1)S(1)}, bf16[512,256]{1,0:T(8,128)(2,1)}, u32[]{:S(2)}) copy-start(bf16[512,256]{1,0:T(8,128)(2,1)} %weight_ref.3) | copy-start | bytes 786436
  35.9 2.8 %collective-permute-start = (bf16[64,256]{1,0:T(8,128)(2,1)S(1)}, bf16[64,256]{1,0:T(8,128)(2,1)S(1)}, u32[]{:S(2)}, u32[]{:S(2)}) collective-permute-start(bf16[64,256]{1,0:T(8,128)(2,1)S(1)} %attend.1), channel_id=1, source_target_pairs={{0,1},{1,0},{2,3},{3,2},{4,5},{5,4},{6,7},{7,6},{8,9},{9,8},{10,11... | collective-permute-start | bytes 98312 | tf_op jit(solution)/shard_map/ppermute | solution.py:442
  35.9 4.0 %collective-permute-start.1 = (bf16[64,256]{1,0:T(8,128)(2,1)S(1)}, bf16[64,256]{1,0:T(8,128)(2,1)S(1)}, u32[]{:S(2)}, u32[]{:S(2)}) collective-permute-start(bf16[64,256]{1,0:T(8,128)(2,1)S(1)} %attend.1), channel_id=1, source_target_pairs={{0,2},{1,3},{2,0},{3,1},{4,6},{5,7},{6,4},{7,5},{8,10},{9,11},{10,... | collective-permute-start | bytes 98312 | tf_op jit(solution)/shard_map/ppermute | solution.py:442
  37.5 3.4 %collective-permute-start.2 = (bf16[64,256]{1,0:T(8,128)(2,1)S(1)}, bf16[64,256]{1,0:T(8,128)(2,1)S(1)}, u32[]{:S(2)}, u32[]{:S(2)}) collective-permute-start(bf16[64,256]{1,0:T(8,128)(2,1)S(1)} %attend.1), channel_id=1, source_target_pairs={{0,3},{1,2},{2,1},{3,0},{4,7},{5,6},{6,5},{7,4},{8,11},{9,10},{10,... | collective-permute-start | bytes 98312 | tf_op jit(solution)/shard_map/ppermute | solution.py:442
  37.8 29.1 %copy-start.1 = (bf16[2048,256]{1,0:T(8,128)(2,1)S(1)}, bf16[2048,256]{1,0:T(8,128)(2,1)}, u32[]{:S(2)}) copy-start(bf16[2048,256]{1,0:T(8,128)(2,1)} %weight_ref.5) | copy-start | bytes 3145732
  67.2 3.5 %collective-permute-start.3 = (bf16[64,256]{1,0:T(8,128)(2,1)S(1)}, bf16[64,256]{1,0:T(8,128)(2,1)S(1)}, u32[]{:S(2)}, u32[]{:S(2)}) collective-permute-start(bf16[64,256]{1,0:T(8,128)(2,1)S(1)} %narrow.1), channel_id=1, source_target_pairs={{0,1},{1,0},{2,3},{3,2},{4,5},{5,4},{6,7},{7,6},{8,9},{9,8},{10,11... | collective-permute-start | bytes 98312 | tf_op jit(solution)/shard_map/ppermute | solution.py:442
  67.2 4.0 %collective-permute-start.4 = (bf16[64,256]{1,0:T(8,128)(2,1)S(1)}, bf16[64,256]{1,0:T(8,128)(2,1)S(1)}, u32[]{:S(2)}, u32[]{:S(2)}) collective-permute-start(bf16[64,256]{1,0:T(8,128)(2,1)S(1)} %narrow.1), channel_id=1, source_target_pairs={{0,2},{1,3},{2,0},{3,1},{4,6},{5,7},{6,4},{7,5},{8,10},{9,11},{10,... | collective-permute-start | bytes 98312 | tf_op jit(solution)/shard_map/ppermute | solution.py:442
  68.2 3.5 %collective-permute-start.5 = (bf16[64,256]{1,0:T(8,128)(2,1)S(1)}, bf16[64,256]{1,0:T(8,128)(2,1)S(1)}, u32[]{:S(2)}, u32[]{:S(2)}) collective-permute-start(bf16[64,256]{1,0:T(8,128)(2,1)S(1)} %narrow.1), channel_id=1, source_target_pairs={{0,3},{1,2},{2,1},{3,0},{4,7},{5,6},{6,5},{7,4},{8,11},{9,10},{10,... | collective-permute-start | bytes 98312 | tf_op jit(solution)/shard_map/ppermute | solution.py:442

commit v4 on v3

v4 whole, which is shorter than its diff:
```python
import functools

import jax
import jax.numpy as jnp
from jax import lax
from jax.experimental import pallas as pl
from jax.experimental.pallas import tpu as pltpu
from jax.sharding import PartitionSpec as P

MODEL = 2048
EPS = 1e-06
LANES = 128
VMEM = pltpu.VMEM
SMEM = pltpu.SMEM


def in_vmem():
    return pl.BlockSpec(memory_space=VMEM)


def room(megabytes):
    return pltpu.CompilerParams(vmem_limit_bytes=megabytes << 20)


def held(value):
    return pltpu.with_memory_space_constraint(value, VMEM)


def afar(value):
    return pltpu.with_memory_space_constraint(value, pltpu.HBM)


def in_smem():
    return pl.BlockSpec(memory_space=SMEM)


def dot(left, right, contract=((1,), (0,)), precision=None):
    return lax.dot_general(
        left,
        right,
        (contract, ((), ())),
        precision=precision,
        preferred_element_type=jnp.float32,
    )


def halves(value):
    high = value.astype(jnp.bfloat16).astype(jnp.float32)
    return high, value - high


def project_kernel(
    tokens_ref,
    gain_ref,
    beta_ref,
    decay_ref,
    mlp_gain_ref,
    *rest,
    count,
    extras,
    sliced,
):
    far, rest = rest[:count], rest[count:]
    far_extras, rest = rest[:extras], rest[extras:]
    (out_ref, near_tokens_ref, near_mlp_gain_ref), rest = rest[:3], rest[3:]
    near_extras, rest = rest[:extras], rest[extras:]
    (gain_row, beta_rows, decay_rows), rest = rest[:3], rest[3:]
    near, semaphore = rest[:count], rest[count]
    columns = tokens_ref.shape[1]
    part = pl.ds(0 if sliced else lax.axis_index("kv") * columns, columns)
    pairs = [
        (tokens_ref, near_tokens_ref),
        (gain_ref, gain_row),
        (beta_ref.at[:, part], beta_rows),
        (decay_ref.at[:, part], decay_rows),
    ]
    pairs += list(zip(far, near)) + list(zip(far_extras, near_extras))
    pairs.append((mlp_gain_ref.at[:, part], near_mlp_gain_ref))
    copies = [
        pltpu.make_async_copy(source, target, semaphore.at[i])
        for i, (source, target) in enumerate(pairs)
    ]
    for copy in copies:
        copy.start()
    for copy in copies[:4]:
        copy.wait()
    parts, rows, _ = out_ref.shape
    tokens = near_tokens_ref[...].astype(jnp.float32)
    batch = tokens.shape[0]
    normed = (tokens * gain_row[...]).astype(jnp.bfloat16)
    squares = jnp.sum(tokens * tokens, axis=1, keepdims=True)
    heads = beta_rows.shape[0]
    small = jnp.concatenate(
        [
            beta_rows[...],
            decay_rows[...],
            jnp.zeros((LANES - 2 * heads, columns), jnp.bfloat16),
        ],
        axis=0,
    )
    gating = dot(normed, small, ((1,), (1,)))
    lane = lax.broadcasted_iota(jnp.int32, (batch, LANES), 1)
    high, low = halves(gating)
    square_high, square_low = halves(squares)
    tile = high + pltpu.roll(low, 2 * heads, axis=1)
    tile = jnp.where(lane == 4 * heads, square_high, tile)
    tile = jnp.where(lane == 4 * heads + 1, square_low, tile)
    width = near[0].shape[1]
    out_ref[:, :, count * width :] = tile.reshape(parts, rows, LANES).astype(jnp.bfloat16)
    for i in range(count):
        copies[4 + i].wait()
        made = dot(normed, near[i][...])
        out_ref[:, :, i * width : (i + 1) * width] = made.reshape(parts, rows, width).astype(
            jnp.bfloat16
        )
    for copy in copies[4 + count :]:
        copy.wait()


def project(parts, tokens, norm_gain, weights, beta_weight, decay_weight, mlp_gain, extras):
    batch, columns = tokens.shape
    width = weights[0].shape[1]
    count = len(weights)
    by_feature = [beta_weight.T, decay_weight.T, mlp_gain.reshape(1, -1)]
    heads = beta_weight.shape[1]
    sliced = bool(columns % LANES)
    if sliced:
        start = lax.axis_index("kv") * columns
        by_feature = [lax.dynamic_slice_in_dim(w, start, columns, 1) for w in by_feature]
    return pl.pallas_call(
        functools.partial(project_kernel, count=count, extras=len(extras), sliced=sliced),
        in_specs=[pl.BlockSpec(memory_space=pl.ANY)] * (5 + count + len(extras)),
        out_specs=[in_vmem()] * (3 + len(extras)),
        out_shape=[
            VMEM((parts, batch // parts, count * width + LANES), jnp.bfloat16),
            VMEM((batch, columns), jnp.bfloat16),
            VMEM((1, columns), jnp.float32),
        ]
        + [VMEM(extra.shape, extra.dtype) for extra in extras],
        scratch_shapes=[
            VMEM((1, columns), jnp.float32),
            VMEM((heads, columns), jnp.bfloat16),
            VMEM((heads, columns), jnp.bfloat16),
        ]
        + [VMEM((columns, width), jnp.bfloat16)] * count
        + [pltpu.SemaphoreType.DMA((5 + count + len(extras),))],
        compiler_params=room(4),
        name="project",
    )(
        afar(tokens),
        afar(norm_gain.reshape(1, columns)),
        *[afar(value) for value in by_feature + list(weights) + list(extras)],
    )


def block_kernel(
    live_ref,
    keys_ref,
    values_ref,
    betas_ref,
    decays_ref,
    far_state_ref,
    out_ref,
    state_ref,
    semaphore,
    *,
    heads,
    pack,
):
    pairs, slots, width = keys_ref.shape
    fetch = pltpu.make_async_copy(far_state_ref, state_ref, semaphore)
    fetch.start()
    owner_row = lax.broadcasted_iota(jnp.int32, (pairs, slots), 0) // heads
    limit = jnp.zeros((pairs, slots), jnp.int32)
    for s in range(pairs // heads):
        limit = jnp.where(owner_row == s, live_ref[:, s : s + 1] - 1, limit)
    pending = lax.broadcasted_iota(jnp.int32, (pairs, slots), 1) < limit
    betas = jnp.where(pending, betas_ref[...], 0.0)
    decays = jnp.where(pending, decays_ref[...], 0.0)
    upto = (
        lax.broadcasted_iota(jnp.int32, (slots, slots), 0)
        <= lax.broadcasted_iota(jnp.int32, (slots, slots), 1)
    ).astype(jnp.float32)
    totals = dot(decays, upto, precision=lax.Precision.HIGHEST)
    columns = jnp.concatenate([totals, betas], axis=0).T
    total_columns = columns[:, :pairs]
    beta_columns = columns[:, pairs:]
    ending = total_columns[slots - 1 : slots, :]
    grown = jnp.exp(total_columns)
    faded = jnp.exp(ending - total_columns)
    whole_fade = jnp.exp(totals[:, slots - 1 : slots])
    across = pack * slots
    row = lax.broadcasted_iota(jnp.int32, (slots, across), 0)
    lane = lax.broadcasted_iota(jnp.int32, (slots, across), 1)
    column = lane % slots
    owner = lane // slots
    strict = row > column
    identity = (row == column).astype(jnp.float32)
    sizes = []
    size = 1
    while size < slots:
        sizes.append(size)
        size *= 2
    joins = [(row // (2 * s) == column // (2 * s)) & (row // s != column // s) for s in sizes]

    def choose(pieces):
        chosen = pieces[-1]
        for m in range(pack - 2, -1, -1):
            chosen = jnp.where(owner == m, pieces[m], chosen)
        return chosen

    def spread_out(value):
        return jnp.concatenate(
            [jnp.where(owner == m, value, 0.0).astype(jnp.bfloat16) for m in range(pack)], axis=0
        )

    packs = range(pairs // pack)
    lower = []
    inverse = []
    for g in packs:
        members = range(g * pack, (g + 1) * pack)
        stacked = keys_ref[g * pack : (g + 1) * pack].reshape(across, width)
        overlaps = dot(stacked, stacked, ((1,), (1,)))
        overlap = choose([overlaps[m * slots : (m + 1) * slots] for m in range(pack)])
        along = jnp.concatenate([totals[p : p + 1, :] for p in members], axis=1)
        down = choose([total_columns[:, p : p + 1] for p in members])
        beta = choose([beta_columns[:, p : p + 1] for p in members])
        weight = jnp.exp(jnp.where(strict, down - along, 0.0))
        lower.append(jnp.where(strict, beta * overlap * weight, 0.0))
        inverse.append(identity - jnp.where(joins[0], lower[g], 0.0))
    for level in range(1, len(sizes)):
        middle = [
            dot(
                inverse[g].astype(jnp.bfloat16),
                spread_out(jnp.where(joins[level], lower[g], 0.0)),
            )
            for g in packs
        ]
        for g in packs:
            inverse[g] = inverse[g] - dot(middle[g].astype(jnp.bfloat16), spread_out(inverse[g]))
    fetch.wait()
    for g in packs:
        members = range(g * pack, (g + 1) * pack)
        wanted = []
        for p in members:
            recalled = dot(keys_ref[p], state_ref[p].astype(jnp.bfloat16))
            wanted.append(
                beta_columns[:, p : p + 1]
                * (values_ref[p].astype(jnp.float32) - grown[:, p : p + 1] * recalled)
            )
        wanted = jnp.concatenate(wanted, axis=0).astype(jnp.bfloat16)
        updates = dot(spread_out(inverse[g]), wanted)
        for m, p in enumerate(members):
            update = faded[:, p : p + 1] * updates[m * slots : (m + 1) * slots]
            made = dot(keys_ref[p], update.astype(jnp.bfloat16), ((0,), (0,)))
            out_ref[p] = whole_fade[p : p + 1, :] * state_ref[p] + made


def block_state(live_count, keys, values, betas, decays, state, pack=4):
    seqs, heads, slots, width = keys.shape
    pairs = seqs * heads
    return pl.pallas_call(
        functools.partial(block_kernel, heads=heads, pack=pack),
        in_specs=[in_vmem()] * 5 + [pl.BlockSpec(memory_space=pl.ANY)],
        out_specs=in_vmem(),
        scratch_shapes=[VMEM((pairs, width, width), jnp.float32), pltpu.SemaphoreType.DMA],
        out_shape=VMEM((pairs, width, width), jnp.float32),
        cost_estimate=pl.CostEstimate(
            flops=60_000_000, bytes_accessed=5_000_000, transcendentals=0
        ),
        compiler_params=room(24),
        name="block_state",
    )(
        held(live_count),
        held(keys.reshape(pairs, slots, width)),
        held(values.reshape(pairs, slots, width)),
        held(betas),
        held(decays),
        afar(state.reshape(pairs, width, width)),
    )


def newest_kernel(
    rate_ref,
    arrived_ref,
    state_ref,
    gain_ref,
    mixed_ref,
    update_ref,
    columns_ref,
    fade_ref,
    recalled_ref,
    answered_ref,
    *,
    heads,
    total_heads,
):
    seqs = arrived_ref.shape[1]
    width = state_ref.shape[1]
    summed = jnp.sum(arrived_ref[...].astype(jnp.float32), axis=0)
    raw = lambda i, h: summed[:, (i * heads + h) * width : (i * heads + h + 1) * width]
    key_and_query = [raw(1, h) for h in range(heads)] + [raw(0, h) for h in range(heads)]
    columns = jnp.concatenate(key_and_query, axis=0).T
    columns_ref[...] = columns
    lines = [
        jnp.concatenate([raw(1, h), raw(0, h)], axis=0).astype(jnp.bfloat16) for h in range(heads)
    ]
    for h in range(heads):
        for s in range(seqs):
            found = dot(lines[h], state_ref[s * heads + h].astype(jnp.bfloat16))
            j = h * seqs + s
            recalled_ref[j : j + 1, :] = found[s : s + 1, :]
            answered_ref[j : j + 1, :] = found[seqs + s : seqs + s + 1, :]
    tail = summed[:, 4 * heads * width :]
    lane = lax.broadcasted_iota(jnp.int32, (seqs, LANES), 1)
    is_square = (lane == 4 * total_heads) | (lane == 4 * total_heads + 1)
    squares = jnp.sum(jnp.where(is_square, tail, 0.0), axis=1, keepdims=True)
    scale = lax.rsqrt(squares / MODEL + EPS)
    gating = (tail + pltpu.roll(tail, LANES - 2 * total_heads, axis=1)) * scale
    first = lax.axis_index("tp") * heads
    pick = lambda at: jnp.sum(jnp.where(lane == at, gating, 0.0), axis=1, keepdims=True)
    for h in range(heads):
        beta = jax.nn.sigmoid(pick(first + h))
        before = pick(total_heads + first + h)
        softplus = jnp.maximum(before, 0.0) + jnp.log1p(jnp.exp(-jnp.abs(before)))
        fade = jnp.exp(-rate_ref[:, h : h + 1] * softplus)
        rows = slice(h * seqs, (h + 1) * seqs)
        key = raw(1, h) * scale
        key_scale = lax.rsqrt(jnp.sum(key * key, axis=1, keepdims=True) + EPS)
        query = raw(0, h) * scale
        agreement = jnp.sum(key * query, axis=1, keepdims=True) * key_scale
        value = raw(2, h) * scale
        gate = raw(3, h) * scale
        update = beta * (value - fade * (key_scale * scale) * recalled_ref[rows, :])
        readout = fade * scale * answered_ref[rows, :] + agreement * update
        power = jnp.mean(readout * readout, axis=1, keepdims=True)
        mixed = readout * lax.rsqrt(power + EPS) * gain_ref[...] * (gate * jax.nn.sigmoid(gate))
        shape = (mixed_ref.shape[0], seqs, width)
        mixed_ref[:, :, h * width : (h + 1) * width] = jnp.broadcast_to(mixed[None], shape).astype(
            jnp.bfloat16
        )
        update_ref[rows, :] = update * (key_scale * scale)
        fade_ref[rows, :] = jnp.broadcast_to(fade, (seqs, width))


def newest(decay_rate, arrived, state, head_gain, heads, total_heads):
    parts, seqs, _ = arrived.shape
    width = state.shape[1]
    count = heads * seqs
    return pl.pallas_call(
        functools.partial(newest_kernel, heads=heads, total_heads=total_heads),
        in_specs=[in_vmem()] * 4,
        out_specs=[in_vmem()] * 4,
        out_shape=[
            VMEM((parts, seqs, heads * width), jnp.bfloat16),
            VMEM((count, width), jnp.float32),
            VMEM((width, 2 * count), jnp.float32),
            VMEM((count, width), jnp.float32),
        ],
        scratch_shapes=[pltpu.VMEM((count, width), jnp.float32)] * 2,
        compiler_params=room(4),
        name="newest",
    )(
        held(decay_rate),
        held(arrived),
        held(state),
        held(head_gain),
    )


def refresh_kernel(state_ref, update_ref, columns_ref, fade_ref, out_ref, made_ref, semaphore):
    pairs = state_ref.shape[0]
    seqs = made_ref.shape[0]
    heads = pairs // seqs
    columns = columns_ref[...]
    copies = []
    for s in range(seqs):
        for h in range(heads):
            j = h * seqs + s
            made_ref[s, h] = (
                fade_ref[j : j + 1, :] * state_ref[s * heads + h]
                + columns[:, j : j + 1] * update_ref[j : j + 1, :]
            )
        copies.append(pltpu.make_async_copy(made_ref.at[s], out_ref.at[s], semaphore.at[s]))
        copies[-1].start()
    for copy in copies:
        copy.wait()


def refresh(state, update, columns, fade, seqs):
    pairs, width, _ = state.shape
    shape = (seqs, pairs // seqs, width, width)
    return pl.pallas_call(
        refresh_kernel,
        in_specs=[in_vmem()] * 4,
        out_specs=pl.BlockSpec(memory_space=pl.ANY),
        out_shape=jax.ShapeDtypeStruct(shape, jnp.float32),
        scratch_shapes=[pltpu.VMEM(shape, jnp.float32), pltpu.SemaphoreType.DMA((seqs,))],
        cost_estimate=pl.CostEstimate(
            flops=10_000_000, bytes_accessed=4_000_000, transcendentals=0
        ),
        compiler_params=room(8),
        name="refresh",
    )(held(state), held(update), held(columns), held(fade))


def widen_kernel(residual_ref, scaled_ref, weight_ref, out_ref):
    parts, rows, _ = out_ref.shape
    value = residual_ref[...].astype(jnp.float32)
    batch = value.shape[0]
    high, low = halves(jnp.sum(value * value, axis=1, keepdims=True))
    lane = lax.broadcasted_iota(jnp.int32, (batch, LANES), 1)
    tile = jnp.where(lane == 0, high, jnp.where(lane == 1, low, 0.0))
    units = weight_ref.shape[1]
    out_ref[:, :, units:] = tile.reshape(parts, rows, LANES).astype(jnp.bfloat16)
    made = dot(scaled_ref[...], weight_ref[...])
    out_ref[:, :, :units] = made.reshape(parts, rows, units).astype(jnp.bfloat16)


def widen(parts, residual, scaled, up_weight):
    batch = residual.shape[0]
    units = up_weight.shape[1]
    return pl.pallas_call(
        widen_kernel,
        in_specs=[in_vmem()] * 3,
        out_specs=in_vmem(),
        out_shape=VMEM((parts, batch // parts, units + LANES), jnp.bfloat16),
        compiler_params=room(6),
        name="widen",
    )(held(residual), held(scaled), held(up_weight))


def activate_kernel(arrived_ref, out_ref):
    units = out_ref.shape[2]
    summed = jnp.sum(arrived_ref[...].astype(jnp.float32), axis=0)
    tail = summed[:, units:]
    lane = lax.broadcasted_iota(jnp.int32, tail.shape, 1)
    squares = jnp.sum(jnp.where(lane < 2, tail, 0.0), axis=1, keepdims=True)
    scale = lax.rsqrt(squares / MODEL + EPS)
    hidden = jnp.square(jnp.maximum(summed[:, :units] * scale, 0.0))
    out_ref[...] = jnp.broadcast_to(hidden[None], out_ref.shape).astype(jnp.bfloat16)


def activate(arrived):
    parts, seqs, wide = arrived.shape
    return pl.pallas_call(
        activate_kernel,
        in_specs=[in_vmem()],
        out_specs=in_vmem(),
        out_shape=VMEM((parts, seqs, wide - LANES), jnp.bfloat16),
        compiler_params=room(4),
        name="activate",
    )(held(arrived))


def narrow_kernel(rows_ref, weight_ref, out_ref):
    rows = rows_ref[...]
    rows = rows.reshape(rows.shape[0] * rows.shape[1], rows.shape[2])
    out_ref[...] = dot(rows, weight_ref[...]).astype(jnp.bfloat16)


def narrow(rows, weight, name):
    return pl.pallas_call(
        narrow_kernel,
        in_specs=[in_vmem()] * 2,
        out_specs=in_vmem(),
        out_shape=VMEM((rows.shape[0] * rows.shape[1], weight.shape[1]), jnp.bfloat16),
        compiler_params=room(4),
        name=name,
    )(held(rows), held(weight))


def swap_over_kv(payload):
    return lax.all_to_all(payload, "kv", 0, 0, tiled=True)


def over_tp(mine):
    count = lax.axis_size("tp")
    parts = [mine]
    for step in range(1, count):
        swaps = [(place, place ^ step) for place in range(count)]
        parts.append(lax.ppermute(mine, "tp", swaps))
    return parts


def body(
    tokens,
    norm_gain,
    query_weight,
    key_weight,
    value_weight,
    gate_weight,
    beta_weight,
    decay_weight,
    decay_rate,
    head_gain,
    carried_state,
    block_keys,
    block_values,
    block_beta,
    block_decay,
    live_count,
    out_weight,
    mlp_gain,
    up_weight,
    down_weight,
):
    parts = lax.axis_size("kv")
    seqs, heads, slots, width = block_keys.shape
    pairs = seqs * heads
    payload, near_tokens, gain, live, betas, decays, rates, head_gains = project(
        parts,
        tokens,
        norm_gain,
        [query_weight, key_weight, value_weight, gate_weight],
        beta_weight,
        decay_weight,
        mlp_gain,
        [
            live_count.reshape(1, seqs),
            block_beta.reshape(pairs, slots),
            block_decay.reshape(pairs, slots),
            decay_rate.reshape(1, heads),
            head_gain.reshape(1, width),
        ],
    )
    arrived = swap_over_kv(payload)
    state = block_state(live, block_keys, block_values, betas, decays, carried_state)
    copies, update, columns, fade = newest(
        rates, arrived, state, head_gains, heads, beta_weight.shape[1]
    )
    new_state = refresh(state, update, columns, fade, seqs)
    attended = over_tp(narrow(swap_over_kv(copies), out_weight, "attend"))
    residual = near_tokens.astype(jnp.float32) + sum(part.astype(jnp.float32) for part in attended)
    residual = residual.astype(jnp.bfloat16)
    scaled = (residual.astype(jnp.float32) * gain).astype(jnp.bfloat16)
    hidden = activate(swap_over_kv(widen(parts, residual, scaled, up_weight)))
    shares = over_tp(narrow(swap_over_kv(hidden), down_weight, "narrow"))
    mixed = residual.astype(jnp.float32) + sum(share.astype(jnp.float32) for share in shares)
    return (mixed.astype(jnp.bfloat16), new_state)


def solution(mesh):
    placed = (
        P(None, "kv"),
        P("kv"),
        P("kv", "tp"),
        P("kv", "tp"),
        P("kv", "tp"),
        P("kv", "tp"),
        P(),
        P(),
        P("tp"),
        P(),
        P("kv", "tp", None, None),
        P("kv", "tp", None, None),
        P("kv", "tp", None, None),
        P("kv", "tp", None),
        P("kv", "tp", None),
        P("kv"),
        P("tp", "kv"),
        P(),
        P("kv", "tp"),
        P("tp", "kv"),
    )
    return jax.shard_map(
        body,
        mesh=mesh,
        in_specs=placed,
        out_specs=(P(None, "kv"), P("kv", "tp", None, None)),
        check_vma=False,
    )
```

time: 72.8 us -> 66 us (0.907)
  Pallas kernels: 16.5 us -> 12.1 us
  waiting for transfers between devices: 3.27 us -> 5.65 us
  blocking collectives: 37.4 us -> 35.4 us
  local copies, waits for them, and re-layouts: 1.69 us -> 0.02 us
  other arithmetic: 1.43 us -> 0.67 us
    pallas_call x2, Pallas kernels: 11.9 us -> 9.13 us  [the longest x1 6.51 us: block_state(): pl.pallas_call(functools.partial(block_kernel, heads=heads, pack=pack), i...]
    all_to_all x1, waiting for transfers between devices: 0.01 us -> 2.71 us  [swap_over_kv(): return lax.all_to_all(payload, 'kv', 0, 0, tiled=True)]
    all_to_all x3, blocking collectives: 37.4 us -> 35.4 us  [swap_over_kv(): return lax.all_to_all(payload, 'kv', 0, 0, tiled=True)]
    pallas_call x1, Pallas kernels: 2.22 us -> 0.52 us  [newest(): pl.pallas_call(functools.partial(newest_kernel, heads=heads, total_heads=...]
    dynamic_slice x1 -> x0, local copies, waits for them, and re-layouts: 0.85 us -> none  [body(): lax.dynamic_slice_in_dim(mlp_gain, kv_index * tokens.shape[1], tokens.sha...]
    convert_element_type x1, other arithmetic: 0.79 us -> 0.03 us  [body(): scaled = (residual.astype(jnp.float32) * gain).astype(jnp.bfloat16)]
  transfers between devices with their start and end apart: 7 -> 7, of which waited for: 4 -> 4; matrix products, arithmetic and copies ran while one was open for 2% -> 0% of each run, Pallas kernels for 14% -> 12%
where the time goes in v4:
time: 66 us; the launch traced here: 65.7 us
  blocking collectives  35.4 us (54%)
  Pallas kernels  12.1 us (18%)
  starting transfers between devices  11.1 us (17%)
  waiting for transfers between devices  5.65 us (9%)
  between operations  0.76 us (1%)
  other arithmetic  0.67 us (1%)
    all_to_all x3, blocking collectives, swap_over_kv(): return lax.all_to_all(payload, 'kv', 0, 0, tiled=True)  35.4 us
    all_to_all x1, starting transfers between devices, swap_over_kv(): return lax.all_to_all(payload, 'kv', 0, 0, tiled=True)  7.3 us
    pallas_call x1, Pallas kernels, block_state(): pl.pallas_call(functools.partial(block_kernel, heads=heads, pack=pack), i...  6.51 us
    ppermute x6, starting transfers between devices, over_tp(): parts.append(lax.ppermute(mine, 'tp', swaps))  3.84 us
    ppermute x6, waiting for transfers between devices, over_tp(): parts.append(lax.ppermute(mine, 'tp', swaps))  2.94 us
    all_to_all x1, waiting for transfers between devices, swap_over_kv(): return lax.all_to_all(payload, 'kv', 0, 0, tiled=True)  2.71 us
    pallas_call x1, Pallas kernels, project(): pl.pallas_call(functools.partial(project_kernel, count=count, extras=len(...  2.62 us
    pallas_call x1, Pallas kernels, refresh(): pl.pallas_call(refresh_kernel, in_specs=[in_vmem()] * 4, out_specs=pl.Blo...  1.51 us
  transfers between devices with their start and end apart: 7, of which 4 were waited for; matrix products, arithmetic and copies ran while one was open for 0% of the time, Pallas kernels for 12%

profile of v4, /device:TPU:0, one launch (start us, length us, event | category | flops | bytes accessed | tf_op | source)
XLA Modules:
  0.0 65.7 jit_solution(6177807786789713213)
XLA Ops:
  0.6 0.0 copy-start.2
  0.6 0.0 copy-start.3
  0.7 2.6 %project.1 = (bf16[8,8,2176]{2,1,0:T(8,128)(2,1)}, bf16[64,256]{1,0:T(8,128)(2,1)S(1)}, f32[1,256]{1,0:T(1,128)S(1)}, s32[1,8]{1,0:T(1,128)S(1)}, f32[32,64]{1,0...) custom-call(bf16[64,256]{1,0:T(8,128)(2,1)} %tokens_ref.1, f32[1,256]{1,0:T(1,128)} %bitcast.22, ...), custom_call_target="tpu_custom_call" | custom-call | tf_op jit(solution)/shard_map/project/pallas_call | solution.py:130
  3.3 7.3 %all-to-all-start = ((bf16[8,8,2176]{2,1,0:T(8,128)(2,1)}), bf16[8,8,2176]{2,1,0:T(8,128)(2,1)S(1)}, u32[]{:S(2)}, u32[]{:S(2)}) async-start(bf16[8,8,2176]{2,1,0:T(8,128)(2,1)} %get-tuple-element.16), calls=%async_computation | async-start | bytes 557056 | tf_op jit(solution)/shard_map/all_to_all | solution.py:474
  10.6 0.0 copy-done.2
  10.6 0.0 copy-done.3
  10.6 6.5 %block_state.1.state_ref = f32[32,128,128]{2,1,0:T(8,128)S(1)} custom-call(s32[1,8]{1,0:T(1,128)S(1)} %get-tuple-element.17.live_ref, bf16[32,64,128]{2,1,0:T(8,128)(2,1)S(1)} %bitcast.13, bf16[32,64,128]{2,1,0:T(8,128)(2,1)S(1)} %bitcast.14, f32[32,64]{1,0:T(8,128)S(1)} %get-tuple-element.18.betas_ref, f32[32,64]{1,0:T(8,128)S(1)} %get-tuple-element.19.decays_ref, ...), custom_call_target="tpu_custom_call" | custom-call | flops 60000000 | bytes 5000000 | tf_op jit(solution)/shard_map/block_state/pallas_call | solution.py:262
  17.1 0.0 copy-start
  17.1 2.7 %all-to-all-done.arrived_ref = bf16[8,8,2176]{2,1,0:T(8,128)(2,1)S(1)} async-done(((bf16[8,8,2176]{2,1,0:T(8,128)(2,1)}), bf16[8,8,2176]{2,1,0:T(8,128)(2,1)S(1)}, u32[]{:S(2)}, u32[]{:S(2)}) %all-to-all-start) | async-done | bytes 278560 | tf_op jit(solution)/shard_map/all_to_all | solution.py:474
  19.8 0.0 copy-start.4
  19.8 0.5 newest.1
  20.4 0.0 copy-start.1
  20.4 10.4 %all_to_all.20.rows_ref = bf16[8,8,512]{2,1,0:T(8,128)(2,1)S(1)} all-to-all(bf16[8,8,512]{2,1,0:T(8,128)(2,1)S(1)} %get-tuple-element.21), channel_id=1, replica_groups=mesh['kv'=8,'tp'=4] {'kv'}, dimensions={0} | all-to-all | bytes 131072 | tf_op jit(solution)/shard_map/all_to_all | solution.py:474
  30.8 0.0 copy-done.4
  30.8 0.2 attend.1
  31.0 0.1 collective-permute-start.2
  31.1 1.6 %collective-permute-start.1 = (bf16[64,256]{1,0:T(8,128)(2,1)S(1)}, bf16[64,256]{1,0:T(8,128)(2,1)S(1)}, u32[]{:S(2)}, u32[]{:S(2)}) collective-permute-start(bf16[64,256]{1,0:T(8,128)(2,1)S(1)} %attend.1), channel_id=1, source_target_pairs={{0,2},{1,3},{2,0},{3,1},{4,6},{5,7},{6,4},{7,5},{8,10},{9,11},{10,... | collective-permute-start | bytes 98312 | tf_op jit(solution)/shard_map/ppermute | solution.py:482
  32.6 0.3 collective-permute-start
  32.9 1.8 %collective-permute-done.2 = bf16[64,256]{1,0:T(8,128)(2,1)S(1)} collective-permute-done((bf16[64,256]{1,0:T(8,128)(2,1)S(1)}, bf16[64,256]{1,0:T(8,128)(2,1)S(1)}, u32[]{:S(2)}, u32[]{:S(2)}) %collective-permute-start.2) | collective-permute-done | bytes 32800 | tf_op jit(solution)/shard_map/ppermute | solution.py:482
  34.7 0.4 collective-permute-done.1
  35.1 0.0 collective-permute-done
  35.1 0.0 copy-done
  35.1 0.3 widen.1
  35.4 13.3 %all_to_all.21.arrived_ref = bf16[8,8,2176]{2,1,0:T(8,128)(2,1)S(1)} all-to-all(bf16[8,8,2176]{2,1,0:T(8,128)(2,1)S(1)} %widen.1), channel_id=1, replica_groups=mesh['kv'=8,'tp'=4] {'kv'}, dimensions={0} | all-to-all | bytes 557056 | tf_op jit(solution)/shard_map/all_to_all | solution.py:474
  48.7 0.1 activate.1
  48.8 11.7 %all_to_all.22.rows_ref = bf16[8,8,2048]{2,1,0:T(8,128)(2,1)S(1)} all-to-all(bf16[8,8,2048]{2,1,0:T(8,128)(2,1)S(1)} %activate.1), channel_id=1, replica_groups=mesh['kv'=8,'tp'=4] {'kv'}, dimensions={0} | all-to-all | bytes 524288 | tf_op jit(solution)/shard_map/all_to_all | solution.py:474
  60.5 0.0 copy-done.1
  60.5 0.3 narrow.1
  60.8 0.1 collective-permute-start.5
  60.9 0.8 %collective-permute-start.4 = (bf16[64,256]{1,0:T(8,128)(2,1)S(1)}, bf16[64,256]{1,0:T(8,128)(2,1)S(1)}, u32[]{:S(2)}, u32[]{:S(2)}) collective-permute-start(bf16[64,256]{1,0:T(8,128)(2,1)S(1)} %narrow.1), channel_id=1, source_target_pairs={{0,2},{1,3},{2,0},{3,1},{4,6},{5,7},{6,4},{7,5},{8,10},{9,11},{10,... | collective-permute-start | bytes 98312 | tf_op jit(solution)/shard_map/ppermute | solution.py:482
  61.7 1.0 %collective-permute-start.3 = (bf16[64,256]{1,0:T(8,128)(2,1)S(1)}, bf16[64,256]{1,0:T(8,128)(2,1)S(1)}, u32[]{:S(2)}, u32[]{:S(2)}) collective-permute-start(bf16[64,256]{1,0:T(8,128)(2,1)S(1)} %narrow.1), channel_id=1, source_target_pairs={{0,1},{1,0},{2,3},{3,2},{4,5},{5,4},{6,7},{7,6},{8,9},{9,8},{10,11... | collective-permute-start | bytes 98312 | tf_op jit(solution)/shard_map/ppermute | solution.py:482
  62.7 1.5 %refresh.1 = f32[8,4,128,128]{3,2,1,0:T(8,128)} custom-call(f32[32,128,128]{2,1,0:T(8,128)S(1)} %block_state.1.state_ref, f32[32,128]{1,0:T(8,128)S(1)} %get-tuple-element.23.update_ref, f32[128,64]{1,0:T(8,128)S(1)} %get-tuple-element.24.columns_ref, f32[32,128]{1,0:T(8,128)S(1)} %get-tuple-element.25.fade_ref), custom_call_target="tpu_custom_call" | custom-call | flops 10000000 | bytes 4000000 | tf_op jit(solution)/shard_map/refresh/pallas_call | solution.py:393
  64.3 0.0 collective-permute-done.5
  64.3 0.8 %collective-permute-done.4 = bf16[64,256]{1,0:T(8,128)(2,1)S(1)} collective-permute-done((bf16[64,256]{1,0:T(8,128)(2,1)S(1)}, bf16[64,256]{1,0:T(8,128)(2,1)S(1)}, u32[]{:S(2)}, u32[]{:S(2)}) %collective-permute-start.4) | collective-permute-done | bytes 32800 | tf_op jit(solution)/shard_map/ppermute | solution.py:482
  65.0 0.0 collective-permute-done.3
  65.0 0.6 fusion.1
  (1 shorter events, 0.0 us)
Async XLA Ops:
  0.6 10.0 %copy-start.2 = (bf16[8,4,64,128]{3,2,1,0:T(8,128)(2,1)S(1)}, bf16[8,4,64,128]{3,2,1,0:T(8,128)(2,1)}, u32[]{:S(2)}) copy-start(bf16[8,4,64,128]{3,2,1,0:T(8,128)(2,1)} %param.31) | copy-start | bytes 1572868
  0.6 10.0 %copy-start.3 = (bf16[8,4,64,128]{3,2,1,0:T(8,128)(2,1)S(1)}, bf16[8,4,64,128]{3,2,1,0:T(8,128)(2,1)}, u32[]{:S(2)}) copy-start(bf16[8,4,64,128]{3,2,1,0:T(8,128)(2,1)} %param.32) | copy-start | bytes 1572868
  3.3 16.6 %all-to-all-start = ((bf16[8,8,2176]{2,1,0:T(8,128)(2,1)}), bf16[8,8,2176]{2,1,0:T(8,128)(2,1)S(1)}, u32[]{:S(2)}, u32[]{:S(2)}) async-start(bf16[8,8,2176]{2,1,0:T(8,128)(2,1)} %get-tuple-element.16), calls=%async_computation | async-start | bytes 557056 | tf_op jit(solution)/shard_map/all_to_all | solution.py:474
  17.1 18.0 %copy-start = (bf16[256,2048]{1,0:T(8,128)(2,1)S(1)}, bf16[256,2048]{1,0:T(8,128)(2,1)}, u32[]{:S(2)}) copy-start(bf16[256,2048]{1,0:T(8,128)(2,1)} %weight_ref.4) | copy-start | bytes 3145732
  19.8 11.0 %copy-start.4 = (bf16[512,256]{1,0:T(8,128)(2,1)S(1)}, bf16[512,256]{1,0:T(8,128)(2,1)}, u32[]{:S(2)}) copy-start(bf16[512,256]{1,0:T(8,128)(2,1)} %weight_ref.3) | copy-start | bytes 786436
  20.4 40.1 %copy-start.1 = (bf16[2048,256]{1,0:T(8,128)(2,1)S(1)}, bf16[2048,256]{1,0:T(8,128)(2,1)}, u32[]{:S(2)}) copy-start(bf16[2048,256]{1,0:T(8,128)(2,1)} %weight_ref.5) | copy-start | bytes 3145732
  31.0 3.7 %collective-permute-start.2 = (bf16[64,256]{1,0:T(8,128)(2,1)S(1)}, bf16[64,256]{1,0:T(8,128)(2,1)S(1)}, u32[]{:S(2)}, u32[]{:S(2)}) collective-permute-start(bf16[64,256]{1,0:T(8,128)(2,1)S(1)} %attend.1), channel_id=1, source_target_pairs={{0,3},{1,2},{2,1},{3,0},{4,7},{5,6},{6,5},{7,4},{8,11},{9,10},{10,... | collective-permute-start | bytes 98312 | tf_op jit(solution)/shard_map/ppermute | solution.py:482
  31.1 4.0 %collective-permute-start.1 = (bf16[64,256]{1,0:T(8,128)(2,1)S(1)}, bf16[64,256]{1,0:T(8,128)(2,1)S(1)}, u32[]{:S(2)}, u32[]{:S(2)}) collective-permute-start(bf16[64,256]{1,0:T(8,128)(2,1)S(1)} %attend.1), channel_id=1, source_target_pairs={{0,2},{1,3},{2,0},{3,1},{4,6},{5,7},{6,4},{7,5},{8,10},{9,11},{10,... | collective-permute-start | bytes 98312 | tf_op jit(solution)/shard_map/ppermute | solution.py:482
  32.6 2.4 %collective-permute-start = (bf16[64,256]{1,0:T(8,128)(2,1)S(1)}, bf16[64,256]{1,0:T(8,128)(2,1)S(1)}, u32[]{:S(2)}, u32[]{:S(2)}) collective-permute-start(bf16[64,256]{1,0:T(8,128)(2,1)S(1)} %attend.1), channel_id=1, source_target_pairs={{0,1},{1,0},{2,3},{3,2},{4,5},{5,4},{6,7},{7,6},{8,9},{9,8},{10,11... | collective-permute-start | bytes 98312 | tf_op jit(solution)/shard_map/ppermute | solution.py:482
  60.8 3.5 %collective-permute-start.5 = (bf16[64,256]{1,0:T(8,128)(2,1)S(1)}, bf16[64,256]{1,0:T(8,128)(2,1)S(1)}, u32[]{:S(2)}, u32[]{:S(2)}) collective-permute-start(bf16[64,256]{1,0:T(8,128)(2,1)S(1)} %narrow.1), channel_id=1, source_target_pairs={{0,3},{1,2},{2,1},{3,0},{4,7},{5,6},{6,5},{7,4},{8,11},{9,10},{10,... | collective-permute-start | bytes 98312 | tf_op jit(solution)/shard_map/ppermute | solution.py:482
  60.9 4.1 %collective-permute-start.4 = (bf16[64,256]{1,0:T(8,128)(2,1)S(1)}, bf16[64,256]{1,0:T(8,128)(2,1)S(1)}, u32[]{:S(2)}, u32[]{:S(2)}) collective-permute-start(bf16[64,256]{1,0:T(8,128)(2,1)S(1)} %narrow.1), channel_id=1, source_target_pairs={{0,2},{1,3},{2,0},{3,1},{4,6},{5,7},{6,4},{7,5},{8,10},{9,11},{10,... | collective-permute-start | bytes 98312 | tf_op jit(solution)/shard_map/ppermute | solution.py:482
  61.7 3.3 %collective-permute-start.3 = (bf16[64,256]{1,0:T(8,128)(2,1)S(1)}, bf16[64,256]{1,0:T(8,128)(2,1)S(1)}, u32[]{:S(2)}, u32[]{:S(2)}) collective-permute-start(bf16[64,256]{1,0:T(8,128)(2,1)S(1)} %narrow.1), channel_id=1, source_target_pairs={{0,1},{1,0},{2,3},{3,2},{4,5},{5,4},{6,7},{7,6},{8,9},{9,8},{10,11... | collective-permute-start | bytes 98312 | tf_op jit(solution)/shard_map/ppermute | solution.py:482

commit v5 on v4

--- a/solution.py
+++ b/solution.py
@@ -47,6 +47,17 @@
 def halves(value):
     high = value.astype(jnp.bfloat16).astype(jnp.float32)
     return high, value - high
+
+
+def exchange_order(parts):
+    stride = 3 if parts % 3 else 1
+    return [(parts // 2 + 1 + stride * i) % parts for i in range(parts)]
+
+
+def deal(out_ref, lanes, value):
+    parts, rows, _ = out_ref.shape
+    for slot, place in enumerate(exchange_order(parts)):
+        out_ref[slot, :, lanes] = value[place * rows : (place + 1) * rows].astype(jnp.bfloat16)
 
 
 def project_kernel(
@@ -84,7 +95,6 @@
         copy.start()
     for copy in copies[:4]:
         copy.wait()
-    parts, rows, _ = out_ref.shape
     tokens = near_tokens_ref[...].astype(jnp.float32)
     batch = tokens.shape[0]
     normed = (tokens * gain_row[...]).astype(jnp.bfloat16)
@@ -106,13 +116,10 @@
     tile = jnp.where(lane == 4 * heads, square_high, tile)
     tile = jnp.where(lane == 4 * heads + 1, square_low, tile)
     width = near[0].shape[1]
-    out_ref[:, :, count * width :] = tile.reshape(parts, rows, LANES).astype(jnp.bfloat16)
+    deal(out_ref, slice(count * width, count * width + LANES), tile)
     for i in range(count):
         copies[4 + i].wait()
-        made = dot(normed, near[i][...])
-        out_ref[:, :, i * width : (i + 1) * width] = made.reshape(parts, rows, width).astype(
-            jnp.bfloat16
-        )
+        deal(out_ref, slice(i * width, (i + 1) * width), dot(normed, near[i][...]))
     for copy in copies[4 + count :]:
         copy.wait()
 
@@ -405,16 +412,14 @@
 
 
 def widen_kernel(residual_ref, scaled_ref, weight_ref, out_ref):
-    parts, rows, _ = out_ref.shape
     value = residual_ref[...].astype(jnp.float32)
     batch = value.shape[0]
     high, low = halves(jnp.sum(value * value, axis=1, keepdims=True))
     lane = lax.broadcasted_iota(jnp.int32, (batch, LANES), 1)
     tile = jnp.where(lane == 0, high, jnp.where(lane == 1, low, 0.0))
     units = weight_ref.shape[1]
-    out_ref[:, :, units:] = tile.reshape(parts, rows, LANES).astype(jnp.bfloat16)
-    made = dot(scaled_ref[...], weight_ref[...])
-    out_ref[:, :, :units] = made.reshape(parts, rows, units).astype(jnp.bfloat16)
+    deal(out_ref, slice(units, units + LANES), tile)
+    deal(out_ref, slice(0, units), dot(scaled_ref[...], weight_ref[...]))
 
 
 def widen(parts, residual, scaled, up_weight):
@@ -454,9 +459,12 @@
 
 
 def narrow_kernel(rows_ref, weight_ref, out_ref):
-    rows = rows_ref[...]
-    rows = rows.reshape(rows.shape[0] * rows.shape[1], rows.shape[2])
-    out_ref[...] = dot(rows, weight_ref[...]).astype(jnp.bfloat16)
+    parts, rows, width = rows_ref.shape
+    made = dot(rows_ref[...].reshape(parts * rows, width), weight_ref[...])
+    order = exchange_order(parts)
+    slots = [order.index(place) for place in range(parts)]
+    pieces = [made[slot * rows : (slot + 1) * rows] for slot in slots]
+    out_ref[...] = jnp.concatenate(pieces, axis=0).astype(jnp.bfloat16)
 
 
 def narrow(rows, weight, name):
@@ -471,7 +479,8 @@
 
 
 def swap_over_kv(payload):
-    return lax.all_to_all(payload, "kv", 0, 0, tiled=True)
+    groups = [exchange_order(payload.shape[0])]
+    return lax.all_to_all(payload, "kv", 0, 0, axis_index_groups=groups, tiled=True)
 
 
 def over_tp(mine):

time: 66 us -> 61 us (0.924)
  blocking collectives: 35.4 us -> 31.5 us
  waiting for transfers between devices: 5.65 us -> 3.45 us
  starting transfers between devices: 11.1 us -> 12.2 us
    all_to_all x3, blocking collectives: 35.4 us -> 31.5 us  [swap_over_kv(): lax.all_to_all(payload, 'kv', 0, 0, axis_index_groups=groups, tiled=True)]
    all_to_all x1, waiting for transfers between devices: 2.71 us -> 0.62 us  [swap_over_kv(): lax.all_to_all(payload, 'kv', 0, 0, axis_index_groups=groups, tiled=True)]
    all_to_all x1, starting transfers between devices: 7.3 us -> 8.33 us  [swap_over_kv(): lax.all_to_all(payload, 'kv', 0, 0, axis_index_groups=groups, tiled=True)]
  transfers between devices with their start and end apart: 7 -> 7, of which waited for: 4 -> 4; matrix products, arithmetic and copies ran while one was open for 0% -> 0% of each run, Pallas kernels for 12% -> 13%
where the time goes in v5:
time: 61 us; the launch traced here: 60.7 us
  blocking collectives  31.5 us (52%)
  starting transfers between devices  12.2 us (20%)
  Pallas kernels  12.1 us (20%)
  waiting for transfers between devices  3.45 us (6%)
  between operations  0.76 us (1%)
  other arithmetic  0.67 us (1%)
    all_to_all x3, blocking collectives, swap_over_kv(): lax.all_to_all(payload, 'kv', 0, 0, axis_index_groups=groups, tiled=True)  31.5 us
    all_to_all x1, starting transfers between devices, swap_over_kv(): lax.all_to_all(payload, 'kv', 0, 0, axis_index_groups=groups, tiled=True)  8.33 us
    pallas_call x1, Pallas kernels, block_state(): pl.pallas_call(functools.partial(block_kernel, heads=heads, pack=pack), i...  6.52 us
    ppermute x6, starting transfers between devices, over_tp(): parts.append(lax.ppermute(mine, 'tp', swaps))  3.83 us
    ppermute x6, waiting for transfers between devices, over_tp(): parts.append(lax.ppermute(mine, 'tp', swaps))  2.83 us
    pallas_call x1, Pallas kernels, project(): pl.pallas_call(functools.partial(project_kernel, count=count, extras=len(...  2.62 us
    pallas_call x1, Pallas kernels, refresh(): pl.pallas_call(refresh_kernel, in_specs=[in_vmem()] * 4, out_specs=pl.Blo...  1.51 us
  transfers between devices with their start and end apart: 7, of which 4 were waited for; matrix products, arithmetic and copies ran while one was open for 0% of the time, Pallas kernels for 13%

profile of v5, /device:TPU:0, one launch (start us, length us, event | category | flops | bytes accessed | tf_op | source)
XLA Modules:
  0.0 60.7 jit_solution(10120984413962542520)
XLA Ops:
  0.6 0.0 copy-start.2
  0.6 0.0 copy-start.3
  0.7 2.6 %project.1 = (bf16[8,8,2176]{2,1,0:T(8,128)(2,1)}, bf16[64,256]{1,0:T(8,128)(2,1)S(1)}, f32[1,256]{1,0:T(1,128)S(1)}, s32[1,8]{1,0:T(1,128)S(1)}, f32[32,64]{1,0...) custom-call(bf16[64,256]{1,0:T(8,128)(2,1)} %tokens_ref.1, f32[1,256]{1,0:T(1,128)} %bitcast.22, ...), custom_call_target="tpu_custom_call" | custom-call | tf_op jit(solution)/shard_map/project/pallas_call | solution.py:137
  3.3 8.3 %all-to-all-start = ((bf16[8,8,2176]{2,1,0:T(8,128)(2,1)}), bf16[8,8,2176]{2,1,0:T(8,128)(2,1)S(1)}, u32[]{:S(2)}, u32[]{:S(2)}) async-start(bf16[8,8,2176]{2,1,0:T(8,128)(2,1)} %get-tuple-element.16), calls=%async_computation | async-start | bytes 557056 | tf_op jit(solution)/shard_map/all_to_all | solution.py:483
  11.6 0.0 copy-done.2
  11.6 0.0 copy-done.3
  11.6 6.5 %block_state.1.state_ref = f32[32,128,128]{2,1,0:T(8,128)S(1)} custom-call(s32[1,8]{1,0:T(1,128)S(1)} %get-tuple-element.17.live_ref, bf16[32,64,128]{2,1,0:T(8,128)(2,1)S(1)} %bitcast.13, bf16[32,64,128]{2,1,0:T(8,128)(2,1)S(1)} %bitcast.14, f32[32,64]{1,0:T(8,128)S(1)} %get-tuple-element.18.betas_ref, f32[32,64]{1,0:T(8,128)S(1)} %get-tuple-element.19.decays_ref, ...), custom_call_target="tpu_custom_call" | custom-call | flops 60000000 | bytes 5000000 | tf_op jit(solution)/shard_map/block_state/pallas_call | solution.py:269
  18.2 0.0 copy-start
  18.2 0.6 %all-to-all-done.arrived_ref = bf16[8,8,2176]{2,1,0:T(8,128)(2,1)S(1)} async-done(((bf16[8,8,2176]{2,1,0:T(8,128)(2,1)}), bf16[8,8,2176]{2,1,0:T(8,128)(2,1)S(1)}, u32[]{:S(2)}, u32[]{:S(2)}) %all-to-all-start) | async-done | bytes 278560 | tf_op jit(solution)/shard_map/all_to_all | solution.py:483
  18.8 0.0 copy-start.4
  18.8 0.5 newest.1
  19.3 0.0 copy-start.1
  19.3 8.4 %all_to_all.20.rows_ref = bf16[8,8,512]{2,1,0:T(8,128)(2,1)S(1)} all-to-all(bf16[8,8,512]{2,1,0:T(8,128)(2,1)S(1)} %get-tuple-element.21), channel_id=1, replica_groups={{20,0,12,24,4,16,28,8},{21,1,13,25,5,17,29,9},{22,2,14,26,6,18,30,10},{..., dimensions={0} | all-to-all | bytes 131072 | tf_op jit(solution)/shard_map/all_to_all | solution.py:483
  27.7 0.0 copy-done.4
  27.7 0.2 attend.1
  27.9 0.1 collective-permute-start.2
  28.0 1.6 %collective-permute-start.1 = (bf16[64,256]{1,0:T(8,128)(2,1)S(1)}, bf16[64,256]{1,0:T(8,128)(2,1)S(1)}, u32[]{:S(2)}, u32[]{:S(2)}) collective-permute-start(bf16[64,256]{1,0:T(8,128)(2,1)S(1)} %attend.1), channel_id=1, source_target_pairs={{0,2},{1,3},{2,0},{3,1},{4,6},{5,7},{6,4},{7,5},{8,10},{9,11},{10,... | collective-permute-start | bytes 98312 | tf_op jit(solution)/shard_map/ppermute | solution.py:491
  29.6 0.3 collective-permute-start
  29.8 1.7 %collective-permute-done.2 = bf16[64,256]{1,0:T(8,128)(2,1)S(1)} collective-permute-done((bf16[64,256]{1,0:T(8,128)(2,1)S(1)}, bf16[64,256]{1,0:T(8,128)(2,1)S(1)}, u32[]{:S(2)}, u32[]{:S(2)}) %collective-permute-start.2) | collective-permute-done | bytes 32800 | tf_op jit(solution)/shard_map/ppermute | solution.py:491
  31.6 0.4 collective-permute-done.1
  32.0 0.0 collective-permute-done
  32.1 0.0 copy-done
  32.1 0.3 widen.1
  32.4 12.5 %all_to_all.21.arrived_ref = bf16[8,8,2176]{2,1,0:T(8,128)(2,1)S(1)} all-to-all(bf16[8,8,2176]{2,1,0:T(8,128)(2,1)S(1)} %widen.1), channel_id=1, replica_groups={{20,0,12,24,4,16,28,8},{21,1,13,25,5,17,29,9},{22,2,14,26,6,18,30,10},{..., dimensions={0} | all-to-all | bytes 557056 | tf_op jit(solution)/shard_map/all_to_all | solution.py:483
  44.9 0.1 activate.1
  45.0 10.6 %all_to_all.22.rows_ref = bf16[8,8,2048]{2,1,0:T(8,128)(2,1)S(1)} all-to-all(bf16[8,8,2048]{2,1,0:T(8,128)(2,1)S(1)} %activate.1), channel_id=1, replica_groups={{20,0,12,24,4,16,28,8},{21,1,13,25,5,17,29,9},{22,2,14,26,6,18,30,10},{..., dimensions={0} | all-to-all | bytes 524288 | tf_op jit(solution)/shard_map/all_to_all | solution.py:483
  55.6 0.0 copy-done.1
  55.6 0.3 narrow.1
  55.9 0.1 collective-permute-start.5
  56.0 0.1 collective-permute-start.4
  56.1 1.8 %collective-permute-start.3 = (bf16[64,256]{1,0:T(8,128)(2,1)S(1)}, bf16[64,256]{1,0:T(8,128)(2,1)S(1)}, u32[]{:S(2)}, u32[]{:S(2)}) collective-permute-start(bf16[64,256]{1,0:T(8,128)(2,1)S(1)} %narrow.1), channel_id=1, source_target_pairs={{0,1},{1,0},{2,3},{3,2},{4,5},{5,4},{6,7},{7,6},{8,9},{9,8},{10,11... | collective-permute-start | bytes 98312 | tf_op jit(solution)/shard_map/ppermute | solution.py:491
  57.8 1.5 %refresh.1 = f32[8,4,128,128]{3,2,1,0:T(8,128)} custom-call(f32[32,128,128]{2,1,0:T(8,128)S(1)} %block_state.1.state_ref, f32[32,128]{1,0:T(8,128)S(1)} %get-tuple-element.23.update_ref, f32[128,64]{1,0:T(8,128)S(1)} %get-tuple-element.24.columns_ref, f32[32,128]{1,0:T(8,128)S(1)} %get-tuple-element.25.fade_ref), custom_call_target="tpu_custom_call" | custom-call | flops 10000000 | bytes 4000000 | tf_op jit(solution)/shard_map/refresh/pallas_call | solution.py:400
  59.4 0.0 collective-permute-done.5
  59.4 0.6 %collective-permute-done.4 = bf16[64,256]{1,0:T(8,128)(2,1)S(1)} collective-permute-done((bf16[64,256]{1,0:T(8,128)(2,1)S(1)}, bf16[64,256]{1,0:T(8,128)(2,1)S(1)}, u32[]{:S(2)}, u32[]{:S(2)}) %collective-permute-start.4) | collective-permute-done | bytes 32800 | tf_op jit(solution)/shard_map/ppermute | solution.py:491
  60.0 0.0 collective-permute-done.3
  60.0 0.6 %fusion.1 = bf16[64,256]{1,0:T(8,128)(2,1)} fusion(bf16[64,256]{1,0:T(8,128)(2,1)S(1)} %get-tuple-element.27.residual_ref, bf16[64,256]{1,0:T(8,128)(2,1)S(1)} %collective-permute-done.5, bf16[64,256]{1,0:T(8,128)(2,1)S(1)} %collective-permute-done.4, bf16[64,256]{1,0:T(8,128)(2,1)S(1)} %collective-permute-done.3, bf16[64,256]{1,0:T(8,128)(2,1)S(1)} %narrow.1), kind=kLoop, calls=%fused_computation.3 | loop fusion | flops 163840 | bytes 196608 | tf_op jit(solution)/shard_map/convert_element_type | solution.py:549
  (1 shorter events, 0.0 us)
Async XLA Ops:
  0.6 11.0 %copy-start.2 = (bf16[8,4,64,128]{3,2,1,0:T(8,128)(2,1)S(1)}, bf16[8,4,64,128]{3,2,1,0:T(8,128)(2,1)}, u32[]{:S(2)}) copy-start(bf16[8,4,64,128]{3,2,1,0:T(8,128)(2,1)} %param.31) | copy-start | bytes 1572868
  0.6 11.0 %copy-start.3 = (bf16[8,4,64,128]{3,2,1,0:T(8,128)(2,1)S(1)}, bf16[8,4,64,128]{3,2,1,0:T(8,128)(2,1)}, u32[]{:S(2)}) copy-start(bf16[8,4,64,128]{3,2,1,0:T(8,128)(2,1)} %param.32) | copy-start | bytes 1572868
  3.3 15.5 %all-to-all-start = ((bf16[8,8,2176]{2,1,0:T(8,128)(2,1)}), bf16[8,8,2176]{2,1,0:T(8,128)(2,1)S(1)}, u32[]{:S(2)}, u32[]{:S(2)}) async-start(bf16[8,8,2176]{2,1,0:T(8,128)(2,1)} %get-tuple-element.16), calls=%async_computation | async-start | bytes 557056 | tf_op jit(solution)/shard_map/all_to_all | solution.py:483
  18.2 13.9 %copy-start = (bf16[256,2048]{1,0:T(8,128)(2,1)S(1)}, bf16[256,2048]{1,0:T(8,128)(2,1)}, u32[]{:S(2)}) copy-start(bf16[256,2048]{1,0:T(8,128)(2,1)} %weight_ref.4) | copy-start | bytes 3145732
  18.8 9.0 %copy-start.4 = (bf16[512,256]{1,0:T(8,128)(2,1)S(1)}, bf16[512,256]{1,0:T(8,128)(2,1)}, u32[]{:S(2)}) copy-start(bf16[512,256]{1,0:T(8,128)(2,1)} %weight_ref.3) | copy-start | bytes 786436
  19.3 36.3 %copy-start.1 = (bf16[2048,256]{1,0:T(8,128)(2,1)S(1)}, bf16[2048,256]{1,0:T(8,128)(2,1)}, u32[]{:S(2)}) copy-start(bf16[2048,256]{1,0:T(8,128)(2,1)} %weight_ref.5) | copy-start | bytes 3145732
  27.9 3.7 %collective-permute-start.2 = (bf16[64,256]{1,0:T(8,128)(2,1)S(1)}, bf16[64,256]{1,0:T(8,128)(2,1)S(1)}, u32[]{:S(2)}, u32[]{:S(2)}) collective-permute-start(bf16[64,256]{1,0:T(8,128)(2,1)S(1)} %attend.1), channel_id=1, source_target_pairs={{0,3},{1,2},{2,1},{3,0},{4,7},{5,6},{6,5},{7,4},{8,11},{9,10},{10,... | collective-permute-start | bytes 98312 | tf_op jit(solution)/shard_map/ppermute | solution.py:491
  28.0 4.0 %collective-permute-start.1 = (bf16[64,256]{1,0:T(8,128)(2,1)S(1)}, bf16[64,256]{1,0:T(8,128)(2,1)S(1)}, u32[]{:S(2)}, u32[]{:S(2)}) collective-permute-start(bf16[64,256]{1,0:T(8,128)(2,1)S(1)} %attend.1), channel_id=1, source_target_pairs={{0,2},{1,3},{2,0},{3,1},{4,6},{5,7},{6,4},{7,5},{8,10},{9,11},{10,... | collective-permute-start | bytes 98312 | tf_op jit(solution)/shard_map/ppermute | solution.py:491
  29.6 2.4 %collective-permute-start = (bf16[64,256]{1,0:T(8,128)(2,1)S(1)}, bf16[64,256]{1,0:T(8,128)(2,1)S(1)}, u32[]{:S(2)}, u32[]{:S(2)}) collective-permute-start(bf16[64,256]{1,0:T(8,128)(2,1)S(1)} %attend.1), channel_id=1, source_target_pairs={{0,1},{1,0},{2,3},{3,2},{4,5},{5,4},{6,7},{7,6},{8,9},{9,8},{10,11... | collective-permute-start | bytes 98312 | tf_op jit(solution)/shard_map/ppermute | solution.py:491
  55.9 3.5 %collective-permute-start.5 = (bf16[64,256]{1,0:T(8,128)(2,1)S(1)}, bf16[64,256]{1,0:T(8,128)(2,1)S(1)}, u32[]{:S(2)}, u32[]{:S(2)}) collective-permute-start(bf16[64,256]{1,0:T(8,128)(2,1)S(1)} %narrow.1), channel_id=1, source_target_pairs={{0,3},{1,2},{2,1},{3,0},{4,7},{5,6},{6,5},{7,4},{8,11},{9,10},{10,... | collective-permute-start | bytes 98312 | tf_op jit(solution)/shard_map/ppermute | solution.py:491
  56.0 4.0 %collective-permute-start.4 = (bf16[64,256]{1,0:T(8,128)(2,1)S(1)}, bf16[64,256]{1,0:T(8,128)(2,1)S(1)}, u32[]{:S(2)}, u32[]{:S(2)}) collective-permute-start(bf16[64,256]{1,0:T(8,128)(2,1)S(1)} %narrow.1), channel_id=1, source_target_pairs={{0,2},{1,3},{2,0},{3,1},{4,6},{5,7},{6,4},{7,5},{8,10},{9,11},{10,... | collective-permute-start | bytes 98312 | tf_op jit(solution)/shard_map/ppermute | solution.py:491
  56.1 4.0 %collective-permute-start.3 = (bf16[64,256]{1,0:T(8,128)(2,1)S(1)}, bf16[64,256]{1,0:T(8,128)(2,1)S(1)}, u32[]{:S(2)}, u32[]{:S(2)}) collective-permute-start(bf16[64,256]{1,0:T(8,128)(2,1)S(1)} %narrow.1), channel_id=1, source_target_pairs={{0,1},{1,0},{2,3},{3,2},{4,5},{5,4},{6,7},{7,6},{8,9},{9,8},{10,11... | collective-permute-start | bytes 98312 | tf_op jit(solution)/shard_map/ppermute | solution.py:491

commit v6 on v5

--- a/solution.py
+++ b/solution.py
@@ -10,6 +10,7 @@
 MODEL = 2048
 EPS = 1e-06
 LANES = 128
+MEASURED_ORDERS = {8: (5, 7, 1, 4, 6, 3, 0, 2)}
 VMEM = pltpu.VMEM
 SMEM = pltpu.SMEM
 
@@ -50,6 +51,8 @@
 
 
 def exchange_order(parts):
+    if parts in MEASURED_ORDERS:
+        return list(MEASURED_ORDERS[parts])
     stride = 3 if parts % 3 else 1
     return [(parts // 2 + 1 + stride * i) % parts for i in range(parts)]
 

time: 61 us -> 60.3 us (0.989)
  waiting for transfers between devices: 3.45 us -> 2.84 us
    all_to_all x1, waiting for transfers between devices: 0.62 us -> 0.01 us  [swap_over_kv(): lax.all_to_all(payload, 'kv', 0, 0, axis_index_groups=groups, tiled=True)]
  transfers between devices with their start and end apart: 7 -> 7, of which waited for: 4 -> 3; matrix products, arithmetic and copies ran while one was open for 0% -> 0% of each run, Pallas kernels for 13% -> 13%
where the time goes in v6:
time: 60.3 us; the launch traced here: 59.9 us
  blocking collectives  31.4 us (52%)
  starting transfers between devices  12.2 us (20%)
  Pallas kernels  12.1 us (20%)
  waiting for transfers between devices  2.84 us (5%)
  between operations  0.77 us (1%)
  other arithmetic  0.67 us (1%)
    all_to_all x3, blocking collectives, swap_over_kv(): lax.all_to_all(payload, 'kv', 0, 0, axis_index_groups=groups, tiled=True)  31.4 us
    all_to_all x1, starting transfers between devices, swap_over_kv(): lax.all_to_all(payload, 'kv', 0, 0, axis_index_groups=groups, tiled=True)  8.36 us
    pallas_call x1, Pallas kernels, block_state(): pl.pallas_call(functools.partial(block_kernel, heads=heads, pack=pack), i...  6.51 us
    ppermute x6, starting transfers between devices, over_tp(): parts.append(lax.ppermute(mine, 'tp', swaps))  3.84 us
    ppermute x6, waiting for transfers between devices, over_tp(): parts.append(lax.ppermute(mine, 'tp', swaps))  2.83 us
    pallas_call x1, Pallas kernels, project(): pl.pallas_call(functools.partial(project_kernel, count=count, extras=len(...  2.62 us
    pallas_call x1, Pallas kernels, refresh(): pl.pallas_call(refresh_kernel, in_specs=[in_vmem()] * 4, out_specs=pl.Blo...  1.51 us
  transfers between devices with their start and end apart: 7, of which 3 were waited for; matrix products, arithmetic and copies ran while one was open for 0% of the time, Pallas kernels for 13%

profile of v6, /device:TPU:0, one launch (start us, length us, event | category | flops | bytes accessed | tf_op | source)
XLA Modules:
  0.0 59.9 jit_solution(326328605280891550)
XLA Ops:
  0.6 0.0 copy-start.2
  0.6 0.0 copy-start.3
  0.7 2.6 %project.1 = (bf16[8,8,2176]{2,1,0:T(8,128)(2,1)}, bf16[64,256]{1,0:T(8,128)(2,1)S(1)}, f32[1,256]{1,0:T(1,128)S(1)}, s32[1,8]{1,0:T(1,128)S(1)}, f32[32,64]{1,0...) custom-call(bf16[64,256]{1,0:T(8,128)(2,1)} %tokens_ref.1, f32[1,256]{1,0:T(1,128)} %bitcast.22, ...), custom_call_target="tpu_custom_call" | custom-call | tf_op jit(solution)/shard_map/project/pallas_call | solution.py:140
  3.3 8.4 %all-to-all-start = ((bf16[8,8,2176]{2,1,0:T(8,128)(2,1)}), bf16[8,8,2176]{2,1,0:T(8,128)(2,1)S(1)}, u32[]{:S(2)}, u32[]{:S(2)}) async-start(bf16[8,8,2176]{2,1,0:T(8,128)(2,1)} %get-tuple-element.16), calls=%async_computation | async-start | bytes 557056 | tf_op jit(solution)/shard_map/all_to_all | solution.py:486
  11.7 0.0 copy-done.2
  11.7 0.0 copy-done.3
  11.7 6.5 %block_state.1.state_ref = f32[32,128,128]{2,1,0:T(8,128)S(1)} custom-call(s32[1,8]{1,0:T(1,128)S(1)} %get-tuple-element.17.live_ref, bf16[32,64,128]{2,1,0:T(8,128)(2,1)S(1)} %bitcast.13, bf16[32,64,128]{2,1,0:T(8,128)(2,1)S(1)} %bitcast.14, f32[32,64]{1,0:T(8,128)S(1)} %get-tuple-element.18.betas_ref, f32[32,64]{1,0:T(8,128)S(1)} %get-tuple-element.19.decays_ref, ...), custom_call_target="tpu_custom_call" | custom-call | flops 60000000 | bytes 5000000 | tf_op jit(solution)/shard_map/block_state/pallas_call | solution.py:272
  18.2 0.0 copy-start
  18.2 0.0 all-to-all-done.arrived_ref
  18.2 0.0 copy-start.4
  18.2 0.5 newest.1
  18.7 0.0 copy-start.1
  18.7 8.6 %all_to_all.20.rows_ref = bf16[8,8,512]{2,1,0:T(8,128)(2,1)S(1)} all-to-all(bf16[8,8,512]{2,1,0:T(8,128)(2,1)S(1)} %get-tuple-element.21), channel_id=1, replica_groups={{20,28,4,16,24,12,0,8},{21,29,5,17,25,13,1,9},{22,30,6,18,26,14,2,10},{..., dimensions={0} | all-to-all | bytes 131072 | tf_op jit(solution)/shard_map/all_to_all | solution.py:486
  27.4 0.0 copy-done.4
  27.4 0.2 attend.1
  27.6 0.1 collective-permute-start.2
  27.6 1.6 %collective-permute-start.1 = (bf16[64,256]{1,0:T(8,128)(2,1)S(1)}, bf16[64,256]{1,0:T(8,128)(2,1)S(1)}, u32[]{:S(2)}, u32[]{:S(2)}) collective-permute-start(bf16[64,256]{1,0:T(8,128)(2,1)S(1)} %attend.1), channel_id=1, source_target_pairs={{0,2},{1,3},{2,0},{3,1},{4,6},{5,7},{6,4},{7,5},{8,10},{9,11},{10,... | collective-permute-start | bytes 98312 | tf_op jit(solution)/shard_map/ppermute | solution.py:494
  29.2 0.3 collective-permute-start
  29.5 1.7 %collective-permute-done.2 = bf16[64,256]{1,0:T(8,128)(2,1)S(1)} collective-permute-done((bf16[64,256]{1,0:T(8,128)(2,1)S(1)}, bf16[64,256]{1,0:T(8,128)(2,1)S(1)}, u32[]{:S(2)}, u32[]{:S(2)}) %collective-permute-start.2) | collective-permute-done | bytes 32800 | tf_op jit(solution)/shard_map/ppermute | solution.py:494
  31.2 0.4 collective-permute-done.1
  31.7 0.0 collective-permute-done
  31.7 0.0 copy-done
  31.7 0.3 widen.1
  32.0 12.4 %all_to_all.21.arrived_ref = bf16[8,8,2176]{2,1,0:T(8,128)(2,1)S(1)} all-to-all(bf16[8,8,2176]{2,1,0:T(8,128)(2,1)S(1)} %widen.1), channel_id=1, replica_groups={{20,28,4,16,24,12,0,8},{21,29,5,17,25,13,1,9},{22,30,6,18,26,14,2,10},{..., dimensions={0} | all-to-all | bytes 557056 | tf_op jit(solution)/shard_map/all_to_all | solution.py:486
  44.4 0.1 activate.1
  44.5 10.3 %all_to_all.22.rows_ref = bf16[8,8,2048]{2,1,0:T(8,128)(2,1)S(1)} all-to-all(bf16[8,8,2048]{2,1,0:T(8,128)(2,1)S(1)} %activate.1), channel_id=1, replica_groups={{20,28,4,16,24,12,0,8},{21,29,5,17,25,13,1,9},{22,30,6,18,26,14,2,10},{..., dimensions={0} | all-to-all | bytes 524288 | tf_op jit(solution)/shard_map/all_to_all | solution.py:486
  54.9 0.0 copy-done.1
  54.9 0.3 narrow.1
  55.2 0.1 collective-permute-start.5
  55.3 0.3 collective-permute-start.4
  55.6 1.5 %collective-permute-start.3 = (bf16[64,256]{1,0:T(8,128)(2,1)S(1)}, bf16[64,256]{1,0:T(8,128)(2,1)S(1)}, u32[]{:S(2)}, u32[]{:S(2)}) collective-permute-start(bf16[64,256]{1,0:T(8,128)(2,1)S(1)} %narrow.1), channel_id=1, source_target_pairs={{0,1},{1,0},{2,3},{3,2},{4,5},{5,4},{6,7},{7,6},{8,9},{9,8},{10,11... | collective-permute-start | bytes 98312 | tf_op jit(solution)/shard_map/ppermute | solution.py:494
  57.1 1.5 %refresh.1 = f32[8,4,128,128]{3,2,1,0:T(8,128)} custom-call(f32[32,128,128]{2,1,0:T(8,128)S(1)} %block_state.1.state_ref, f32[32,128]{1,0:T(8,128)S(1)} %get-tuple-element.23.update_ref, f32[128,64]{1,0:T(8,128)S(1)} %get-tuple-element.24.columns_ref, f32[32,128]{1,0:T(8,128)S(1)} %get-tuple-element.25.fade_ref), custom_call_target="tpu_custom_call" | custom-call | flops 10000000 | bytes 4000000 | tf_op jit(solution)/shard_map/refresh/pallas_call | solution.py:403
  58.6 0.0 collective-permute-done.5
  58.6 0.6 %collective-permute-done.4 = bf16[64,256]{1,0:T(8,128)(2,1)S(1)} collective-permute-done((bf16[64,256]{1,0:T(8,128)(2,1)S(1)}, bf16[64,256]{1,0:T(8,128)(2,1)S(1)}, u32[]{:S(2)}, u32[]{:S(2)}) %collective-permute-start.4) | collective-permute-done | bytes 32800 | tf_op jit(solution)/shard_map/ppermute | solution.py:494
  59.3 0.0 collective-permute-done.3
  59.3 0.6 %fusion.1 = bf16[64,256]{1,0:T(8,128)(2,1)} fusion(bf16[64,256]{1,0:T(8,128)(2,1)S(1)} %get-tuple-element.27.residual_ref, bf16[64,256]{1,0:T(8,128)(2,1)S(1)} %collective-permute-done.5, bf16[64,256]{1,0:T(8,128)(2,1)S(1)} %collective-permute-done.4, bf16[64,256]{1,0:T(8,128)(2,1)S(1)} %collective-permute-done.3, bf16[64,256]{1,0:T(8,128)(2,1)S(1)} %narrow.1), kind=kLoop, calls=%fused_computation.3 | loop fusion | flops 163840 | bytes 196608 | tf_op jit(solution)/shard_map/convert_element_type | solution.py:552
  (1 shorter events, 0.0 us)
Async XLA Ops:
  0.6 11.0 %copy-start.2 = (bf16[8,4,64,128]{3,2,1,0:T(8,128)(2,1)S(1)}, bf16[8,4,64,128]{3,2,1,0:T(8,128)(2,1)}, u32[]{:S(2)}) copy-start(bf16[8,4,64,128]{3,2,1,0:T(8,128)(2,1)} %param.31) | copy-start | bytes 1572868
  0.6 11.0 %copy-start.3 = (bf16[8,4,64,128]{3,2,1,0:T(8,128)(2,1)S(1)}, bf16[8,4,64,128]{3,2,1,0:T(8,128)(2,1)}, u32[]{:S(2)}) copy-start(bf16[8,4,64,128]{3,2,1,0:T(8,128)(2,1)} %param.32) | copy-start | bytes 1572868
  3.3 14.9 %all-to-all-start = ((bf16[8,8,2176]{2,1,0:T(8,128)(2,1)}), bf16[8,8,2176]{2,1,0:T(8,128)(2,1)S(1)}, u32[]{:S(2)}, u32[]{:S(2)}) async-start(bf16[8,8,2176]{2,1,0:T(8,128)(2,1)} %get-tuple-element.16), calls=%async_computation | async-start | bytes 557056 | tf_op jit(solution)/shard_map/all_to_all | solution.py:486
  18.2 13.5 %copy-start = (bf16[256,2048]{1,0:T(8,128)(2,1)S(1)}, bf16[256,2048]{1,0:T(8,128)(2,1)}, u32[]{:S(2)}) copy-start(bf16[256,2048]{1,0:T(8,128)(2,1)} %weight_ref.4) | copy-start | bytes 3145732
  18.2 9.2 %copy-start.4 = (bf16[512,256]{1,0:T(8,128)(2,1)S(1)}, bf16[512,256]{1,0:T(8,128)(2,1)}, u32[]{:S(2)}) copy-start(bf16[512,256]{1,0:T(8,128)(2,1)} %weight_ref.3) | copy-start | bytes 786436
  18.7 36.1 %copy-start.1 = (bf16[2048,256]{1,0:T(8,128)(2,1)S(1)}, bf16[2048,256]{1,0:T(8,128)(2,1)}, u32[]{:S(2)}) copy-start(bf16[2048,256]{1,0:T(8,128)(2,1)} %weight_ref.5) | copy-start | bytes 3145732
  27.6 3.7 %collective-permute-start.2 = (bf16[64,256]{1,0:T(8,128)(2,1)S(1)}, bf16[64,256]{1,0:T(8,128)(2,1)S(1)}, u32[]{:S(2)}, u32[]{:S(2)}) collective-permute-start(bf16[64,256]{1,0:T(8,128)(2,1)S(1)} %attend.1), channel_id=1, source_target_pairs={{0,3},{1,2},{2,1},{3,0},{4,7},{5,6},{6,5},{7,4},{8,11},{9,10},{10,... | collective-permute-start | bytes 98312 | tf_op jit(solution)/shard_map/ppermute | solution.py:494
  27.6 4.0 %collective-permute-start.1 = (bf16[64,256]{1,0:T(8,128)(2,1)S(1)}, bf16[64,256]{1,0:T(8,128)(2,1)S(1)}, u32[]{:S(2)}, u32[]{:S(2)}) collective-permute-start(bf16[64,256]{1,0:T(8,128)(2,1)S(1)} %attend.1), channel_id=1, source_target_pairs={{0,2},{1,3},{2,0},{3,1},{4,6},{5,7},{6,4},{7,5},{8,10},{9,11},{10,... | collective-permute-start | bytes 98312 | tf_op jit(solution)/shard_map/ppermute | solution.py:494
  29.2 2.4 %collective-permute-start = (bf16[64,256]{1,0:T(8,128)(2,1)S(1)}, bf16[64,256]{1,0:T(8,128)(2,1)S(1)}, u32[]{:S(2)}, u32[]{:S(2)}) collective-permute-start(bf16[64,256]{1,0:T(8,128)(2,1)S(1)} %attend.1), channel_id=1, source_target_pairs={{0,1},{1,0},{2,3},{3,2},{4,5},{5,4},{6,7},{7,6},{8,9},{9,8},{10,11... | collective-permute-start | bytes 98312 | tf_op jit(solution)/shard_map/ppermute | solution.py:494
  55.2 3.5 %collective-permute-start.5 = (bf16[64,256]{1,0:T(8,128)(2,1)S(1)}, bf16[64,256]{1,0:T(8,128)(2,1)S(1)}, u32[]{:S(2)}, u32[]{:S(2)}) collective-permute-start(bf16[64,256]{1,0:T(8,128)(2,1)S(1)} %narrow.1), channel_id=1, source_target_pairs={{0,3},{1,2},{2,1},{3,0},{4,7},{5,6},{6,5},{7,4},{8,11},{9,10},{10,... | collective-permute-start | bytes 98312 | tf_op jit(solution)/shard_map/ppermute | solution.py:494
  55.3 4.0 %collective-permute-start.4 = (bf16[64,256]{1,0:T(8,128)(2,1)S(1)}, bf16[64,256]{1,0:T(8,128)(2,1)S(1)}, u32[]{:S(2)}, u32[]{:S(2)}) collective-permute-start(bf16[64,256]{1,0:T(8,128)(2,1)S(1)} %narrow.1), channel_id=1, source_target_pairs={{0,2},{1,3},{2,0},{3,1},{4,6},{5,7},{6,4},{7,5},{8,10},{9,11},{10,... | collective-permute-start | bytes 98312 | tf_op jit(solution)/shard_map/ppermute | solution.py:494
  55.6 3.7 %collective-permute-start.3 = (bf16[64,256]{1,0:T(8,128)(2,1)S(1)}, bf16[64,256]{1,0:T(8,128)(2,1)S(1)}, u32[]{:S(2)}, u32[]{:S(2)}) collective-permute-start(bf16[64,256]{1,0:T(8,128)(2,1)S(1)} %narrow.1), channel_id=1, source_target_pairs={{0,1},{1,0},{2,3},{3,2},{4,5},{5,4},{6,7},{7,6},{8,9},{9,8},{10,11... | collective-permute-start | bytes 98312 | tf_op jit(solution)/shard_map/ppermute | solution.py:494

commit v7 on v6

--- a/solution.py
+++ b/solution.py
@@ -76,10 +76,10 @@
 ):
     far, rest = rest[:count], rest[count:]
     far_extras, rest = rest[:extras], rest[extras:]
-    (out_ref, near_tokens_ref, near_mlp_gain_ref), rest = rest[:3], rest[3:]
+    (far_out_ref, near_tokens_ref, near_mlp_gain_ref), rest = rest[:3], rest[3:]
     near_extras, rest = rest[:extras], rest[extras:]
-    (gain_row, beta_rows, decay_rows), rest = rest[:3], rest[3:]
-    near, semaphore = rest[:count], rest[count]
+    (out_ref, gain_row, beta_rows, decay_rows), rest = rest[:4], rest[4:]
+    near, semaphore, leaving = rest[:count], rest[count], rest[count + 1]
     columns = tokens_ref.shape[1]
     part = pl.ds(0 if sliced else lax.axis_index("kv") * columns, columns)
     pairs = [
@@ -119,11 +119,20 @@
     tile = jnp.where(lane == 4 * heads, square_high, tile)
     tile = jnp.where(lane == 4 * heads + 1, square_low, tile)
     width = near[0].shape[1]
-    deal(out_ref, slice(count * width, count * width + LANES), tile)
+    departures = []
+
+    def depart(lanes, value):
+        deal(out_ref, lanes, value)
+        source, target = out_ref.at[:, :, lanes], far_out_ref.at[:, :, lanes]
+        semaphore_here = leaving.at[len(departures)]
+        departures.append(pltpu.make_async_copy(source, target, semaphore_here))
+        departures[-1].start()
+
+    depart(slice(count * width, count * width + LANES), tile)
     for i in range(count):
         copies[4 + i].wait()
-        deal(out_ref, slice(i * width, (i + 1) * width), dot(normed, near[i][...]))
-    for copy in copies[4 + count :]:
+        depart(slice(i * width, (i + 1) * width), dot(normed, near[i][...]))
+    for copy in copies[4 + count :] + departures:
         copy.wait()
 
 
@@ -140,20 +149,24 @@
     return pl.pallas_call(
         functools.partial(project_kernel, count=count, extras=len(extras), sliced=sliced),
         in_specs=[pl.BlockSpec(memory_space=pl.ANY)] * (5 + count + len(extras)),
-        out_specs=[in_vmem()] * (3 + len(extras)),
+        out_specs=[pl.BlockSpec(memory_space=pl.ANY)] + [in_vmem()] * (2 + len(extras)),
         out_shape=[
-            VMEM((parts, batch // parts, count * width + LANES), jnp.bfloat16),
+            pltpu.HBM((parts, batch // parts, count * width + LANES), jnp.bfloat16),
             VMEM((batch, columns), jnp.bfloat16),
             VMEM((1, columns), jnp.float32),
         ]
         + [VMEM(extra.shape, extra.dtype) for extra in extras],
         scratch_shapes=[
+            VMEM((parts, batch // parts, count * width + LANES), jnp.bfloat16),
             VMEM((1, columns), jnp.float32),
             VMEM((heads, columns), jnp.bfloat16),
             VMEM((heads, columns), jnp.bfloat16),
         ]
         + [VMEM((columns, width), jnp.bfloat16)] * count
-        + [pltpu.SemaphoreType.DMA((5 + count + len(extras),))],
+        + [
+            pltpu.SemaphoreType.DMA((5 + count + len(extras),)),
+            pltpu.SemaphoreType.DMA((1 + count,)),
+        ],
         compiler_params=room(4),
         name="project",
     )(

time: 60.3 us -> 60.2 us (level)
  no operation moved by 1% of the time
where the time goes in v7:
time: 60.2 us; the launch traced here: 59.9 us
  blocking collectives  31.3 us (52%)
  starting transfers between devices  12.2 us (20%)
  Pallas kernels  12 us (20%)
  waiting for transfers between devices  2.84 us (5%)
  between operations  0.77 us (1%)
  other arithmetic  0.67 us (1%)
    all_to_all x3, blocking collectives, swap_over_kv(): lax.all_to_all(payload, 'kv', 0, 0, axis_index_groups=groups, tiled=True)  31.3 us
    all_to_all x1, starting transfers between devices, swap_over_kv(): lax.all_to_all(payload, 'kv', 0, 0, axis_index_groups=groups, tiled=True)  8.36 us
    pallas_call x1, Pallas kernels, block_state(): pl.pallas_call(functools.partial(block_kernel, heads=heads, pack=pack), i...  6.53 us
    ppermute x6, starting transfers between devices, over_tp(): parts.append(lax.ppermute(mine, 'tp', swaps))  3.84 us
    ppermute x6, waiting for transfers between devices, over_tp(): parts.append(lax.ppermute(mine, 'tp', swaps))  2.83 us
    pallas_call x1, Pallas kernels, project(): pl.pallas_call(functools.partial(project_kernel, count=count, extras=len(...  2.58 us
    pallas_call x1, Pallas kernels, refresh(): pl.pallas_call(refresh_kernel, in_specs=[in_vmem()] * 4, out_specs=pl.Blo...  1.51 us
  transfers between devices with their start and end apart: 7, of which 3 were waited for; matrix products, arithmetic and copies ran while one was open for 0% of the time, Pallas kernels for 13%

profile of v7, /device:TPU:0, one launch (start us, length us, event | category | flops | bytes accessed | tf_op | source)
XLA Modules:
  0.0 59.9 jit_solution(6137968480391878078)
XLA Ops:
  0.6 0.0 copy-start.2
  0.6 0.0 copy-start.3
  0.7 2.6 %project.1 = (bf16[8,8,2176]{2,1,0:T(8,128)(2,1)}, bf16[64,256]{1,0:T(8,128)(2,1)S(1)}, f32[1,256]{1,0:T(1,128)S(1)}, s32[1,8]{1,0:T(1,128)S(1)}, f32[32,64]{1,0...) custom-call(bf16[64,256]{1,0:T(8,128)(2,1)} %tokens_ref.1, f32[1,256]{1,0:T(1,128)} %bitcast.22, ...), custom_call_target="tpu_custom_call" | custom-call | tf_op jit(solution)/shard_map/project/pallas_call | solution.py:149
  3.2 8.4 %all-to-all-start = ((bf16[8,8,2176]{2,1,0:T(8,128)(2,1)}), bf16[8,8,2176]{2,1,0:T(8,128)(2,1)S(1)}, u32[]{:S(2)}, u32[]{:S(2)}) async-start(bf16[8,8,2176]{2,1,0:T(8,128)(2,1)} %get-tuple-element.16), calls=%async_computation | async-start | bytes 557056 | tf_op jit(solution)/shard_map/all_to_all | solution.py:499
  11.6 0.0 copy-done.2
  11.6 0.0 copy-done.3
  11.6 6.5 %block_state.1.state_ref = f32[32,128,128]{2,1,0:T(8,128)S(1)} custom-call(s32[1,8]{1,0:T(1,128)S(1)} %get-tuple-element.17.live_ref, bf16[32,64,128]{2,1,0:T(8,128)(2,1)S(1)} %bitcast.13, bf16[32,64,128]{2,1,0:T(8,128)(2,1)S(1)} %bitcast.14, f32[32,64]{1,0:T(8,128)S(1)} %get-tuple-element.18.betas_ref, f32[32,64]{1,0:T(8,128)S(1)} %get-tuple-element.19.decays_ref, ...), custom_call_target="tpu_custom_call" | custom-call | flops 60000000 | bytes 5000000 | tf_op jit(solution)/shard_map/block_state/pallas_call | solution.py:285
  18.1 0.0 copy-start
  18.2 0.0 all-to-all-done.arrived_ref
  18.2 0.0 copy-start.4
  18.2 0.5 newest.1
  18.7 0.0 copy-start.1
  18.7 8.6 %all_to_all.20.rows_ref = bf16[8,8,512]{2,1,0:T(8,128)(2,1)S(1)} all-to-all(bf16[8,8,512]{2,1,0:T(8,128)(2,1)S(1)} %get-tuple-element.21), channel_id=1, replica_groups={{20,28,4,16,24,12,0,8},{21,29,5,17,25,13,1,9},{22,30,6,18,26,14,2,10},{..., dimensions={0} | all-to-all | bytes 131072 | tf_op jit(solution)/shard_map/all_to_all | solution.py:499
  27.3 0.0 copy-done.4
  27.3 0.2 attend.1
  27.5 0.1 collective-permute-start.2
  27.6 1.6 %collective-permute-start.1 = (bf16[64,256]{1,0:T(8,128)(2,1)S(1)}, bf16[64,256]{1,0:T(8,128)(2,1)S(1)}, u32[]{:S(2)}, u32[]{:S(2)}) collective-permute-start(bf16[64,256]{1,0:T(8,128)(2,1)S(1)} %attend.1), channel_id=1, source_target_pairs={{0,2},{1,3},{2,0},{3,1},{4,6},{5,7},{6,4},{7,5},{8,10},{9,11},{10,... | collective-permute-start | bytes 98312 | tf_op jit(solution)/shard_map/ppermute | solution.py:507
  29.2 0.3 collective-permute-start
  29.4 1.8 %collective-permute-done.2 = bf16[64,256]{1,0:T(8,128)(2,1)S(1)} collective-permute-done((bf16[64,256]{1,0:T(8,128)(2,1)S(1)}, bf16[64,256]{1,0:T(8,128)(2,1)S(1)}, u32[]{:S(2)}, u32[]{:S(2)}) %collective-permute-start.2) | collective-permute-done | bytes 32800 | tf_op jit(solution)/shard_map/ppermute | solution.py:507
  31.2 0.4 collective-permute-done.1
  31.6 0.0 collective-permute-done
  31.7 0.0 copy-done
  31.7 0.3 widen.1
  32.0 12.4 %all_to_all.21.arrived_ref = bf16[8,8,2176]{2,1,0:T(8,128)(2,1)S(1)} all-to-all(bf16[8,8,2176]{2,1,0:T(8,128)(2,1)S(1)} %widen.1), channel_id=1, replica_groups={{20,28,4,16,24,12,0,8},{21,29,5,17,25,13,1,9},{22,30,6,18,26,14,2,10},{..., dimensions={0} | all-to-all | bytes 557056 | tf_op jit(solution)/shard_map/all_to_all | solution.py:499
  44.4 0.1 activate.1
  44.5 10.3 %all_to_all.22.rows_ref = bf16[8,8,2048]{2,1,0:T(8,128)(2,1)S(1)} all-to-all(bf16[8,8,2048]{2,1,0:T(8,128)(2,1)S(1)} %activate.1), channel_id=1, replica_groups={{20,28,4,16,24,12,0,8},{21,29,5,17,25,13,1,9},{22,30,6,18,26,14,2,10},{..., dimensions={0} | all-to-all | bytes 524288 | tf_op jit(solution)/shard_map/all_to_all | solution.py:499
  54.8 0.0 copy-done.1
  54.8 0.3 narrow.1
  55.1 0.1 collective-permute-start.5
  55.2 0.3 collective-permute-start.4
  55.5 1.5 %collective-permute-start.3 = (bf16[64,256]{1,0:T(8,128)(2,1)S(1)}, bf16[64,256]{1,0:T(8,128)(2,1)S(1)}, u32[]{:S(2)}, u32[]{:S(2)}) collective-permute-start(bf16[64,256]{1,0:T(8,128)(2,1)S(1)} %narrow.1), channel_id=1, source_target_pairs={{0,1},{1,0},{2,3},{3,2},{4,5},{5,4},{6,7},{7,6},{8,9},{9,8},{10,11... | collective-permute-start | bytes 98312 | tf_op jit(solution)/shard_map/ppermute | solution.py:507
  57.0 1.5 %refresh.1 = f32[8,4,128,128]{3,2,1,0:T(8,128)} custom-call(f32[32,128,128]{2,1,0:T(8,128)S(1)} %block_state.1.state_ref, f32[32,128]{1,0:T(8,128)S(1)} %get-tuple-element.23.update_ref, f32[128,64]{1,0:T(8,128)S(1)} %get-tuple-element.24.columns_ref, f32[32,128]{1,0:T(8,128)S(1)} %get-tuple-element.25.fade_ref), custom_call_target="tpu_custom_call" | custom-call | flops 10000000 | bytes 4000000 | tf_op jit(solution)/shard_map/refresh/pallas_call | solution.py:416
  58.6 0.0 collective-permute-done.5
  58.6 0.6 %collective-permute-done.4 = bf16[64,256]{1,0:T(8,128)(2,1)S(1)} collective-permute-done((bf16[64,256]{1,0:T(8,128)(2,1)S(1)}, bf16[64,256]{1,0:T(8,128)(2,1)S(1)}, u32[]{:S(2)}, u32[]{:S(2)}) %collective-permute-start.4) | collective-permute-done | bytes 32800 | tf_op jit(solution)/shard_map/ppermute | solution.py:507
  59.2 0.0 collective-permute-done.3
  59.2 0.6 %fusion.1 = bf16[64,256]{1,0:T(8,128)(2,1)} fusion(bf16[64,256]{1,0:T(8,128)(2,1)S(1)} %get-tuple-element.27.residual_ref, bf16[64,256]{1,0:T(8,128)(2,1)S(1)} %collective-permute-done.5, bf16[64,256]{1,0:T(8,128)(2,1)S(1)} %collective-permute-done.4, bf16[64,256]{1,0:T(8,128)(2,1)S(1)} %collective-permute-done.3, bf16[64,256]{1,0:T(8,128)(2,1)S(1)} %narrow.1), kind=kLoop, calls=%fused_computation.3 | loop fusion | flops 163840 | bytes 196608 | tf_op jit(solution)/shard_map/convert_element_type | solution.py:565
  (1 shorter events, 0.0 us)
Async XLA Ops:
  0.6 11.0 %copy-start.2 = (bf16[8,4,64,128]{3,2,1,0:T(8,128)(2,1)S(1)}, bf16[8,4,64,128]{3,2,1,0:T(8,128)(2,1)}, u32[]{:S(2)}) copy-start(bf16[8,4,64,128]{3,2,1,0:T(8,128)(2,1)} %param.31) | copy-start | bytes 1572868
  0.6 11.0 %copy-start.3 = (bf16[8,4,64,128]{3,2,1,0:T(8,128)(2,1)S(1)}, bf16[8,4,64,128]{3,2,1,0:T(8,128)(2,1)}, u32[]{:S(2)}) copy-start(bf16[8,4,64,128]{3,2,1,0:T(8,128)(2,1)} %param.32) | copy-start | bytes 1572868
  3.2 14.9 %all-to-all-start = ((bf16[8,8,2176]{2,1,0:T(8,128)(2,1)}), bf16[8,8,2176]{2,1,0:T(8,128)(2,1)S(1)}, u32[]{:S(2)}, u32[]{:S(2)}) async-start(bf16[8,8,2176]{2,1,0:T(8,128)(2,1)} %get-tuple-element.16), calls=%async_computation | async-start | bytes 557056 | tf_op jit(solution)/shard_map/all_to_all | solution.py:499
  18.1 13.5 %copy-start = (bf16[256,2048]{1,0:T(8,128)(2,1)S(1)}, bf16[256,2048]{1,0:T(8,128)(2,1)}, u32[]{:S(2)}) copy-start(bf16[256,2048]{1,0:T(8,128)(2,1)} %weight_ref.4) | copy-start | bytes 3145732
  18.2 9.2 %copy-start.4 = (bf16[512,256]{1,0:T(8,128)(2,1)S(1)}, bf16[512,256]{1,0:T(8,128)(2,1)}, u32[]{:S(2)}) copy-start(bf16[512,256]{1,0:T(8,128)(2,1)} %weight_ref.3) | copy-start | bytes 786436
  18.7 36.1 %copy-start.1 = (bf16[2048,256]{1,0:T(8,128)(2,1)S(1)}, bf16[2048,256]{1,0:T(8,128)(2,1)}, u32[]{:S(2)}) copy-start(bf16[2048,256]{1,0:T(8,128)(2,1)} %weight_ref.5) | copy-start | bytes 3145732
  27.5 3.7 %collective-permute-start.2 = (bf16[64,256]{1,0:T(8,128)(2,1)S(1)}, bf16[64,256]{1,0:T(8,128)(2,1)S(1)}, u32[]{:S(2)}, u32[]{:S(2)}) collective-permute-start(bf16[64,256]{1,0:T(8,128)(2,1)S(1)} %attend.1), channel_id=1, source_target_pairs={{0,3},{1,2},{2,1},{3,0},{4,7},{5,6},{6,5},{7,4},{8,11},{9,10},{10,... | collective-permute-start | bytes 98312 | tf_op jit(solution)/shard_map/ppermute | solution.py:507
  27.6 4.0 %collective-permute-start.1 = (bf16[64,256]{1,0:T(8,128)(2,1)S(1)}, bf16[64,256]{1,0:T(8,128)(2,1)S(1)}, u32[]{:S(2)}, u32[]{:S(2)}) collective-permute-start(bf16[64,256]{1,0:T(8,128)(2,1)S(1)} %attend.1), channel_id=1, source_target_pairs={{0,2},{1,3},{2,0},{3,1},{4,6},{5,7},{6,4},{7,5},{8,10},{9,11},{10,... | collective-permute-start | bytes 98312 | tf_op jit(solution)/shard_map/ppermute | solution.py:507
  29.2 2.4 %collective-permute-start = (bf16[64,256]{1,0:T(8,128)(2,1)S(1)}, bf16[64,256]{1,0:T(8,128)(2,1)S(1)}, u32[]{:S(2)}, u32[]{:S(2)}) collective-permute-start(bf16[64,256]{1,0:T(8,128)(2,1)S(1)} %attend.1), channel_id=1, source_target_pairs={{0,1},{1,0},{2,3},{3,2},{4,5},{5,4},{6,7},{7,6},{8,9},{9,8},{10,11... | collective-permute-start | bytes 98312 | tf_op jit(solution)/shard_map/ppermute | solution.py:507
  55.1 3.5 %collective-permute-start.5 = (bf16[64,256]{1,0:T(8,128)(2,1)S(1)}, bf16[64,256]{1,0:T(8,128)(2,1)S(1)}, u32[]{:S(2)}, u32[]{:S(2)}) collective-permute-start(bf16[64,256]{1,0:T(8,128)(2,1)S(1)} %narrow.1), channel_id=1, source_target_pairs={{0,3},{1,2},{2,1},{3,0},{4,7},{5,6},{6,5},{7,4},{8,11},{9,10},{10,... | collective-permute-start | bytes 98312 | tf_op jit(solution)/shard_map/ppermute | solution.py:507
  55.2 4.0 %collective-permute-start.4 = (bf16[64,256]{1,0:T(8,128)(2,1)S(1)}, bf16[64,256]{1,0:T(8,128)(2,1)S(1)}, u32[]{:S(2)}, u32[]{:S(2)}) collective-permute-start(bf16[64,256]{1,0:T(8,128)(2,1)S(1)} %narrow.1), channel_id=1, source_target_pairs={{0,2},{1,3},{2,0},{3,1},{4,6},{5,7},{6,4},{7,5},{8,10},{9,11},{10,... | collective-permute-start | bytes 98312 | tf_op jit(solution)/shard_map/ppermute | solution.py:507
  55.5 3.7 %collective-permute-start.3 = (bf16[64,256]{1,0:T(8,128)(2,1)S(1)}, bf16[64,256]{1,0:T(8,128)(2,1)S(1)}, u32[]{:S(2)}, u32[]{:S(2)}) collective-permute-start(bf16[64,256]{1,0:T(8,128)(2,1)S(1)} %narrow.1), channel_id=1, source_target_pairs={{0,1},{1,0},{2,3},{3,2},{4,5},{5,4},{6,7},{7,6},{8,9},{9,8},{10,11... | collective-permute-start | bytes 98312 | tf_op jit(solution)/shard_map/ppermute | solution.py:507
